TPU v7x, 512 devices: a whole 4x8x8 slice. The times are simulated.
512 devices in a mesh: sp: 64 (over z, y), fs: 4 (over x), tp: 2 (over core).
Axes of the slice: x: 4, y: 8, z: 8, core: 2. Of those that a mesh axis runs over, the one named last changes fastest.
Arguments:
- tokens: bfloat16 [32768, 2048], P(('fs', 'sp'), 'tp'), parts along dimension 0, may hold values from -450 to 450
- documents: int32 [32768], P(('fs', 'sp')), parts along dimension 0, may hold values from 0 to 7, never falling along the last dimension, each value on 1 to 4096 neighbouring positions
- norm_gain: bfloat16 [2048], P('tp'), may hold values from 0.099609375 to 1.8984375
- out_gate_weight: bfloat16 [2048, 1024], P('sp', 'tp'), may hold values from -0.125 to 0.125
- in_gate_weight: bfloat16 [2048, 1024], P('sp', 'tp'), may hold values from -0.125 to 0.125
- value_weight: bfloat16 [2048, 1024], P('sp', 'tp'), may hold values from -0.125 to 0.125
- conv_taps: bfloat16 [3, 1024], P(None, 'tp'), may hold values from -3.5 to 3.5
- state_in_weight: bfloat16 [2048, 1024], P('sp', 'tp'), may hold values from -0.125 to 0.125
- decay_rate: float32 [64, 64], P('tp'), may hold values from 4e-05 to 2.01
- frequency: float32 [64, 64], P('tp'), may hold values from 0 to 32
- step_log: float32 [64], P('tp'), may hold values from -3.9121 to -1.6094
- input_real: float32 [64, 64, 16], P('tp'), may hold values from -1 to 1
- input_imag: float32 [64, 64, 16], P('tp'), may hold values from -1 to 1
- readout_real: float32 [64, 16, 64], P('tp'), may hold values from -0.75 to 0.75
- readout_imag: float32 [64, 16, 64], P('tp'), may hold values from -0.75 to 0.75
- skip_gain: float32 [1024], P('tp'), may hold values from -4 to 4
- conv_out_weight: bfloat16 [1024, 2048], P('tp', 'sp'), may hold values from -0.125 to 0.125
- state_out_weight: bfloat16 [1024, 2048], P('tp', 'sp'), may hold values from -0.125 to 0.125
Outputs:
- mixed: bfloat16 [32768, 2048], P(('fs', 'sp', 'tp')), parts along dimension 0
There are 4 independent parts, one for each index of `fs`. A program takes and returns all parts, laid end to end along the dimension named above; an argument that names none is the same for every part. Nothing has to cross between parts.
All inputs are finite; a program needn't handle non-finite values.
Results may differ from a plain program's by a relative error of at most 0.015.
Values may be sent and summed in bfloat16 or wider, within the bound.
A program may use at most 64 MiB of HBM per device.

v0:
```python
import math

import jax
import jax.numpy as jnp
from jax import lax
from jax.sharding import Mesh
from jax.sharding import PartitionSpec as P

TAPS = 3
SP = ("sp_0", "sp_1")
FS_SP = ("fs", "sp_0", "sp_1")
FS_SP_TP = ("fs", "sp_0", "sp_1", "tp")


EPS = 1e-06


def rows_first(arrays, axis, dims):
    turned = [jnp.moveaxis(a, dim, 0) for a, dim in zip(arrays, dims)]
    widths = [t[0].size for t in turned]
    both = jnp.concatenate([t.reshape(-1, w) for t, w in zip(turned, widths)], axis=1)
    whole = lax.all_gather(both, axis, axis=0, tiled=True)
    parts = jnp.split(whole, [sum(widths[:k]) for k in range(1, len(widths))], axis=1)
    return tuple(
        (
            jnp.moveaxis(b.reshape(-1, *t.shape[1:]), 0, dim)
            for b, t, dim in zip(parts, turned, dims)
        )
    )


def filled_with(array, identity):
    return jax.tree.map(
        lambda part, zero: jnp.zeros_like(part) + jnp.asarray(zero, part.dtype), array, identity
    )


def gathered_once(array, axis):
    leaves = jax.tree.leaves(array)
    sequence = sorted(range(len(leaves)), key=lambda k: -leaves[k].size)
    width = (1, *leaves[sequence[0]].shape)[-1]
    lines = [
        jnp.pad(leaves[k].reshape(-1), (0, -leaves[k].size % width)).reshape(-1, width)
        for k in sequence
    ]
    both, at, found = (lax.all_gather(jnp.concatenate(lines), axis), 0, {})
    for k, line in zip(sequence, lines):
        section = both[:, at : at + len(line)].reshape(len(both), -1)
        found[k] = section[:, : leaves[k].size].reshape(-1, *leaves[k].shape)
        at += len(line)
    numbers = iter(range(len(leaves)))
    return jax.tree.map(lambda _: found[next(numbers)], array)


def entering(array, axes, combine, identity):
    before = start = filled_with(array, identity)
    total = array
    for axis in reversed(axes):
        devices, here = (lax.axis_size(axis), lax.axis_index(axis))
        pieces = gathered_once(total, axis)
        inside, total = (start, start)
        for k in range(devices):
            passed = k < here
            total = combine(total, jax.tree.map(lambda part: part[k], pieces))
            inside = jax.tree.map(lambda new, old: jnp.where(passed, new, old), total, inside)
        before = combine(inside, before)
    return before


def sent_together(arrays, axis, dim, along):
    widths = [a.shape[along] for a in arrays]
    both = jnp.concatenate(arrays, axis=along)
    whole = lax.all_gather(both, axis, axis=dim, tiled=True)
    return tuple(jnp.split(whole, [sum(widths[:k]) for k in range(1, len(widths))], axis=along))


def from_behind(block, axis, distance):
    devices = range(lax.axis_size(axis))
    route = [(i - distance, i) for i in devices if i - distance in devices]
    return lax.ppermute(block, axis, route)


def cut_along(array, dim, devices):
    shape = array.shape
    parts = array.reshape(*shape[:dim], devices, shape[dim] // devices, *shape[dim + 1 :])
    return jnp.moveaxis(parts, dim, 0)


def summed_on_arrival(array, axis, dim):
    devices = lax.axis_size(axis)
    parts = lax.all_to_all(cut_along(array, dim, devices), axis, 0, 0, tiled=True)
    return jnp.sum(parts.astype(jnp.float32), axis=0)


def chain_step(earlier, later):
    dec_real, dec_imag, end_real, end_imag, first_doc, last_doc = earlier
    late_dec_real, late_dec_imag, late_end_real, late_end_imag, late_first, late_last = later
    joined = (late_first == last_doc) | (last_doc < 0.0) | (late_first < 0.0)
    link = joined.astype(jnp.float32)
    carried_real = late_dec_real * end_real - late_dec_imag * end_imag
    carried_imag = late_dec_real * end_imag + late_dec_imag * end_real
    return (
        link * (late_dec_real * dec_real - late_dec_imag * dec_imag),
        link * (late_dec_real * dec_imag + late_dec_imag * dec_real),
        late_end_real + link * carried_real,
        late_end_imag + link * carried_imag,
        jnp.where(first_doc < 0.0, late_first, first_doc),
        jnp.where(late_last < 0.0, last_doc, late_last),
    )


def ssm_constants(decay_rate, frequency, step_log, input_real, input_imag):
    step_size = jnp.exp(step_log)[:, None]
    damping = decay_rate * step_size
    turning = frequency * step_size
    fading = jnp.exp(-damping)
    coef_imag = fading * jnp.sin(turning)
    half_sine = jnp.sin(turning / 2.0)
    less_real = jnp.expm1(-damping) * jnp.cos(turning) - 2.0 * half_sine * half_sine
    denominator = decay_rate * decay_rate + frequency * frequency
    ratio_real = (-less_real * decay_rate + coef_imag * frequency) / denominator
    ratio_imag = (-coef_imag * decay_rate - less_real * frequency) / denominator
    bbar_real = ratio_real[..., None] * input_real - ratio_imag[..., None] * input_imag
    bbar_imag = ratio_real[..., None] * input_imag + ratio_imag[..., None] * input_real
    return (bbar_real, bbar_imag, damping.reshape(-1), turning.reshape(-1))


def block_recurrence(
    damping,
    turning,
    bbar_real,
    bbar_imag,
    driven,
    keep_rows,
    doc_rows,
    carry_real,
    carry_imag,
    readout_real,
    readout_imag,
):
    groups, group_size, state_size = readout_real.shape
    row_count = driven.shape[0]
    block = math.gcd(row_count, 16)
    blocks = row_count // block
    steps = jnp.arange(block, dtype=jnp.float32)
    gap = steps[:, None] - steps[None, :]
    lower = (gap >= 0.0).astype(jnp.float32)
    gap_pos = jnp.maximum(gap, 0.0)[:, :, None]
    pair_fade = jnp.exp(-gap_pos * damping[None, None, :])
    pair_real = pair_fade * jnp.cos(gap_pos * turning[None, None, :])
    pair_imag = pair_fade * jnp.sin(gap_pos * turning[None, None, :])
    lead = (steps + 1.0)[:, None]
    lead_fade = jnp.exp(-lead * damping[None, :])
    lead_real = lead_fade * jnp.cos(lead * turning[None, :])
    lead_imag = lead_fade * jnp.sin(lead * turning[None, :])

    def one_block(carry, pieces):
        start_real, start_imag = carry
        inputs, keeps, docs = pieces
        split_rows = inputs.reshape(block, groups, group_size)
        push_real = jnp.einsum("tgh,gph->tgp", split_rows, bbar_real).reshape(
            block, groups * state_size
        )
        push_imag = jnp.einsum("tgh,gph->tgp", split_rows, bbar_imag).reshape(
            block, groups * state_size
        )
        same = lower * (docs[:, None] == docs[None, :]).astype(jnp.float32)
        weigh_real = same[:, :, None] * pair_real
        weigh_imag = same[:, :, None] * pair_imag
        alive = (keeps[0] * (docs == docs[0]).astype(jnp.float32))[:, None]
        held_real = jnp.sum(
            weigh_real * push_real[None, :, :] - weigh_imag * push_imag[None, :, :], axis=1
        ) + alive * (lead_real * start_real[None, :] - lead_imag * start_imag[None, :])
        held_imag = jnp.sum(
            weigh_real * push_imag[None, :, :] + weigh_imag * push_real[None, :, :], axis=1
        ) + alive * (lead_real * start_imag[None, :] + lead_imag * start_real[None, :])
        result = jnp.einsum(
            "tgp,ghp->tgh", held_real.reshape(block, groups, state_size), readout_real
        )
        result = result - jnp.einsum(
            "tgp,ghp->tgh", held_imag.reshape(block, groups, state_size), readout_imag
        )
        return ((held_real[-1], held_imag[-1]), result.reshape(block, groups * group_size))

    _, outputs = lax.scan(
        one_block,
        (carry_real, carry_imag),
        (
            driven.reshape(blocks, block, -1),
            keep_rows.reshape(blocks, block),
            doc_rows.reshape(blocks, block),
        ),
    )
    return outputs.reshape(row_count, groups * group_size)


def shards(
    tokens,
    documents,
    norm_gain,
    out_gate_weight,
    in_gate_weight,
    value_weight,
    conv_taps,
    state_in_weight,
    decay_rate,
    frequency,
    step_log,
    input_real,
    input_imag,
    readout_real,
    readout_imag,
    skip_gain,
    conv_out_weight,
    state_out_weight,
):
    row_count = tokens.shape[0]
    groups, state_size = decay_rate.shape
    group_size = input_real.shape[2]
    whole, gains = rows_first((tokens, norm_gain), "tp", (1, 0))
    values = whole.astype(jnp.float32)
    scale = lax.rsqrt(jnp.mean(values * values, axis=1, keepdims=True) + EPS)
    normed = (values * scale * gains.astype(jnp.float32)[None, :]).astype(jnp.bfloat16)

    def add_rows(pieces):
        return tuple(
            (jnp.dot(normed, piece, preferred_element_type=jnp.float32) for piece in pieces)
        )

    bbar_real, bbar_imag, damping, turning = ssm_constants(
        decay_rate, frequency, step_log, input_real, input_imag
    )
    doc_float = documents.astype(jnp.float32)
    (driven_sum,) = add_rows((lax.all_gather(state_in_weight, SP, axis=0, tiled=True),))
    driven_wide = driven_sum.astype(jnp.bfloat16).astype(jnp.float32)
    split_rows = driven_wide.reshape(row_count, groups, group_size)
    backward = (row_count - 1 - jnp.arange(row_count)).astype(jnp.float32)[:, None]
    alive = (documents == documents[-1]).astype(jnp.float32)[:, None]
    fading = jnp.exp(-backward * damping[None, :]) * alive
    weigh_real = (fading * jnp.cos(backward * turning[None, :])).reshape(
        row_count, groups, state_size
    )
    weigh_imag = (fading * jnp.sin(backward * turning[None, :])).reshape(
        row_count, groups, state_size
    )
    moment_real = jnp.einsum("tgp,tgh->gph", weigh_real, split_rows)
    moment_imag = jnp.einsum("tgp,tgh->gph", weigh_imag, split_rows)
    end_real = jnp.sum(bbar_real * moment_real - bbar_imag * moment_imag, axis=2).reshape(-1)
    end_imag = jnp.sum(bbar_real * moment_imag + bbar_imag * moment_real, axis=2).reshape(-1)
    whole_doc = (documents[0] == documents[-1]).astype(jnp.float32)
    total_fade = jnp.exp(-row_count * damping) * whole_doc
    element = (
        total_fade * jnp.cos(row_count * turning),
        total_fade * jnp.sin(row_count * turning),
        end_real,
        end_imag,
        doc_float[:1],
        doc_float[-1:],
    )
    identity = (
        jnp.ones_like(end_real),
        jnp.zeros_like(end_real),
        jnp.zeros_like(end_real),
        jnp.zeros_like(end_real),
        jnp.full((1,), -1.0, jnp.float32),
        jnp.full((1,), -1.0, jnp.float32),
    )
    incoming = entering(element, SP, chain_step, identity)
    driven_wide, incoming = (driven_wide, incoming)
    gate_sum, inner_sum, value_sum = add_rows(
        sent_together((out_gate_weight, in_gate_weight, value_weight), SP, 0, 1)
    )
    out_gate = gate_sum.astype(jnp.bfloat16).astype(jnp.float32)
    in_gate = inner_sum.astype(jnp.bfloat16).astype(jnp.float32)
    value = value_sum.astype(jnp.bfloat16).astype(jnp.float32)
    product = (in_gate * value).astype(jnp.bfloat16)
    margin = TAPS - 1
    tail_same = documents[row_count - margin :] == documents[-1]
    tail_rows = jnp.where(
        tail_same[:, None], product[row_count - margin :], jnp.zeros_like(product[:margin])
    )
    rim_rows = from_behind(tail_rows, SP, 1)
    in_dec_real, in_dec_imag, in_real, in_imag, in_first, in_last = incoming
    padded = jnp.concatenate([rim_rows, product], axis=0)
    padded_docs = jnp.concatenate([jnp.broadcast_to(in_last, (margin,)), doc_float], axis=0)
    total = jnp.zeros(product.shape, jnp.float32)
    for index in range(TAPS):
        same_doc = (padded_docs[index : index + row_count] == doc_float).astype(jnp.float32)
        total = (
            total
            + conv_taps[index].astype(jnp.float32)[None, :]
            * padded[index : index + row_count].astype(jnp.float32)
            * same_doc[:, None]
        )
    conv_out = (out_gate * total).astype(jnp.bfloat16)
    link_first = (in_last == doc_float[:1]).astype(jnp.float32)
    keep_rows = jnp.concatenate(
        [link_first, (documents[1:] == documents[:-1]).astype(jnp.float32)], axis=0
    )
    readout = block_recurrence(
        damping,
        turning,
        bbar_real,
        bbar_imag,
        driven_wide,
        keep_rows,
        doc_float,
        in_real,
        in_imag,
        readout_real,
        readout_imag,
    )
    ssm_out = jax.nn.gelu(readout + skip_gain[None, :] * driven_wide, approximate=True).astype(
        jnp.bfloat16
    )
    conv_columns, state_columns = rows_first((conv_out_weight, state_out_weight), SP, (1, 1))
    summed = summed_on_arrival(
        (
            jnp.dot(conv_out, conv_columns, preferred_element_type=jnp.float32)
            + jnp.dot(ssm_out, state_columns, preferred_element_type=jnp.float32)
        ).astype(jnp.bfloat16),
        "tp",
        0,
    )
    return summed.astype(jnp.bfloat16)


def solution(mesh):
    torus = Mesh(
        mesh.devices.reshape(8, 8, mesh.shape["fs"], mesh.shape["tp"]), ("sp_0", "sp_1", "fs", "tp")
    )
    in_specs = (
        P(FS_SP, "tp"),
        P(FS_SP),
        P("tp"),
        P(SP, "tp"),
        P(SP, "tp"),
        P(SP, "tp"),
        P(None, "tp"),
        P(SP, "tp"),
        P("tp", None),
        P("tp", None),
        P("tp"),
        P("tp", None, None),
        P("tp", None, None),
        P("tp", None, None),
        P("tp", None, None),
        P("tp"),
        P("tp", SP),
        P("tp", SP),
    )
    out_specs = P(FS_SP_TP, None)
    return jax.shard_map(
        shards, mesh=torus, in_specs=in_specs, out_specs=out_specs, check_vma=False
    )
```

profile of v0, /device:TPU:1, one launch (start us, length us, event | category | flops | bytes accessed | tf_op | source)
XLA Modules:
  0.0 351.0 jit_solution(8348065107115574287)
XLA Ops:
  6.6 0.7 all-gather.10.cloned.1.call-update
  7.4 1.4 pad_maximum_fusion.3
  8.9 1.4 pad_maximum_fusion.4
  10.3 0.7 reshape.1674
  11.0 1.0 pad_maximum_fusion
  12.0 8.7 %all_gather.24 = bf16[2048,129]{0,1:T(8,128)(2,1)S(1)} all-gather(bf16[1024,129]{0,1:T(8,128)(2,1)S(1)} %pad_maximum_fusion), channel_id=1, replica_groups=mesh['sp_0'=8,'sp_1'=8,'fs'=4,'tp'=2] {'tp'}, dimensions={0}, use_global_device_ids=true | all-gather | bytes 792576 | tf_op jit(solution)/shard_map/all_gather | solution.py:22
  20.9 0.6 fusion.204
  21.5 0.6 fusion.203
  22.2 0.6 compare_convert_fusion.3
  22.9 0.7 slice_compare_fusion.1
  24.8 0.3 fusion.120
  25.3 0.6 pad.14
  25.8 0.5 pad.15
  26.7 68.4 %all-gather.10.cloned.1.call-done = bf16[2048,512]{1,0:T(8,128)(2,1)} async-done(((bf16[32,512]{1,0:T(8,128)(2,1)}), bf16[2048,512]{1,0:T(8,128)(2,1)}) %all-gather.10.cloned.1.call-update) | async-done | bytes 2097168 | tf_op jit(solution)/shard_map/all_gather | solution.py:234
  95.1 2.1 convolution_convert_fusion
  97.4 3.8 %fusion.79 = f32[32,64,16]{1,2,0:T(8,128)S(1)} fusion(bf16[128,32,16]{0,2,1:T(8,128)(2,1)S(1)} %bitcast.596, f32[32,64]{1,0:T(8,128)S(1)} %get-tuple-element.406, f32[128]{0:T(128)S(1)} %subtract_convert_fusion, f32[128]{0:T(128)S(1)} %get-tuple-element.414, f32[32,64]{1,0:T(8,128)S(1)} %get-tuple-element.405, f32[128]{0:T(128)S(1)} %fusion.178), kind=kOutput, calls=%fused_computation.77 | convolution fusion | flops 9437184 | bytes 280064 | tf_op jit(solution)/shard_map/tgp,tgh->gph/dot_general | solution.py:247
  101.1 4.4 %add_reduce_fusion = (f32[32,64]{1,0:T(8,128)S(1)}, f32[32,64]{1,0:T(8,128)S(1)}) fusion(f32[32,64,16]{1,2,0:T(8,128)S(1)} %get-tuple-element.304, f32[32,64,16]{1,2,0:T(8,128)S(1)} %get-tuple-element.253, f32[32,64,16]{1,2,0:T(8,128)S(1)} %fusion.79, bf16[128,32,16]{0,2,1:T(8,128)(2,1)S(1)} %bitcast.597, f32[32,64]{1,0:T(8,128)S(1)} %get-tuple-element.406, ...), kind=kOutput, calls=%fused_computation.109 | convolution fusion | flops 9695232 | bytes 558592 | tf_op jit(solution)/shard_map/tgp,tgh->gph/dot_general | solution.py:246
  105.8 20.5 %all-gather.2 = f32[8,6,2048]{2,1,0:T(8,128)S(1)} all-gather(f32[1,6,2048]{2,1,0:T(8,128)S(1)} %bitcast.593), channel_id=2, replica_groups=mesh['sp_0'=8,'sp_1'=8,'fs'=4,'tp'=2] {'sp_1'}, dimensions={0}, use_global_device_ids=true | all-gather | bytes 442368 | tf_op jit(solution)/shard_map/all_gather | solution.py:46
  126.4 0.6 fusion.201
  127.0 0.6 fusion.202
  153.2 23.8 %all-gather.3 = f32[8,6,2048]{2,1,0:T(8,128)S(1)} all-gather(f32[1,6,2048]{2,1,0:T(8,128)S(1)} %bitcast.594), channel_id=3, replica_groups=mesh['sp_0'=8,'sp_1'=8,'fs'=4,'tp'=2] {'sp_0'}, dimensions={0}, use_global_device_ids=true | all-gather | bytes 442368 | tf_op jit(solution)/shard_map/all_gather | solution.py:46
  177.2 0.6 fusion.200
  183.1 0.6 fusion.199
  200.0 111.0 %while.16 = (s32[]{:T(128)}, f32[2048]{0:T(1024)S(1)}, f32[2048]{0:T(1024)S(1)}, f32[8,16,512]{2,1,0:T(8,128)S(1)}, f32[8,16]{1,0:T(8,128)S(1)}, /*index=5*/bf16...) while((s32[]{:T(128)}, f32[2048]{0:T(1024)S(1)}, ...), condition=%wide.region_6.7_spmd.clone.clone, body=%wide.region_3.6_spmd.clone.clone.sunk | while | flops 12023074 | bytes 4772677 | solution.py:185
  201.1 9.6 %fusion.233 = (f32[16,2048]{1,0:T(8,128)S(1)}, f32[16,2048]{1,0:T(8,128)S(1)}) fusion(f32[2048]{0:T(1024)S(1)} %get-tuple-element.596, f32[16,16]{1,0:T(8,128)S(1)} %get-tuple-element.597, f32[2048]{0:T(1024)S(1)} %get-tuple-element.594, f32[16,16]{1,0:T(8,128)S(1)} %get-tuple-element.595, f32[16,2048]{1,0:T(8,128)S(1)} %mul.4733, ...), kind=kLoop, calls=%fused_computation.19.clone.1 | loop fusion | flops 7274496 | bytes 543744 | tf_op jit(solution)/shard_map/while/body/eval_jaxpr/reduce_sum | solution.py:174
  211.0 0.6 fusion.234
  212.7 0.6 slice.1072
  213.3 0.6 slice_add_fusion.18
  215.0 9.6 %fusion.233 = (f32[16,2048]{1,0:T(8,128)S(1)}, f32[16,2048]{1,0:T(8,128)S(1)}) fusion(f32[2048]{0:T(1024)S(1)} %get-tuple-element.596, f32[16,16]{1,0:T(8,128)S(1)} %get-tuple-element.597, f32[2048]{0:T(1024)S(1)} %get-tuple-element.594, f32[16,16]{1,0:T(8,128)S(1)} %get-tuple-element.595, f32[16,2048]{1,0:T(8,128)S(1)} %mul.4733, ...), kind=kLoop, calls=%fused_computation.19.clone.1 | loop fusion | flops 7274496 | bytes 543744 | tf_op jit(solution)/shard_map/while/body/eval_jaxpr/reduce_sum | solution.py:174
  224.8 0.6 fusion.234
  226.6 0.6 slice.1072
  227.2 0.6 slice_add_fusion.18
  228.9 9.6 %fusion.233 = (f32[16,2048]{1,0:T(8,128)S(1)}, f32[16,2048]{1,0:T(8,128)S(1)}) fusion(f32[2048]{0:T(1024)S(1)} %get-tuple-element.596, f32[16,16]{1,0:T(8,128)S(1)} %get-tuple-element.597, f32[2048]{0:T(1024)S(1)} %get-tuple-element.594, f32[16,16]{1,0:T(8,128)S(1)} %get-tuple-element.595, f32[16,2048]{1,0:T(8,128)S(1)} %mul.4733, ...), kind=kLoop, calls=%fused_computation.19.clone.1 | loop fusion | flops 7274496 | bytes 543744 | tf_op jit(solution)/shard_map/while/body/eval_jaxpr/reduce_sum | solution.py:174
  238.7 0.6 fusion.234
  240.5 0.6 slice.1072
  241.0 0.6 slice_add_fusion.18
  242.7 9.6 %fusion.233 = (f32[16,2048]{1,0:T(8,128)S(1)}, f32[16,2048]{1,0:T(8,128)S(1)}) fusion(f32[2048]{0:T(1024)S(1)} %get-tuple-element.596, f32[16,16]{1,0:T(8,128)S(1)} %get-tuple-element.597, f32[2048]{0:T(1024)S(1)} %get-tuple-element.594, f32[16,16]{1,0:T(8,128)S(1)} %get-tuple-element.595, f32[16,2048]{1,0:T(8,128)S(1)} %mul.4733, ...), kind=kLoop, calls=%fused_computation.19.clone.1 | loop fusion | flops 7274496 | bytes 543744 | tf_op jit(solution)/shard_map/while/body/eval_jaxpr/reduce_sum | solution.py:174
  252.6 0.6 fusion.234
  254.3 0.6 slice.1072
  254.9 0.6 slice_add_fusion.18
  256.6 9.6 %fusion.233 = (f32[16,2048]{1,0:T(8,128)S(1)}, f32[16,2048]{1,0:T(8,128)S(1)}) fusion(f32[2048]{0:T(1024)S(1)} %get-tuple-element.596, f32[16,16]{1,0:T(8,128)S(1)} %get-tuple-element.597, f32[2048]{0:T(1024)S(1)} %get-tuple-element.594, f32[16,16]{1,0:T(8,128)S(1)} %get-tuple-element.595, f32[16,2048]{1,0:T(8,128)S(1)} %mul.4733, ...), kind=kLoop, calls=%fused_computation.19.clone.1 | loop fusion | flops 7274496 | bytes 543744 | tf_op jit(solution)/shard_map/while/body/eval_jaxpr/reduce_sum | solution.py:174
  266.5 0.6 fusion.234
  268.2 0.6 slice.1072
  268.8 0.6 slice_add_fusion.18
  270.5 9.6 %fusion.233 = (f32[16,2048]{1,0:T(8,128)S(1)}, f32[16,2048]{1,0:T(8,128)S(1)}) fusion(f32[2048]{0:T(1024)S(1)} %get-tuple-element.596, f32[16,16]{1,0:T(8,128)S(1)} %get-tuple-element.597, f32[2048]{0:T(1024)S(1)} %get-tuple-element.594, f32[16,16]{1,0:T(8,128)S(1)} %get-tuple-element.595, f32[16,2048]{1,0:T(8,128)S(1)} %mul.4733, ...), kind=kLoop, calls=%fused_computation.19.clone.1 | loop fusion | flops 7274496 | bytes 543744 | tf_op jit(solution)/shard_map/while/body/eval_jaxpr/reduce_sum | solution.py:174
  280.3 0.6 fusion.234
  282.1 0.6 slice.1072
  282.7 0.6 slice_add_fusion.18
  284.4 9.6 %fusion.233 = (f32[16,2048]{1,0:T(8,128)S(1)}, f32[16,2048]{1,0:T(8,128)S(1)}) fusion(f32[2048]{0:T(1024)S(1)} %get-tuple-element.596, f32[16,16]{1,0:T(8,128)S(1)} %get-tuple-element.597, f32[2048]{0:T(1024)S(1)} %get-tuple-element.594, f32[16,16]{1,0:T(8,128)S(1)} %get-tuple-element.595, f32[16,2048]{1,0:T(8,128)S(1)} %mul.4733, ...), kind=kLoop, calls=%fused_computation.19.clone.1 | loop fusion | flops 7274496 | bytes 543744 | tf_op jit(solution)/shard_map/while/body/eval_jaxpr/reduce_sum | solution.py:174
  294.2 0.6 fusion.234
  296.0 0.6 slice.1072
  296.5 0.6 slice_add_fusion.18
  298.3 9.6 %fusion.233 = (f32[16,2048]{1,0:T(8,128)S(1)}, f32[16,2048]{1,0:T(8,128)S(1)}) fusion(f32[2048]{0:T(1024)S(1)} %get-tuple-element.596, f32[16,16]{1,0:T(8,128)S(1)} %get-tuple-element.597, f32[2048]{0:T(1024)S(1)} %get-tuple-element.594, f32[16,16]{1,0:T(8,128)S(1)} %get-tuple-element.595, f32[16,2048]{1,0:T(8,128)S(1)} %mul.4733, ...), kind=kLoop, calls=%fused_computation.19.clone.1 | loop fusion | flops 7274496 | bytes 543744 | tf_op jit(solution)/shard_map/while/body/eval_jaxpr/reduce_sum | solution.py:174
  308.1 0.6 fusion.234
  309.8 0.6 slice.1072
  310.4 0.6 slice_add_fusion.18
  311.2 2.1 fusion.67
  313.3 2.1 fusion.61
  315.4 2.3 collective-permute-start
  317.9 0.6 collective-permute-done
  318.5 3.4 fusion.32
  322.0 2.4 fusion.30
  324.4 19.2 %all_to_all.5 = bf16[2,64,2048]{2,1,0:T(8,128)(2,1)S(1)} all-to-all(bf16[2,64,2048]{2,1,0:T(8,128)(2,1)S(1)} %bitcast.586), channel_id=1, replica_groups=mesh['sp_0'=8,'sp_1'=8,'fs'=4,'tp'=2] {'tp'}, dimensions={0} | all-to-all | bytes 1048576 | tf_op jit(solution)/shard_map/all_to_all | solution.py:91
  343.6 0.8 reduce_sum.64
  (284 shorter events, 22.9 us)
Async XLA Ops:
  6.5 14.3 %copy-start.7 = (s32[128]{0:T(128)S(1)}, s32[128]{0:T(128)}, u32[]{:S(2)}) copy-start(s32[128]{0:T(128)} %param.21) | copy-start | bytes 1540
  6.5 18.2 %copy-start.9 = (f32[32]{0:T(128)S(1)}, f32[32]{0:T(128)}, u32[]{:S(2)}) copy-start(f32[32]{0:T(128)} %param.30) | copy-start | bytes 388
  6.5 18.3 %copy-start.5 = (f32[32,64]{1,0:T(8,128)S(1)}, f32[32,64]{1,0:T(8,128)}, u32[]{:S(2)}) copy-start(f32[32,64]{1,0:T(8,128)} %param.28) | copy-start | bytes 24580
  6.5 18.3 %copy-start.4 = (f32[32,64]{1,0:T(8,128)S(1)}, f32[32,64]{1,0:T(8,128)}, u32[]{:S(2)}) copy-start(f32[32,64]{1,0:T(8,128)} %param.29) | copy-start | bytes 24580
  6.5 20.0 %copy-start = (f32[32,16,64]{2,1,0:T(8,128)S(1)}, f32[32,16,64]{2,1,0:T(8,128)}, u32[]{:S(2)}) copy-start(f32[32,16,64]{2,1,0:T(8,128)} %param.33) | copy-start | bytes 393220
  6.5 20.0 %copy-start.1 = (f32[32,16,64]{2,1,0:T(8,128)S(1)}, f32[32,16,64]{2,1,0:T(8,128)}, u32[]{:S(2)}) copy-start(f32[32,16,64]{2,1,0:T(8,128)} %param.34) | copy-start | bytes 393220
  6.6 20.0 %copy-start.6 = (bf16[3,512]{1,0:T(4,128)(2,1)S(1)}, bf16[3,512]{1,0:T(4,128)(2,1)}, u32[]{:S(2)}) copy-start(bf16[3,512]{1,0:T(4,128)(2,1)} %param.26) | copy-start | bytes 9220
  6.6 20.1 %copy-start.3 = (f32[32,64,16]{1,2,0:T(8,128)S(1)}, f32[32,64,16]{1,2,0:T(8,128)}, u32[]{:S(2)}) copy-start(f32[32,64,16]{1,2,0:T(8,128)} %param.31) | copy-start | bytes 393220
  6.6 20.1 %copy-start.2 = (f32[32,64,16]{1,2,0:T(8,128)S(1)}, f32[32,64,16]{1,2,0:T(8,128)}, u32[]{:S(2)}) copy-start(f32[32,64,16]{1,2,0:T(8,128)} %param.32) | copy-start | bytes 393220
  6.6 88.6 %all-gather.10.cloned.1.call-start = ((), (), s32[]{:S(2)}) async-start(), calls=%async_computation.2 | async-start | bytes 2129920 | tf_op jit(solution)/shard_map/all_gather | solution.py:234
  7.3 303.9 %all-gather.8.cloned.1.call-start = ((), (), s32[]{:S(2)}) async-start(), calls=%async_computation.1 | async-start | bytes 6389760 | tf_op jit(solution)/shard_map/all_gather | solution.py:73
  8.8 309.1 %all-gather.12.cloned.1.call-start = ((), (), s32[]{:S(2)}) async-start(), calls=%async_computation.3 | async-start | bytes 4259840 | tf_op jit(solution)/shard_map/all_gather | solution.py:22
  200.0 111.0 %copy-start.8 = (f32[512]{0:T(512)S(1)}, f32[512]{0:T(512)}, u32[]{:S(2)}) copy-start(f32[512]{0:T(512)} %param.35) | copy-start | bytes 6148
  315.4 3.1 collective-permute-start
Sparse Core Ops, SparseCore 0:
  10.5 84.6 all-gather.9
  98.2 95.4 all-gather.7
  196.7 79.9 all-gather.11
where the time goes:
time: 353 us; the launch traced here: 351 us
  other arithmetic  96.2 us (27%)
  blocking collectives  72.2 us (20%)
  waiting for transfers between devices  69.8 us (20%)
  between operations  60.3 us (17%)
  matrix products  26.4 us (7%)
  local copies, waits for them, and re-layouts  22.6 us (6%)
    reduce_sum x8, other arithmetic, one_block(): jnp.sum(weigh_real * push_imag[None, :, :] + weigh_imag * push_real[None,...  76.7 us
    all_gather x1, waiting for transfers between devices, shards(): lax.all_gather(state_in_weight, SP, axis=0, tiled=True)  68.4 us
    all_gather x2, blocking collectives, gathered_once(): both, at, found = (lax.all_gather(jnp.concatenate(lines), axis), 0, {})  44.3 us
    all_to_all x1, blocking collectives, summed_on_arrival(): lax.all_to_all(cut_along(array, dim, devices), axis, 0, 0, tiled=True)  19.2 us
    all_gather x1, blocking collectives, rows_first(): whole = lax.all_gather(both, axis, axis=0, tiled=True)  8.67 us
  transfers between devices with their start and end apart: 4, of which 2 were waited for; matrix products, arithmetic and copies ran while one was open for 39% of the time, Pallas kernels for 0%

commit v1 on v0

v1 whole, which is shorter than its diff:
```python
import functools

import jax
import jax.numpy as jnp
from jax import lax
from jax.experimental import pallas as pl
from jax.experimental.pallas import tpu as pltpu
from jax.sharding import Mesh
from jax.sharding import PartitionSpec as P

SP = ("sp_0", "sp_1")
FS_SP = ("fs", "sp_0", "sp_1")
FS_SP_TP = ("fs", "sp_0", "sp_1", "tp")
EPS = 1e-06
PARTS = 4
ROWS = 128
LANES = 128
STATES = 512
ALL = PARTS * ROWS
BF16 = jnp.bfloat16
F32 = jnp.float32


def nn(a, b):
    return jnp.dot(a, b, preferred_element_type=F32)


def nt(a, b):
    return lax.dot_general(a, b, (((1,), (1,)), ((), ())), preferred_element_type=F32)


def ones_where(mask):
    return jnp.where(mask, 1.0, 0.0)


def mixer_kernel(
    nz, ny, depth, tok_in, w_in, doc_in, gain_in, in_ri, read_ri, lam, chan, out,
    tok, gains, docs, wall, wpeer, normed, perm, unperm, bmat, rmat, driven, pushed,
    docext, prodext, gate, ends, chain1, chain2, links, rim_out, rim_in, acts, pacts,
    part, relay, final, local_sem, tok_s, tok_r, d2d_s, d2d_r, doc_s, doc_r, one_s, one_r,
    ph_s, ph_r, st_s, st_r, ring_s, ring_r, ch_s, ch_r, rs_s, rs_r,
):
    z, y = lax.axis_index("sp_0"), lax.axis_index("sp_1")
    x, c = lax.axis_index("fs"), lax.axis_index("tp")
    half = depth // 2
    other = 1 - c
    sent = []

    def wrap(v, n):
        return lax.rem(v + 4 * n, n)

    def send(src, dst, ssem, rsem, **where):
        names = {"z": "sp_0", "y": "sp_1", "x": "fs", "c": "tp"}
        copy = pltpu.make_async_remote_copy(
            src_ref=src, dst_ref=dst, send_sem=ssem, recv_sem=rsem,
            device_id={names[k]: v for k, v in where.items()},
            device_id_type=pl.DeviceIdType.MESH,
        )
        copy.start()
        sent.append(copy)

    def arrived(dst, rsem):
        pltpu.make_async_copy(dst, dst, rsem).wait()

    xp, xm, xo = wrap(x + 1, PARTS), wrap(x - 1, PARTS), wrap(x + 2, PARTS)
    here = z * ny + y
    after, before = wrap(here + 1, nz * ny), wrap(here - 1, nz * ny)
    after_z, after_y = lax.div(after, ny), lax.rem(after, ny)
    before_z, before_y = lax.div(before, ny), lax.rem(before, ny)

    barrier = pltpu.get_barrier_semaphore()
    count = 0

    def greet(**where):
        names = {"z": "sp_0", "y": "sp_1", "x": "fs", "c": "tp"}
        pl.semaphore_signal(
            barrier, inc=1, device_id={names[k]: v for k, v in where.items()},
            device_id_type=pl.DeviceIdType.MESH,
        )
        return 1

    for d in range(1, ny):
        count += greet(y=wrap(y + d, ny))
    for d in range(1, nz):
        count += greet(z=wrap(z + d, nz))
    for v in (xp, xm, xo):
        count += greet(x=v)
    count += greet(c=other)
    count += greet(z=after_z, y=after_y)
    count += greet(z=before_z, y=before_y)

    local = [
        pltpu.make_async_copy(tok_in, tok.at[x, c], local_sem.at[0]),
        pltpu.make_async_copy(w_in, wall.at[z, y], local_sem.at[1]),
        pltpu.make_async_copy(doc_in, docs.at[x], local_sem.at[2]),
        pltpu.make_async_copy(gain_in, gains.at[c], local_sem.at[3]),
    ]
    for copy in local:
        copy.start()
    for copy in local:
        copy.wait()
    pl.semaphore_wait(barrier, count)

    low, high = pl.ds(0, ROWS // 2), pl.ds(ROWS // 2, ROWS // 2)

    def token_send(block, rows, way):
        ref = tok.at[block, c, rows]
        return ref, (xp if way == 0 else xm)

    def token_start(block, rows, way, turn):
        ref, target = token_send(block, rows, way)
        send(ref, ref, tok_s.at[way, turn], tok_r.at[way, turn], x=target)

    def token_wait(block, rows, way, turn):
        arrived(tok.at[block, c, rows], tok_r.at[way, turn])

    def pass_over(block, turn):
        ref = tok.at[block, c]
        send(ref, ref, d2d_s.at[turn], d2d_r.at[turn], c=other)

    def passed_over(block, turn):
        arrived(tok.at[block, other], d2d_r.at[turn])

    for turn, v in enumerate((xp, xm, xo)):
        send(docs.at[x], docs.at[x], doc_s.at[turn], doc_r.at[turn], x=v)
    send(gains.at[c], gains.at[c], one_s.at[0], one_r.at[0], c=other)
    token_start(x, low, 0, 0)
    token_start(x, high, 1, 0)
    rows_a, rows_b = pl.ds(0, half), pl.ds(half, half)
    for d in range(1, ny):
        ref = wall.at[z, y, rows_a]
        send(ref, ref, ph_s.at[0, d], ph_r.at[0, d], y=wrap(y + d, ny))
    for d in range(1, nz):
        ref = wall.at[z, y, rows_b]
        send(ref, ref, ph_s.at[1, d], ph_r.at[1, d], z=wrap(z + d, nz))
    token_start(x, high, 0, 1)
    token_start(x, low, 1, 1)
    pass_over(x, 0)

    shape = (ALL, ALL)
    r, n = lax.broadcasted_iota(jnp.int32, shape, 0), lax.broadcasted_iota(jnp.int32, shape, 1)
    natural = (r & 3) * ROWS + ((r >> 2) & 7) * 16 + (r >> 5)
    perm[...] = ones_where(n == natural).astype(BF16)
    t = (r >> 8) * (ROWS // 2) + (r & 63)
    turned = (t & 15) * 32 + (t >> 4) * 4 + ((r >> 6) & 3)
    unperm[...] = ones_where(n == turned).astype(BF16)
    spread = ones_where(
        (lax.broadcasted_iota(jnp.int32, (16, LANES), 1) & 15)
        == lax.broadcasted_iota(jnp.int32, (16, LANES), 0)
    ).astype(BF16)
    own_group = ones_where(
        (lax.broadcasted_iota(jnp.int32, (STATES, LANES), 0) >> 6)
        == (lax.broadcasted_iota(jnp.int32, (STATES, LANES), 1) >> 4)
    )
    for k in range(2):
        bmat[k * STATES : (k + 1) * STATES] = (nn(in_ri[k].astype(BF16), spread) * own_group).astype(BF16)
    spread_p = ones_where(
        (lax.broadcasted_iota(jnp.int32, (64, STATES), 1) & 63)
        == lax.broadcasted_iota(jnp.int32, (64, STATES), 0)
    ).astype(BF16)
    own_state = ones_where(
        (lax.broadcasted_iota(jnp.int32, (LANES, STATES), 0) >> 4)
        == (lax.broadcasted_iota(jnp.int32, (LANES, STATES), 1) >> 6)
    )
    for k in range(2):
        rmat[:, k * STATES : (k + 1) * STATES] = (nn(read_ri[k].astype(BF16), spread_p) * own_state).astype(BF16)

    def ring_ref(ab, source, lanes, piece):
        count = (ny, nz)[ab]
        cut = {0: pl.ds(0, count), 1: pl.ds(0, count // 2), 2: pl.ds(count // 2, count // 2)}[piece]
        if ab == 0:
            return wall.at[source, cut, rows_a, lanes]
        return wall.at[cut, source, rows_b, lanes]

    lanes_of = (pl.ds(LANES, 3 * LANES), pl.ds(4 * LANES, 2 * LANES))

    def ring_piece(ab, k, way):
        size = (nz, ny)[ab]
        return 0 if k < size // 2 - 1 else 1 + way

    def ring_start(which, k):
        for ab in range(2):
            me, size = ((z, nz), (y, ny))[ab]
            if k >= size // 2:
                continue
            for way in range(2):
                sign = 1 - 2 * way
                ref = ring_ref(ab, wrap(me - sign * k, size), lanes_of[which], ring_piece(ab, k, way))
                target = wrap(me + sign, size)
                send(
                    ref, ref, ring_s.at[which, ab, way, k], ring_r.at[which, ab, way, k],
                    **{"zy"[ab]: target},
                )

    def ring_wait(which, k):
        for ab in range(2):
            me, size = ((z, nz), (y, ny))[ab]
            if k >= size // 2:
                continue
            for way in range(2):
                sign = 1 - 2 * way
                ref = ring_ref(ab, wrap(me - sign * (k + 1), size), lanes_of[which], ring_piece(ab, k, way))
                arrived(ref, ring_r.at[which, ab, way, k])

    token_wait(xm, low, 0, 0)
    token_start(xm, low, 0, 2)
    token_wait(xp, high, 1, 0)
    token_start(xp, high, 1, 2)

    first_lanes = pl.ds(0, LANES)
    for d in range(1, ny):
        arrived(wall.at[z, wrap(y - d, ny), rows_a], ph_r.at[0, d])
    for d in range(1, nz):
        ref = wall.at[z, :, rows_a, first_lanes]
        send(ref, ref, st_s.at[0, d], st_r.at[0, d], z=wrap(z + d, nz))
    for d in range(1, nz):
        arrived(wall.at[wrap(z - d, nz), y, rows_b], ph_r.at[1, d])
    for d in range(1, ny):
        ref = wall.at[:, y, rows_b, first_lanes]
        send(ref, ref, st_s.at[1, d], st_r.at[1, d], y=wrap(y + d, ny))
    ring_start(0, 0)
    ring_start(1, 0)

    arrived(gains.at[other], one_r.at[0])
    g_low, g_high = gains[0], gains[1]
    width = 2 * tok.shape[3]

    def norm(block):
        def some_rows(i, carry):
            rows = pl.ds(pl.multiple_of(i * 32, 32), 32)
            a, b = tok[block, 0, rows, :].astype(F32), tok[block, 1, rows, :].astype(F32)
            mean = (jnp.sum(a * a, axis=1, keepdims=True) + jnp.sum(b * b, axis=1, keepdims=True)) / width
            scale = lax.rsqrt(mean + EPS)
            target = pl.ds(pl.multiple_of(block * ROWS + i * 32, 32), 32)
            normed[target, : width // 2] = (a * scale * g_low).astype(BF16)
            normed[target, width // 2 :] = (b * scale * g_high).astype(BF16)
            return carry

        lax.fori_loop(0, ROWS // 32, some_rows, 0)

    passed_over(x, 0)
    norm(x)
    token_wait(xm, high, 0, 1)
    pass_over(xm, 1)
    token_wait(xp, low, 1, 1)
    pass_over(xp, 2)
    ring_wait(0, 0)
    ring_start(0, 1)
    passed_over(xm, 1)
    norm(xm)
    passed_over(xp, 2)
    norm(xp)
    ring_wait(1, 0)
    ring_start(1, 1)
    token_wait(xo, low, 0, 2)
    token_wait(xo, high, 1, 2)
    pass_over(xo, 3)

    for turn, v in enumerate((xm, xp, xo)):
        arrived(docs.at[v], doc_r.at[turn])
    row = lax.broadcasted_iota(jnp.int32, (ALL, ROWS), 0)
    lane = lax.broadcasted_iota(jnp.int32, (ALL, ROWS), 1)
    pick_t = ones_where(lane == ((row >> 2) & 7) * 16 + (row >> 5))
    part_row = lax.broadcasted_iota(jnp.int32, (ROWS, ROWS), 0)
    spread_docs = jnp.zeros((ROWS, ROWS), F32)
    for q in range(PARTS):
        spread_docs = jnp.where(part_row == q, docs[q], spread_docs)
    by_part = nt(pick_t.astype(BF16), spread_docs.astype(BF16))
    by_part = by_part * ones_where(lane == (row & 3))
    docext[64:] = nn(by_part.astype(BF16), jnp.ones((ROWS, LANES), BF16))
    docext[4:32] = docext[64 + 448 : 64 + 476]
    docext[36:64] = docext[64 + 480 : 64 + 508]

    passed_over(xo, 3)
    norm(xo)
    ring_wait(0, 1)
    ring_start(0, 2)

    for d in range(1, nz):
        arrived(wall.at[wrap(z - d, nz), :, rows_a, first_lanes], st_r.at[0, d])
    for d in range(1, ny):
        arrived(wall.at[:, wrap(y - d, ny), rows_b, first_lanes], st_r.at[1, d])
    total_depth = nz * ny * depth
    state_in = wall[:, :, :, :LANES].reshape(total_depth, LANES)
    in_order = nn(perm[...], nn(normed[...], state_in).astype(BF16))
    driven[...] = in_order
    pushed[...] = nt(in_order.astype(BF16), bmat[...])

    def lane_cut(k):
        return slice(k * LANES, (k + 1) * LANES), slice(STATES + k * LANES, STATES + (k + 1) * LANES)

    def rows_at(k):
        return slice(k * 32, (k + 1) * 32)

    def docs_at(k):
        return docext[64 + k * 32 : 96 + k * 32]

    for cut in range(STATES // LANES):
        re, im = lane_cut(cut)
        a_re, a_im = lam[0:1, re], lam[1:2, re]
        s_re, s_im = pushed[0:32, re], pushed[0:32, im]
        for k in range(1, 16):
            keep = ones_where(docs_at(k) == docs_at(k - 1))
            s_re, s_im = (
                pushed[rows_at(k), re] + keep * (a_re * s_re - a_im * s_im),
                pushed[rows_at(k), im] + keep * (a_re * s_im + a_im * s_re),
            )
            pushed[rows_at(k), re] = s_re
            pushed[rows_at(k), im] = s_im
    for seg in range(8):
        rows = slice(480 + seg * 4, 484 + seg * 4)
        ends[seg, 0:4, :STATES] = pushed[rows, :STATES]
        ends[seg, 4:8, :STATES] = pushed[rows, STATES:]
        last = docext[544 + seg * 4 : 548 + seg * 4]
        ends[seg, 0:4, STATES:] = last
        ends[seg, 4:8, STATES:] = last

    sign = jnp.where(lax.broadcasted_iota(jnp.int32, (8, STATES), 0) < 4, -1.0, 1.0)

    def joined(carry, piece, power):
        held, doc = carry
        now = piece[:, STATES:]
        link = ones_where(now == doc)
        link = jnp.concatenate([link] * (STATES // LANES), axis=1)
        a_re, a_im = lam[2 * power : 2 * power + 1, :], lam[2 * power + 1 : 2 * power + 2, :]
        moved = a_re * held + (a_im * sign) * pltpu.roll(held, 4, 0)
        return piece[:, :STATES] + link * moved, now

    def fold(carry, pieces, count, limit, power):
        def step(k, carry):
            new = joined(carry, pieces[k], power)
            return tuple(jnp.where(k < limit, a, b) for a, b in zip(new, carry))

        return lax.fori_loop(0, count, step, carry)

    nothing = (jnp.zeros((8, STATES), F32), jnp.full((8, LANES), -1.0, F32))
    end, end_doc = fold(nothing, ends, 8, 8, 1)
    chain1[y, :, :STATES] = end
    chain1[y, :, STATES:] = end_doc
    ring_wait(1, 1)
    ring_start(1, 2)
    for d in range(1, ny):
        send(chain1.at[y], chain1.at[y], ch_s.at[0, d], ch_r.at[0, d], y=wrap(y + d, ny))

    for k in range(2, max(nz, ny) // 2):
        ring_wait(0, k)
        ring_start(0, k + 1)
    if max(nz, ny) // 2 <= 2:
        pass
    conv_in = wall[:, :, :, LANES : 4 * LANES].reshape(total_depth, 3 * LANES)
    projected = nn(perm[...], nn(normed[...], conv_in).astype(BF16))
    gate[...] = projected[:, :LANES]
    prodext[64:] = (projected[:, LANES : 2 * LANES] * projected[:, 2 * LANES :]).astype(BF16).astype(F32)
    prodext[4:32] = prodext[64 + 448 : 64 + 476]
    prodext[36:64] = prodext[64 + 480 : 64 + 508]
    rim_out[0:4, :LANES] = prodext[64 + 476 : 64 + 480]
    rim_out[4:8, :LANES] = prodext[64 + 508 : 64 + 512]
    rim_out[0:4, LANES:] = docext[64 + 476 : 64 + 480]
    rim_out[4:8, LANES:] = docext[64 + 508 : 64 + 512]

    for d in range(1, ny):
        arrived(chain1.at[wrap(y - d, ny)], ch_r.at[0, d])
    end, end_doc = fold(nothing, chain1, ny, ny, 2)
    chain2[z, :, :STATES] = end
    chain2[z, :, STATES:] = end_doc
    send(rim_out, rim_in, one_s.at[1], one_r.at[1], z=after_z, y=after_y)
    for d in range(1, nz):
        send(chain2.at[z], chain2.at[z], ch_s.at[1, d], ch_r.at[1, d], z=wrap(z + d, nz))

    for k in range(2, max(nz, ny) // 2):
        ring_wait(1, k)
        ring_start(1, k + 1)
    out_lanes = lanes_of[1]
    send(wall.at[:, :, :, out_lanes], wpeer, one_s.at[2], one_r.at[2], c=other)

    arrived(rim_in, one_r.at[1])
    first = here == 0
    prodext[0:4] = rim_in[0:4, :LANES]
    prodext[32:36] = rim_in[4:8, :LANES]
    docext[0:4] = jnp.where(first, -1.0, rim_in[0:4, LANES:])
    docext[32:36] = jnp.where(first, -1.0, rim_in[4:8, LANES:])
    now = docext[64:]
    mixed = (
        chan[0:1] * prodext[0:ALL] * ones_where(docext[0:ALL] == now)
        + chan[1:2] * prodext[32 : 32 + ALL] * ones_where(docext[32 : 32 + ALL] == now)
        + chan[2:3] * prodext[64:]
    )
    conv_out = (gate[...] * mixed).astype(BF16)
    acts[:, :LANES] = nn(unperm[...], conv_out).astype(BF16)
    mine, theirs = (pl.ds(pl.multiple_of(v * (ALL // 2), ALL // 2), ALL // 2) for v in (c, other))
    conv_lanes, ssm_lanes = pl.ds(0, LANES), pl.ds(LANES, LANES)

    for d in range(1, nz):
        arrived(chain2.at[wrap(z - d, nz)], ch_r.at[1, d])
    send(acts.at[theirs, conv_lanes], pacts.at[:, conv_lanes], one_s.at[3], one_r.at[3], c=other)
    state = fold(nothing, chain2, nz, z, 3)
    state = fold(state, chain1, ny, y, 2)
    for seg in range(8):
        links[seg] = state[0]
        state = joined(state, ends[seg], 1)
    for seg in range(8):
        rim_state = slice(seg * 4, seg * 4 + 4)
        links[8 + seg // 2, (seg % 2) * 4 : (seg % 2) * 4 + 4] = links[seg, 0:4]
        links[12 + seg // 2, (seg % 2) * 4 : (seg % 2) * 4 + 4] = links[seg, 4:8]
    previous = docext[32:64]
    for cut in range(STATES // LANES):
        re, im = lane_cut(cut)
        a_re, a_im = lam[0:1, re], lam[1:2, re]
        w_re = links[8:12, :, re].reshape(32, LANES)
        w_im = links[12:16, :, re].reshape(32, LANES)
        for k in range(16):
            w_re, w_im = a_re * w_re - a_im * w_im, a_re * w_im + a_im * w_re
            reach = ones_where(docs_at(k) == previous)
            pushed[rows_at(k), re] = pushed[rows_at(k), re] + reach * w_re
            pushed[rows_at(k), im] = pushed[rows_at(k), im] + reach * w_im
    reading = nt(pushed[...].astype(BF16), rmat[...]) + chan[3:4] * driven[...]
    inner = 0.7978845608028654 * (reading + 0.044715 * (reading * reading * reading))
    ssm_out = (0.5 * reading * (1.0 + jnp.tanh(inner))).astype(BF16)
    acts[:, LANES:] = nn(unperm[...], ssm_out).astype(BF16)
    send(acts.at[theirs, ssm_lanes], pacts.at[:, ssm_lanes], one_s.at[4], one_r.at[4], c=other)

    arrived(wpeer, one_r.at[2])
    arrived(pacts.at[:, conv_lanes], one_r.at[3])
    columns = total_depth // 2
    own_weight = wall.at[:, :, :, out_lanes]
    arrived(pacts.at[:, ssm_lanes], one_r.at[4])
    for h in range(2):
        cut = slice(h * nz // 2, (h + 1) * nz // 2)
        total = nt(acts[mine, :], wall[cut, :, :, 4 * LANES :].reshape(columns, 2 * LANES))
        total = total + nt(pacts[...], wpeer[cut].reshape(columns, 2 * LANES))
        part[h] = total.astype(BF16).reshape(PARTS, ROWS // 2, columns)
        if h == 0:
            send(part.at[0, xo], relay.at[0], rs_s.at[0, 0], rs_r.at[0, 0], x=xp)
            send(part.at[0, xm], final.at[1, 0], rs_s.at[1, 1], rs_r.at[1, 1], x=xm)
        else:
            send(part.at[1, xo], relay.at[1], rs_s.at[1, 0], rs_r.at[1, 0], x=xm)
            send(part.at[1, xp], final.at[0, 1], rs_s.at[0, 1], rs_r.at[0, 1], x=xp)
    arrived(relay.at[0], rs_r.at[0, 0])
    part[0, xp] = (part[0, xp].astype(F32) + relay[0].astype(F32)).astype(BF16)
    send(part.at[0, xp], final.at[0, 0], rs_s.at[0, 2], rs_r.at[0, 2], x=xp)
    arrived(relay.at[1], rs_r.at[1, 0])
    part[1, xm] = (part[1, xm].astype(F32) + relay[1].astype(F32)).astype(BF16)
    send(part.at[1, xm], final.at[1, 1], rs_s.at[1, 2], rs_r.at[1, 2], x=xm)
    for h, turns in ((1, (1, 2)), (0, (2, 1))):
        arrived(final.at[0, h], rs_r.at[0, turns[0]])
        arrived(final.at[1, h], rs_r.at[1, turns[1]])
        value = part[h, x].astype(F32) + final[0, h].astype(F32) + final[1, h].astype(F32)
        out[:, h * columns : (h + 1) * columns] = value.astype(BF16)
    for copy in sent:
        copy.wait_send()


def state_tables(decay_rate, frequency, step_log, input_real, input_imag, lengths):
    step_size = jnp.exp(step_log)[:, None]
    damping = decay_rate * step_size
    turning = frequency * step_size
    fading = jnp.exp(-damping)
    coef_imag = fading * jnp.sin(turning)
    half_sine = jnp.sin(turning / 2.0)
    less_real = jnp.expm1(-damping) * jnp.cos(turning) - 2.0 * half_sine * half_sine
    denominator = decay_rate * decay_rate + frequency * frequency
    ratio_real = (-less_real * decay_rate + coef_imag * frequency) / denominator
    ratio_imag = (-coef_imag * decay_rate - less_real * frequency) / denominator
    bbar_real = ratio_real[..., None] * input_real - ratio_imag[..., None] * input_imag
    bbar_imag = ratio_real[..., None] * input_imag + ratio_imag[..., None] * input_real
    rows = []
    for length in lengths:
        fade = jnp.exp(-length * damping)
        rows += [fade * jnp.cos(length * turning), fade * jnp.sin(length * turning)]
    powers = jnp.stack(rows).reshape(len(rows), -1)
    bbar = jnp.stack([bbar_real, bbar_imag]).reshape(2, -1, input_real.shape[2])
    return powers, bbar


def shards(
    nz, ny, tokens, documents, norm_gain, out_gate_weight, in_gate_weight, value_weight,
    conv_taps, state_in_weight, decay_rate, frequency, step_log, input_real, input_imag,
    readout_real, readout_imag, skip_gain, conv_out_weight, state_out_weight,
):
    x = lax.axis_index("fs")
    depth = state_in_weight.shape[0]
    width = tokens.shape[1]

    def own(array, dim):
        size = array.shape[dim] // PARTS
        return lax.dynamic_slice_in_dim(array, x * size, size, dim)

    weights = jnp.concatenate(
        [own(w, 1) for w in (state_in_weight, out_gate_weight, in_gate_weight, value_weight)]
        + [own(w, 0).T for w in (conv_out_weight, state_out_weight)],
        axis=1,
    )
    powers, bbar = state_tables(
        own(decay_rate, 0), own(frequency, 0), own(step_log, 0), own(input_real, 0),
        own(input_imag, 0), (1.0, 16.0, float(ROWS), float(ROWS * ny)),
    )
    readout = jnp.stack([own(readout_real, 0), -own(readout_imag, 0)]).reshape(2, LANES, -1)
    channels = jnp.concatenate(
        [own(conv_taps, 1).astype(F32), own(skip_gain, 0)[None, :], jnp.zeros((4, LANES), F32)]
    )
    doc_row = documents.astype(F32)[None, :]
    gain_row = norm_gain.astype(F32)[None, :]
    columns = nz * ny * depth // 2
    vmem = pl.BlockSpec(memory_space=pltpu.VMEM)
    anywhere = pl.BlockSpec(memory_space=pl.ANY)
    dma = pltpu.SemaphoreType.DMA
    steps = max(nz, ny) // 2
    most = max(nz, ny)
    return pl.pallas_call(
        functools.partial(mixer_kernel, nz, ny, depth),
        out_shape=jax.ShapeDtypeStruct((ROWS // 2, 2 * columns), BF16),
        in_specs=[anywhere] * 4 + [vmem] * 4,
        out_specs=vmem,
        scratch_shapes=[
            pltpu.VMEM((PARTS, 2, ROWS, width), BF16),
            pltpu.VMEM((2, 1, width), F32),
            pltpu.VMEM((PARTS, 1, ROWS), F32),
            pltpu.VMEM((nz, ny, depth, 6 * LANES), BF16),
            pltpu.VMEM((nz, ny, depth, 2 * LANES), BF16),
            pltpu.VMEM((ALL, 2 * width), BF16),
            pltpu.VMEM((ALL, ALL), BF16),
            pltpu.VMEM((ALL, ALL), BF16),
            pltpu.VMEM((2 * STATES, LANES), BF16),
            pltpu.VMEM((LANES, 2 * STATES), BF16),
            pltpu.VMEM((ALL, LANES), F32),
            pltpu.VMEM((ALL, 2 * STATES), F32),
            pltpu.VMEM((64 + ALL, LANES), F32),
            pltpu.VMEM((64 + ALL, LANES), F32),
            pltpu.VMEM((ALL, LANES), F32),
            pltpu.VMEM((8, 8, STATES + LANES), F32),
            pltpu.VMEM((ny, 8, STATES + LANES), F32),
            pltpu.VMEM((nz, 8, STATES + LANES), F32),
            pltpu.VMEM((16, 8, STATES), F32),
            pltpu.VMEM((8, 2 * LANES), F32),
            pltpu.VMEM((8, 2 * LANES), F32),
            pltpu.VMEM((ALL, 2 * LANES), BF16),
            pltpu.VMEM((ALL // 2, 2 * LANES), BF16),
            pltpu.VMEM((2, PARTS, ROWS // 2, columns), BF16),
            pltpu.VMEM((2, ROWS // 2, columns), BF16),
            pltpu.VMEM((2, 2, ROWS // 2, columns), BF16),
            dma((4,)),
            dma((2, 3)), dma((2, 3)),
            dma((4,)), dma((4,)),
            dma((3,)), dma((3,)),
            dma((5,)), dma((5,)),
            dma((2, most)), dma((2, most)),
            dma((2, most)), dma((2, most)),
            dma((2, 2, 2, steps)), dma((2, 2, 2, steps)),
            dma((2, most)), dma((2, most)),
            dma((2, 3)), dma((2, 3)),
        ],
        compiler_params=pltpu.CompilerParams(
            collective_id=0, has_side_effects=True, vmem_limit_bytes=60 * 1024 * 1024
        ),
        name="mixer",
    )(tokens, weights, doc_row, gain_row, bbar, readout, powers, channels)


def solution(mesh, nz=8, ny=8):
    torus = Mesh(
        mesh.devices.reshape(nz, ny, mesh.shape["fs"], mesh.shape["tp"]), ("sp_0", "sp_1", "fs", "tp")
    )
    in_specs = (
        P(FS_SP, "tp"),
        P(FS_SP),
        P("tp"),
        P(SP, "tp"),
        P(SP, "tp"),
        P(SP, "tp"),
        P(None, "tp"),
        P(SP, "tp"),
        P("tp", None),
        P("tp", None),
        P("tp"),
        P("tp", None, None),
        P("tp", None, None),
        P("tp", None, None),
        P("tp", None, None),
        P("tp"),
        P("tp", SP),
        P("tp", SP),
    )
    return jax.shard_map(
        functools.partial(shards, nz, ny), mesh=torus, in_specs=in_specs,
        out_specs=P(FS_SP_TP, None), check_vma=False,
    )
```

time: 353 us -> 88.2 us (0.25)
  other arithmetic: 96.2 us -> 5.78 us
  blocking collectives: 72.2 us -> 0 us
  Pallas kernels: 0 us -> 72 us
  waiting for transfers between devices: 69.8 us -> 0 us
  between operations: 60.3 us -> 0.06 us
  matrix products: 26.4 us -> 0 us
  local copies, waits for them, and re-layouts: 22.6 us -> 9.4 us
    reduce_sum x10 -> x0, other arithmetic: 77.7 us -> none  [the longest x8 76.7 us: one_block(): jnp.sum(weigh_real * push_imag[None, :, :] + weigh_imag * push_real[None,...]
    pallas_call x0 -> x1, Pallas kernels: none -> 72 us  [shards(): pl.pallas_call(functools.partial(mixer_kernel, nz, ny, depth), out_shape=...]
    all_gather x3 -> x0, waiting for transfers between devices: 68.4 us -> none  [the longest x1 68.4 us: shards(): lax.all_gather(state_in_weight, SP, axis=0, tiled=True)]
    all_gather x3 -> x0, blocking collectives: 52.9 us -> none  [the longest x2 44.3 us: gathered_once(): both, at, found = (lax.all_gather(jnp.concatenate(lines), axis), 0, {})]
    dot_general x39 -> x0, matrix products: 26.4 us -> none  [the longest x3 6.23 us: add_rows(): jnp.dot(normed, piece, preferred_element_type=jnp.float32)]
    all_to_all x1 -> x0, blocking collectives: 19.2 us -> none  [summed_on_arrival(): lax.all_to_all(cut_along(array, dim, devices), axis, 0, 0, tiled=True)]
    slice x18 -> x0, local copies, waits for them, and re-layouts: 8.67 us -> none  [the longest x8 4.61 us: one_block(): held_real[-1]]
    add x28 -> x0, other arithmetic: 6.69 us -> none  [the longest x16 6.05 us: one_block(): jnp.sum(weigh_real * push_imag[None, :, :] + weigh_imag * push_real[None,...]
  transfers between devices with their start and end apart: 4 -> 0, of which waited for: 2 -> 0; matrix products, arithmetic and copies ran while one was open for 39% -> 0% of each run, Pallas kernels for 0% -> 0%
where the time goes in v1:
time: 88.2 us; the launch traced here: 87.3 us
  Pallas kernels  72 us (82%)
  local copies, waits for them, and re-layouts  9.4 us (11%)
  other arithmetic  5.78 us (7%)
    pallas_call x1, Pallas kernels, shards(): pl.pallas_call(functools.partial(mixer_kernel, nz, ny, depth), out_shape=...  72 us
    unnamed x16, local copies, waits for them, and re-layouts  6.04 us

profile of v1, /device:TPU:1, one launch (start us, length us, event | category | flops | bytes accessed | tf_op | source)
XLA Modules:
  0.0 87.3 jit_solution(6222213413697135259)
XLA Ops:
  0.0 0.0 copy-start
  0.0 0.0 copy-start.3
  0.0 0.7 copy-done.3
  0.7 0.0 copy-start.4
  0.7 0.5 convert_bitcast_fusion.doc_in
  1.2 0.1 copy-done.4
  1.3 0.1 dynamic-slice_exponential_fusion
  1.4 0.0 copy-done
  1.4 0.1 dynamic-slice_bitcast_fusion
  1.5 0.1 pad.2.clone
  1.6 0.7 fusion.4
  2.2 0.0 copy-start.2
  2.3 0.7 maximum_maximum_fusion.chan
  2.9 0.0 copy-done.2
  2.9 0.6 broadcast_in_dim.24
  3.5 0.9 sine_multiply_fusion
  4.4 0.1 stack.58
  4.5 0.1 stack.51
  4.5 0.1 stack.52
  4.6 0.1 stack.57
  4.7 0.1 stack.55
  4.8 0.1 stack.53
  4.8 0.1 stack.54
  4.9 0.1 stack.56
  5.0 0.6 stack.59.lam
  5.6 0.7 constant_dynamic-update-slice_fusion.5
  6.3 0.7 constant_dynamic-update-slice_fusion.4
  7.0 0.7 constant_dynamic-update-slice_fusion.3
  7.7 0.7 constant_dynamic-update-slice_fusion.2
  8.4 0.7 constant_dynamic-update-slice_fusion.1
  9.2 0.7 constant_dynamic-update-slice_fusion.w_in
  9.9 0.0 copy-start.1
  9.9 0.9 %multiply_subtract_fusion = (f32[8,64,16]{1,2,0:T(8,128)S(1)}, f32[8,64,16]{1,2,0:T(8,128)S(1)}) fusion(f32[32,64,16]{1,2,0:T(8,128)} %param.30, s32[]{:T(128)S(6)} %select_n.5, f32[32,64,16]{1,2,0:T(8,128)} %param.29, f32[8,64]{1,0:T(8,128)S(1)} %get-tuple-element.9, f32[8,64]{1,0:T(8,128)S(1)} %get-tuple-element.16), kind=kLoop, calls=%fused_computation.4 | loop fusion | flops 49152 | bytes 135172 | tf_op jit(solution)/shard_map/sub | solution.py:464
  10.8 0.0 copy-done.1
  10.8 0.1 stack.45
  10.9 0.1 stack.46
  11.0 0.9 %dynamic-slice_negate_fusion = (f32[8,16,64]{2,1,0:T(8,128)S(1)}, f32[8,16,64]{2,1,0:T(8,128)S(1)}) fusion(f32[32,16,64]{2,1,0:T(8,128)} %param.32, s32[]{:T(128)S(6)} %select_n.5, f32[32,16,64]{2,1,0:T(8,128)} %param.31), kind=kLoop, calls=%fused_computation.2 | loop fusion | flops 8192 | bytes 131076 | tf_op jit(solution)/shard_map/neg | solution.py:497
  11.9 0.7 pad_maximum_fusion.read_ri
  12.6 1.0 %copy.23.in_ri = f32[2,512,16]{2,1,0:T(8,128)} copy(f32[2,512,16]{1,2,0:T(8,128)S(1)} %pad_maximum_fusion.1) | data formatting | bytes 131072 | tf_op jit(solution)/shard_map/stack | solution.py:471
  13.6 72.0 %mixer.1 = bf16[64,2048]{1,0:T(8,128)(2,1)} custom-call(bf16[128,1024]{1,0:T(8,128)(2,1)} %tok_in.1, bf16[32,768]{1,0:T(8,128)(2,1)} %copy-done.1, f32[1,128]{1,0:T(1,128)} %convert_bitcast_fusion.doc_in, f32[1,1024]{1,0:T(1,128)} %bitcast.17, f32[2,512,16]{2,1,0:T(8,128)} %copy.23.in_ri, f32[2,128,64]{2,1,0:T(8,128)} %pad_maximum_fusion.read_ri, ...), custom_call_target="tpu_custom_call" | custom-call | tf_op jit(solution)/shard_map/mixer/pallas_call | solution.py:509
  85.6 1.7 %copy.30 = bf16[64,2048]{1,0:T(8,128)(2,1)} copy(bf16[64,2048]{1,0:T(8,128)(2,1)} %mixer.1) | data formatting | bytes 524288
  (4 shorter events, 0.1 us)
Async XLA Ops:
  0.0 1.4 %copy-start = (f32[512]{0:T(512)S(1)}, f32[512]{0:T(512)}, u32[]{:S(2)}) copy-start(f32[512]{0:T(512)} %param.33) | copy-start | bytes 6148
  0.0 0.7 copy-start.3
  0.7 0.7 copy-start.4
  2.2 0.7 copy-start.2
  9.9 0.9 %copy-start.1 = (bf16[32,768]{1,0:T(8,128)(2,1)}, bf16[32,768]{1,0:T(8,128)(2,1)S(1)}, u32[]{:S(2)}) copy-start(bf16[32,768]{1,0:T(8,128)(2,1)S(1)} %constant_dynamic-update-slice_fusion.w_in) | copy-start | bytes 147460

commit v2 on v1

--- a/solution.py
+++ b/solution.py
@@ -34,8 +34,9 @@
 
 
 def mixer_kernel(
-    nz, ny, depth, tok_in, w_in, doc_in, gain_in, in_ri, read_ri, lam, chan, out,
-    tok, gains, docs, wall, wpeer, normed, perm, unperm, bmat, rmat, driven, pushed,
+    nz, ny, depth, tok_in, w_in_0, w_in_1, w_in_2, w_in_3, w_in_4, w_in_5, doc_in, gain_in,
+    decay_in, freq_in, step_in, in_re, in_im, read_re, read_im, taps_in, skip_in, out,
+    rates, step_row, mats, taps, skip, lam, tok, gains, docs, wall, wpeer, normed, perm, unperm, bmat, rmat, driven, pushed,
     docext, prodext, gate, ends, chain1, chain2, links, rim_out, rim_in, acts, pacts,
     part, relay, final, local_sem, tok_s, tok_r, d2d_s, d2d_r, doc_s, doc_r, one_s, one_r,
     ph_s, ph_r, st_s, st_r, ring_s, ring_r, ch_s, ch_r, rs_s, rs_r,
@@ -44,7 +45,14 @@
     x, c = lax.axis_index("fs"), lax.axis_index("tp")
     half = depth // 2
     other = 1 - c
-    sent = []
+    sent, scopes = [], []
+
+    def phase(name):
+        if scopes:
+            scopes.pop().__exit__(None, None, None)
+        if name:
+            scopes.append(jax.named_scope(name))
+            scopes[-1].__enter__()
 
     def wrap(v, n):
         return lax.rem(v + 4 * n, n)
@@ -68,6 +76,7 @@
     after_z, after_y = lax.div(after, ny), lax.rem(after, ny)
     before_z, before_y = lax.div(before, ny), lax.rem(before, ny)
 
+    phase("greet")
     barrier = pltpu.get_barrier_semaphore()
     count = 0
 
@@ -89,16 +98,23 @@
     count += greet(z=after_z, y=after_y)
     count += greet(z=before_z, y=before_y)
 
-    local = [
-        pltpu.make_async_copy(tok_in, tok.at[x, c], local_sem.at[0]),
-        pltpu.make_async_copy(w_in, wall.at[z, y], local_sem.at[1]),
-        pltpu.make_async_copy(doc_in, docs.at[x], local_sem.at[2]),
-        pltpu.make_async_copy(gain_in, gains.at[c], local_sem.at[3]),
-    ]
+    own_channels = pl.ds(pl.multiple_of(x * LANES, LANES), LANES)
+    own_groups = pl.ds(pl.multiple_of(x * 8, 8), 8)
+    moves = [(tok_in, tok.at[x, c]), (doc_in, docs.at[x]), (gain_in, gains.at[c])]
+    for k, w in enumerate((w_in_0, w_in_1, w_in_2, w_in_3, w_in_4, w_in_5)):
+        moves.append((w.at[:, own_channels], wall.at[z, y, :, pl.ds(k * LANES, LANES)]))
+    early = len(moves)
+    moves += [(decay_in.at[own_groups], rates.at[0]), (freq_in.at[own_groups], rates.at[1])]
+    moves += [(step_in, step_row), (taps_in.at[:, own_channels], taps), (skip_in.at[:, own_channels], skip)]
+    for k, m in enumerate((in_re, in_im, read_re, read_im)):
+        moves.append((m.at[own_groups], mats.at[k]))
+    local = [pltpu.make_async_copy(a, b, local_sem.at[k]) for k, (a, b) in enumerate(moves)]
     for copy in local:
         copy.start()
-    for copy in local:
+    phase("enter")
+    for copy in local[:early]:
         copy.wait()
+    phase("barrier")
     pl.semaphore_wait(barrier, count)
 
     low, high = pl.ds(0, ROWS // 2), pl.ds(ROWS // 2, ROWS // 2)
@@ -121,6 +137,7 @@
     def passed_over(block, turn):
         arrived(tok.at[block, other], d2d_r.at[turn])
 
+    phase("first_sends")
     for turn, v in enumerate((xp, xm, xo)):
         send(docs.at[x], docs.at[x], doc_s.at[turn], doc_r.at[turn], x=v)
     send(gains.at[c], gains.at[c], one_s.at[0], one_r.at[0], c=other)
@@ -137,6 +154,7 @@
     token_start(x, low, 1, 1)
     pass_over(x, 0)
 
+    phase("tables")
     shape = (ALL, ALL)
     r, n = lax.broadcasted_iota(jnp.int32, shape, 0), lax.broadcasted_iota(jnp.int32, shape, 1)
     natural = (r & 3) * ROWS + ((r >> 2) & 7) * 16 + (r >> 5)
@@ -144,26 +162,52 @@
     t = (r >> 8) * (ROWS // 2) + (r & 63)
     turned = (t & 15) * 32 + (t >> 4) * 4 + ((r >> 6) & 3)
     unperm[...] = ones_where(n == turned).astype(BF16)
-    spread = ones_where(
-        (lax.broadcasted_iota(jnp.int32, (16, LANES), 1) & 15)
-        == lax.broadcasted_iota(jnp.int32, (16, LANES), 0)
-    ).astype(BF16)
-    own_group = ones_where(
-        (lax.broadcasted_iota(jnp.int32, (STATES, LANES), 0) >> 6)
-        == (lax.broadcasted_iota(jnp.int32, (STATES, LANES), 1) >> 4)
+    for copy in local[early:]:
+        copy.wait()
+    group = lax.broadcasted_iota(jnp.int32, (8, 32), 0) + x * 8
+    step_log = jnp.broadcast_to(step_row[...], (8, 32))
+    mine_only = lax.broadcasted_iota(jnp.int32, (8, 32), 1) == group
+    step = jnp.exp(jnp.sum(jnp.where(mine_only, step_log, 0.0), axis=1, keepdims=True))
+    decay, frequency = rates[0], rates[1]
+    damping, turning = decay * step, frequency * step
+    fading = jnp.exp(-damping)
+    coef_real, coef_imag = fading * jnp.cos(turning), fading * jnp.sin(turning)
+    half_sine = jnp.sin(turning * 0.5)
+    series = jnp.ones_like(damping)
+    for k in range(11, 1, -1):
+        series = 1.0 - damping * (1.0 / k) * series
+    less_real = -damping * series * jnp.cos(turning) - 2.0 * half_sine * half_sine
+    denominator = decay * decay + frequency * frequency
+    ratio_real = (-less_real * decay + coef_imag * frequency) / denominator
+    ratio_imag = (-coef_imag * decay - less_real * frequency) / denominator
+
+    def widened(value):
+        value = jnp.concatenate([value, value], axis=1)
+        return jnp.concatenate([value] * (STATES // LANES), axis=1)
+
+    own_lane = (
+        lax.broadcasted_iota(jnp.int32, (8, STATES), 1) >> 6
+    ) == lax.broadcasted_iota(jnp.int32, (8, STATES), 0)
+
+    def flat(value):
+        return jnp.sum(jnp.where(own_lane, widened(value), 0.0), axis=0, keepdims=True)
+
+    power_re, power_im, squared = coef_real, coef_imag, 1
+    for index, length in enumerate((1, 16, ROWS, ROWS * ny)):
+        while squared < length:
+            power_re, power_im = power_re * power_re - power_im * power_im, 2.0 * power_re * power_im
+            squared *= 2
+        lam[2 * index : 2 * index + 1, :] = flat(power_re)
+        lam[2 * index + 1 : 2 * index + 2, :] = flat(power_im)
+    ratio_real, ratio_imag = flat(ratio_real), flat(ratio_imag)
+    own_state = (lax.broadcasted_iota(jnp.int32, (LANES, STATES), 0) >> 4) == (
+        lax.broadcasted_iota(jnp.int32, (LANES, STATES), 1) >> 6
     )
-    for k in range(2):
-        bmat[k * STATES : (k + 1) * STATES] = (nn(in_ri[k].astype(BF16), spread) * own_group).astype(BF16)
-    spread_p = ones_where(
-        (lax.broadcasted_iota(jnp.int32, (64, STATES), 1) & 63)
-        == lax.broadcasted_iota(jnp.int32, (64, STATES), 0)
-    ).astype(BF16)
-    own_state = ones_where(
-        (lax.broadcasted_iota(jnp.int32, (LANES, STATES), 0) >> 4)
-        == (lax.broadcasted_iota(jnp.int32, (LANES, STATES), 1) >> 6)
-    )
-    for k in range(2):
-        rmat[:, k * STATES : (k + 1) * STATES] = (nn(read_ri[k].astype(BF16), spread_p) * own_state).astype(BF16)
+    input_real, input_imag = (widened(mats[k].reshape(LANES, 64)) for k in range(2))
+    bmat[:, :STATES] = jnp.where(own_state, ratio_real * input_real - ratio_imag * input_imag, 0.0).astype(BF16)
+    bmat[:, STATES:] = jnp.where(own_state, ratio_real * input_imag + ratio_imag * input_real, 0.0).astype(BF16)
+    rmat[:, :STATES] = jnp.where(own_state, widened(mats[2].reshape(LANES, 64)), 0.0).astype(BF16)
+    rmat[:, STATES:] = jnp.where(own_state, -widened(mats[3].reshape(LANES, 64)), 0.0).astype(BF16)
 
     def ring_ref(ab, source, lanes, piece):
         count = (ny, nz)[ab]
@@ -202,11 +246,13 @@
                 ref = ring_ref(ab, wrap(me - sign * (k + 1), size), lanes_of[which], ring_piece(ab, k, way))
                 arrived(ref, ring_r.at[which, ab, way, k])
 
+    phase("tok_forward")
     token_wait(xm, low, 0, 0)
     token_start(xm, low, 0, 2)
     token_wait(xp, high, 1, 0)
     token_start(xp, high, 1, 2)
 
+    phase("phase1_wait")
     first_lanes = pl.ds(0, LANES)
     for d in range(1, ny):
         arrived(wall.at[z, wrap(y - d, ny), rows_a], ph_r.at[0, d])
@@ -221,8 +267,9 @@
     ring_start(0, 0)
     ring_start(1, 0)
 
+    phase("gain_wait")
     arrived(gains.at[other], one_r.at[0])
-    g_low, g_high = gains[0], gains[1]
+    g_low, g_high = gains[0].astype(F32), gains[1].astype(F32)
     width = 2 * tok.shape[3]
 
     def norm(block):
@@ -238,24 +285,31 @@
 
         lax.fori_loop(0, ROWS // 32, some_rows, 0)
 
+    phase("norm_own")
     passed_over(x, 0)
     norm(x)
+    phase("tok_wait1")
     token_wait(xm, high, 0, 1)
     pass_over(xm, 1)
     token_wait(xp, low, 1, 1)
     pass_over(xp, 2)
+    phase("ring00")
     ring_wait(0, 0)
     ring_start(0, 1)
+    phase("norm_mid")
     passed_over(xm, 1)
     norm(xm)
     passed_over(xp, 2)
     norm(xp)
+    phase("ring10")
     ring_wait(1, 0)
     ring_start(1, 1)
+    phase("tok_wait2")
     token_wait(xo, low, 0, 2)
     token_wait(xo, high, 1, 2)
     pass_over(xo, 3)
 
+    phase("documents")
     for turn, v in enumerate((xm, xp, xo)):
         arrived(docs.at[v], doc_r.at[turn])
     row = lax.broadcasted_iota(jnp.int32, (ALL, ROWS), 0)
@@ -264,27 +318,31 @@
     part_row = lax.broadcasted_iota(jnp.int32, (ROWS, ROWS), 0)
     spread_docs = jnp.zeros((ROWS, ROWS), F32)
     for q in range(PARTS):
-        spread_docs = jnp.where(part_row == q, docs[q], spread_docs)
+        spread_docs = jnp.where(part_row == q, docs[q].astype(F32), spread_docs)
     by_part = nt(pick_t.astype(BF16), spread_docs.astype(BF16))
     by_part = by_part * ones_where(lane == (row & 3))
     docext[64:] = nn(by_part.astype(BF16), jnp.ones((ROWS, LANES), BF16))
     docext[4:32] = docext[64 + 448 : 64 + 476]
     docext[36:64] = docext[64 + 480 : 64 + 508]
 
+    phase("norm_last")
     passed_over(xo, 3)
     norm(xo)
+    phase("ring01")
     ring_wait(0, 1)
     ring_start(0, 2)
 
+    phase("state_w_wait")
     for d in range(1, nz):
         arrived(wall.at[wrap(z - d, nz), :, rows_a, first_lanes], st_r.at[0, d])
     for d in range(1, ny):
         arrived(wall.at[:, wrap(y - d, ny), rows_b, first_lanes], st_r.at[1, d])
+    phase("state_in")
     total_depth = nz * ny * depth
     state_in = wall[:, :, :, :LANES].reshape(total_depth, LANES)
     in_order = nn(perm[...], nn(normed[...], state_in).astype(BF16))
     driven[...] = in_order
-    pushed[...] = nt(in_order.astype(BF16), bmat[...])
+    pushed[...] = nn(in_order.astype(BF16), bmat[...])
 
     def lane_cut(k):
         return slice(k * LANES, (k + 1) * LANES), slice(STATES + k * LANES, STATES + (k + 1) * LANES)
@@ -295,6 +353,7 @@
     def docs_at(k):
         return docext[64 + k * 32 : 96 + k * 32]
 
+    phase("scan")
     for cut in range(STATES // LANES):
         re, im = lane_cut(cut)
         a_re, a_im = lam[0:1, re], lam[1:2, re]
@@ -315,6 +374,7 @@
         ends[seg, 0:4, STATES:] = last
         ends[seg, 4:8, STATES:] = last
 
+    phase("fold_local")
     sign = jnp.where(lax.broadcasted_iota(jnp.int32, (8, STATES), 0) < 4, -1.0, 1.0)
 
     def joined(carry, piece, power):
@@ -337,16 +397,19 @@
     end, end_doc = fold(nothing, ends, 8, 8, 1)
     chain1[y, :, :STATES] = end
     chain1[y, :, STATES:] = end_doc
+    phase("ring11")
     ring_wait(1, 1)
     ring_start(1, 2)
     for d in range(1, ny):
         send(chain1.at[y], chain1.at[y], ch_s.at[0, d], ch_r.at[0, d], y=wrap(y + d, ny))
 
+    phase("ring02_03")
     for k in range(2, max(nz, ny) // 2):
         ring_wait(0, k)
         ring_start(0, k + 1)
     if max(nz, ny) // 2 <= 2:
         pass
+    phase("conv_in")
     conv_in = wall[:, :, :, LANES : 4 * LANES].reshape(total_depth, 3 * LANES)
     projected = nn(perm[...], nn(normed[...], conv_in).astype(BF16))
     gate[...] = projected[:, :LANES]
@@ -358,8 +421,10 @@
     rim_out[0:4, LANES:] = docext[64 + 476 : 64 + 480]
     rim_out[4:8, LANES:] = docext[64 + 508 : 64 + 512]
 
+    phase("chain1_wait")
     for d in range(1, ny):
         arrived(chain1.at[wrap(y - d, ny)], ch_r.at[0, d])
+    phase("chain1_fold")
     end, end_doc = fold(nothing, chain1, ny, ny, 2)
     chain2[z, :, :STATES] = end
     chain2[z, :, STATES:] = end_doc
@@ -367,13 +432,16 @@
     for d in range(1, nz):
         send(chain2.at[z], chain2.at[z], ch_s.at[1, d], ch_r.at[1, d], z=wrap(z + d, nz))
 
+    phase("ring12_13")
     for k in range(2, max(nz, ny) // 2):
         ring_wait(1, k)
         ring_start(1, k + 1)
     out_lanes = lanes_of[1]
     send(wall.at[:, :, :, out_lanes], wpeer, one_s.at[2], one_r.at[2], c=other)
 
+    phase("rim_wait")
     arrived(rim_in, one_r.at[1])
+    phase("conv")
     first = here == 0
     prodext[0:4] = rim_in[0:4, :LANES]
     prodext[32:36] = rim_in[4:8, :LANES]
@@ -381,17 +449,19 @@
     docext[32:36] = jnp.where(first, -1.0, rim_in[4:8, LANES:])
     now = docext[64:]
     mixed = (
-        chan[0:1] * prodext[0:ALL] * ones_where(docext[0:ALL] == now)
-        + chan[1:2] * prodext[32 : 32 + ALL] * ones_where(docext[32 : 32 + ALL] == now)
-        + chan[2:3] * prodext[64:]
+        taps[0:1].astype(F32) * prodext[0:ALL] * ones_where(docext[0:ALL] == now)
+        + taps[1:2].astype(F32) * prodext[32 : 32 + ALL] * ones_where(docext[32 : 32 + ALL] == now)
+        + taps[2:3].astype(F32) * prodext[64:]
     )
     conv_out = (gate[...] * mixed).astype(BF16)
     acts[:, :LANES] = nn(unperm[...], conv_out).astype(BF16)
     mine, theirs = (pl.ds(pl.multiple_of(v * (ALL // 2), ALL // 2), ALL // 2) for v in (c, other))
     conv_lanes, ssm_lanes = pl.ds(0, LANES), pl.ds(LANES, LANES)
 
+    phase("chain2_wait")
     for d in range(1, nz):
         arrived(chain2.at[wrap(z - d, nz)], ch_r.at[1, d])
+    phase("chain2_fold")
     send(acts.at[theirs, conv_lanes], pacts.at[:, conv_lanes], one_s.at[3], one_r.at[3], c=other)
     state = fold(nothing, chain2, nz, z, 3)
     state = fold(state, chain1, ny, y, 2)
@@ -402,6 +472,7 @@
         rim_state = slice(seg * 4, seg * 4 + 4)
         links[8 + seg // 2, (seg % 2) * 4 : (seg % 2) * 4 + 4] = links[seg, 0:4]
         links[12 + seg // 2, (seg % 2) * 4 : (seg % 2) * 4 + 4] = links[seg, 4:8]
+    phase("fixup")
     previous = docext[32:64]
     for cut in range(STATES // LANES):
         re, im = lane_cut(cut)
@@ -413,17 +484,20 @@
             reach = ones_where(docs_at(k) == previous)
             pushed[rows_at(k), re] = pushed[rows_at(k), re] + reach * w_re
             pushed[rows_at(k), im] = pushed[rows_at(k), im] + reach * w_im
-    reading = nt(pushed[...].astype(BF16), rmat[...]) + chan[3:4] * driven[...]
+    phase("readout")
+    reading = nt(pushed[...].astype(BF16), rmat[...]) + skip[...] * driven[...]
     inner = 0.7978845608028654 * (reading + 0.044715 * (reading * reading * reading))
     ssm_out = (0.5 * reading * (1.0 + jnp.tanh(inner))).astype(BF16)
     acts[:, LANES:] = nn(unperm[...], ssm_out).astype(BF16)
     send(acts.at[theirs, ssm_lanes], pacts.at[:, ssm_lanes], one_s.at[4], one_r.at[4], c=other)
 
+    phase("pact_wait")
     arrived(wpeer, one_r.at[2])
     arrived(pacts.at[:, conv_lanes], one_r.at[3])
     columns = total_depth // 2
     own_weight = wall.at[:, :, :, out_lanes]
     arrived(pacts.at[:, ssm_lanes], one_r.at[4])
+    phase("out_proj")
     for h in range(2):
         cut = slice(h * nz // 2, (h + 1) * nz // 2)
         total = nt(acts[mine, :], wall[cut, :, :, 4 * LANES :].reshape(columns, 2 * LANES))
@@ -435,41 +509,24 @@
         else:
             send(part.at[1, xo], relay.at[1], rs_s.at[1, 0], rs_r.at[1, 0], x=xm)
             send(part.at[1, xp], final.at[0, 1], rs_s.at[0, 1], rs_r.at[0, 1], x=xp)
+    phase("relay0")
     arrived(relay.at[0], rs_r.at[0, 0])
     part[0, xp] = (part[0, xp].astype(F32) + relay[0].astype(F32)).astype(BF16)
     send(part.at[0, xp], final.at[0, 0], rs_s.at[0, 2], rs_r.at[0, 2], x=xp)
+    phase("relay1")
     arrived(relay.at[1], rs_r.at[1, 0])
     part[1, xm] = (part[1, xm].astype(F32) + relay[1].astype(F32)).astype(BF16)
     send(part.at[1, xm], final.at[1, 1], rs_s.at[1, 2], rs_r.at[1, 2], x=xm)
+    phase("final")
     for h, turns in ((1, (1, 2)), (0, (2, 1))):
         arrived(final.at[0, h], rs_r.at[0, turns[0]])
         arrived(final.at[1, h], rs_r.at[1, turns[1]])
         value = part[h, x].astype(F32) + final[0, h].astype(F32) + final[1, h].astype(F32)
         out[:, h * columns : (h + 1) * columns] = value.astype(BF16)
+    phase("drain")
     for copy in sent:
         copy.wait_send()
-
-
-def state_tables(decay_rate, frequency, step_log, input_real, input_imag, lengths):
-    step_size = jnp.exp(step_log)[:, None]
-    damping = decay_rate * step_size
-    turning = frequency * step_size
-    fading = jnp.exp(-damping)
-    coef_imag = fading * jnp.sin(turning)
-    half_sine = jnp.sin(turning / 2.0)
-    less_real = jnp.expm1(-damping) * jnp.cos(turning) - 2.0 * half_sine * half_sine
-    denominator = decay_rate * decay_rate + frequency * frequency
-    ratio_real = (-less_real * decay_rate + coef_imag * frequency) / denominator
-    ratio_imag = (-coef_imag * decay_rate - less_real * frequency) / denominator
-    bbar_real = ratio_real[..., None] * input_real - ratio_imag[..., None] * input_imag
-    bbar_imag = ratio_real[..., None] * input_imag + ratio_imag[..., None] * input_real
-    rows = []
-    for length in lengths:
-        fade = jnp.exp(-length * damping)
-        rows += [fade * jnp.cos(length * turning), fade * jnp.sin(length * turning)]
-    powers = jnp.stack(rows).reshape(len(rows), -1)
-    bbar = jnp.stack([bbar_real, bbar_imag]).reshape(2, -1, input_real.shape[2])
-    return powers, bbar
+    phase(None)
 
 
 def shards(
@@ -477,29 +534,8 @@
     conv_taps, state_in_weight, decay_rate, frequency, step_log, input_real, input_imag,
     readout_real, readout_imag, skip_gain, conv_out_weight, state_out_weight,
 ):
-    x = lax.axis_index("fs")
     depth = state_in_weight.shape[0]
     width = tokens.shape[1]
-
-    def own(array, dim):
-        size = array.shape[dim] // PARTS
-        return lax.dynamic_slice_in_dim(array, x * size, size, dim)
-
-    weights = jnp.concatenate(
-        [own(w, 1) for w in (state_in_weight, out_gate_weight, in_gate_weight, value_weight)]
-        + [own(w, 0).T for w in (conv_out_weight, state_out_weight)],
-        axis=1,
-    )
-    powers, bbar = state_tables(
-        own(decay_rate, 0), own(frequency, 0), own(step_log, 0), own(input_real, 0),
-        own(input_imag, 0), (1.0, 16.0, float(ROWS), float(ROWS * ny)),
-    )
-    readout = jnp.stack([own(readout_real, 0), -own(readout_imag, 0)]).reshape(2, LANES, -1)
-    channels = jnp.concatenate(
-        [own(conv_taps, 1).astype(F32), own(skip_gain, 0)[None, :], jnp.zeros((4, LANES), F32)]
-    )
-    doc_row = documents.astype(F32)[None, :]
-    gain_row = norm_gain.astype(F32)[None, :]
     columns = nz * ny * depth // 2
     vmem = pl.BlockSpec(memory_space=pltpu.VMEM)
     anywhere = pl.BlockSpec(memory_space=pl.ANY)
@@ -509,18 +545,24 @@
     return pl.pallas_call(
         functools.partial(mixer_kernel, nz, ny, depth),
         out_shape=jax.ShapeDtypeStruct((ROWS // 2, 2 * columns), BF16),
-        in_specs=[anywhere] * 4 + [vmem] * 4,
+        in_specs=[anywhere] * 18,
         out_specs=vmem,
         scratch_shapes=[
+            pltpu.VMEM((2, 8, 64), F32),
+            pltpu.VMEM((1, 32), F32),
+            pltpu.VMEM((4, 8, 16, 64), F32),
+            pltpu.VMEM((3, LANES), BF16),
+            pltpu.VMEM((1, LANES), F32),
+            pltpu.VMEM((8, STATES), F32),
             pltpu.VMEM((PARTS, 2, ROWS, width), BF16),
-            pltpu.VMEM((2, 1, width), F32),
-            pltpu.VMEM((PARTS, 1, ROWS), F32),
+            pltpu.VMEM((2, 1, width), norm_gain.dtype),
+            pltpu.VMEM((PARTS, 1, ROWS), jnp.int32),
             pltpu.VMEM((nz, ny, depth, 6 * LANES), BF16),
             pltpu.VMEM((nz, ny, depth, 2 * LANES), BF16),
             pltpu.VMEM((ALL, 2 * width), BF16),
             pltpu.VMEM((ALL, ALL), BF16),
             pltpu.VMEM((ALL, ALL), BF16),
-            pltpu.VMEM((2 * STATES, LANES), BF16),
+            pltpu.VMEM((LANES, 2 * STATES), BF16),
             pltpu.VMEM((LANES, 2 * STATES), BF16),
             pltpu.VMEM((ALL, LANES), F32),
             pltpu.VMEM((ALL, 2 * STATES), F32),
@@ -538,7 +580,7 @@
             pltpu.VMEM((2, PARTS, ROWS // 2, columns), BF16),
             pltpu.VMEM((2, ROWS // 2, columns), BF16),
             pltpu.VMEM((2, 2, ROWS // 2, columns), BF16),
-            dma((4,)),
+            dma((18,)),
             dma((2, 3)), dma((2, 3)),
             dma((4,)), dma((4,)),
             dma((3,)), dma((3,)),
@@ -553,7 +595,12 @@
             collective_id=0, has_side_effects=True, vmem_limit_bytes=60 * 1024 * 1024
         ),
         name="mixer",
-    )(tokens, weights, doc_row, gain_row, bbar, readout, powers, channels)
+    )(
+        tokens, state_in_weight, out_gate_weight, in_gate_weight, value_weight, conv_out_weight.T,
+        state_out_weight.T, documents[None, :], norm_gain[None, :], decay_rate, frequency,
+        step_log[None, :], input_real.transpose(0, 2, 1), input_imag.transpose(0, 2, 1),
+        readout_real, readout_imag, conv_taps, skip_gain[None, :],
+    )
 
 
 def solution(mesh, nz=8, ny=8):

time: 88.2 us -> 74.6 us (0.85)
  local copies, waits for them, and re-layouts: 9.4 us -> 2.95 us
  other arithmetic: 5.78 us -> 0 us
  Pallas kernels: 72 us -> 71.1 us
    unnamed x16 -> x3, local copies, waits for them, and re-layouts: 6.04 us -> 2.35 us
    another operation x12 -> x0, local copies, waits for them, and re-layouts: 2.39 us -> none  [the longest x9 1.24 us: state_tables(): powers = jnp.stack(rows).reshape(len(rows), -1)]
    broadcast_in_dim x2 -> x0, other arithmetic: 1.1 us -> none  [the longest x1 0.59 us: shards(): gain_row = norm_gain.astype(F32)[None, :]]
    pallas_call x1, Pallas kernels: 72 us -> 71.1 us  [shards(): pl.pallas_call(functools.partial(mixer_kernel, nz, ny, depth), out_shape=...]
    sub x1 -> x0, other arithmetic: 0.91 us -> none  [state_tables(): ratio_real[..., None] * input_real - ratio_imag[..., None] * input_imag]
    neg x1 -> x0, other arithmetic: 0.89 us -> none  [shards(): -own(readout_imag, 0)]
where the time goes in v2:
time: 74.6 us; the launch traced here: 74.1 us
  Pallas kernels  71.1 us (95%)
  local copies, waits for them, and re-layouts  2.95 us (4%)
    pallas_call x1, Pallas kernels, shards(): pl.pallas_call(functools.partial(mixer_kernel, nz, ny, depth), out_shape=...  71.1 us
    unnamed x3, local copies, waits for them, and re-layouts  2.35 us

profile of v2, /device:TPU:1, one launch (start us, length us, event | category | flops | bytes accessed | tf_op | source)
XLA Modules:
  0.0 74.1 jit_solution(11548740653778004359)
XLA Ops:
  0.0 0.0 copy-start
  0.0 0.7 copy-done
  0.7 0.6 broadcast_in_dim.13.gain_in
  1.3 71.1 %mixer.1 = bf16[64,2048]{1,0:T(8,128)(2,1)} custom-call(bf16[128,1024]{1,0:T(8,128)(2,1)} %tok_in.1, bf16[32,512]{1,0:T(8,128)(2,1)} %w_in_0.1, bf16[32,512]{1,0:T(8,128)(2,1)} %w_in_1.1, bf16[32,512]{1,0:T(8,128)(2,1)} %w_in_2.1, bf16[32,512]{1,0:T(8,128)(2,1)} %w_in_3.1, bf16[32,512]{1,0:T(8,128)(2,1)} %bitcast.9, bf16[32,512]{1,0:T(8,128)(2,1)} %bitcast.10, ...), custom_call_target="tpu_custom_call" | custom-call | tf_op jit(solution)/shard_map/mixer/pallas_call | solution.py:545
  72.4 1.7 %copy.20 = bf16[64,2048]{1,0:T(8,128)(2,1)} copy(bf16[64,2048]{1,0:T(8,128)(2,1)} %mixer.1) | data formatting | bytes 524288
Async XLA Ops:
  0.0 0.7 copy-start

commit v3 on v2

--- a/solution.py
+++ b/solution.py
@@ -36,14 +36,15 @@
 def mixer_kernel(
     nz, ny, depth, tok_in, w_in_0, w_in_1, w_in_2, w_in_3, w_in_4, w_in_5, doc_in, gain_in,
     decay_in, freq_in, step_in, in_re, in_im, read_re, read_im, taps_in, skip_in, out,
-    rates, step_row, mats, taps, skip, lam, tok, gains, docs, wall, wpeer, normed, perm, unperm, bmat, rmat, driven, pushed,
+    rates, step_row, mats, taps, skip, lam, tok, gains, gain_rows, docs, wall, wpeer, normed, perm, unperm, bmat, rmat, driven, pushed,
     docext, prodext, gate, ends, chain1, chain2, links, rim_out, rim_in, acts, pacts,
     part, relay, final, local_sem, tok_s, tok_r, d2d_s, d2d_r, doc_s, doc_r, one_s, one_r,
-    ph_s, ph_r, st_s, st_r, ring_s, ring_r, ch_s, ch_r, rs_s, rs_r,
+    ph_s, ph_r, st_s, st_r, ring_s, ring_r, peer_s, peer_r, ch_s, ch_r, rs_s, rs_r,
 ):
     z, y = lax.axis_index("sp_0"), lax.axis_index("sp_1")
     x, c = lax.axis_index("fs"), lax.axis_index("tp")
     half = depth // 2
+    most = max(nz, ny)
     other = 1 - c
     sent, scopes = [], []
 
@@ -138,21 +139,32 @@
         arrived(tok.at[block, other], d2d_r.at[turn])
 
     phase("first_sends")
+    rows_a, rows_b = pl.ds(0, half), pl.ds(half, half)
+    first_lanes, later_lanes = pl.ds(0, LANES), pl.ds(LANES, 5 * LANES)
+
+    def spread_out(turn, lanes):
+        for d in range(1, ny):
+            ref = wall.at[z, y, rows_a, lanes]
+            send(ref, ref, ph_s.at[turn, 0, d], ph_r.at[turn, 0, d], y=wrap(y + d, ny))
+        for d in range(1, nz):
+            ref = wall.at[z, y, rows_b, lanes]
+            send(ref, ref, ph_s.at[turn, 1, d], ph_r.at[turn, 1, d], z=wrap(z + d, nz))
+
+    def spread_in(turn, lanes, ab):
+        for d in range(1, (ny, nz)[ab]):
+            block = (z, wrap(y - d, ny), rows_a) if ab == 0 else (wrap(z - d, nz), y, rows_b)
+            arrived(wall.at[(*block, lanes)], ph_r.at[turn, ab, d])
+
     for turn, v in enumerate((xp, xm, xo)):
         send(docs.at[x], docs.at[x], doc_s.at[turn], doc_r.at[turn], x=v)
     send(gains.at[c], gains.at[c], one_s.at[0], one_r.at[0], c=other)
+    spread_out(0, first_lanes)
     token_start(x, low, 0, 0)
     token_start(x, high, 1, 0)
-    rows_a, rows_b = pl.ds(0, half), pl.ds(half, half)
-    for d in range(1, ny):
-        ref = wall.at[z, y, rows_a]
-        send(ref, ref, ph_s.at[0, d], ph_r.at[0, d], y=wrap(y + d, ny))
-    for d in range(1, nz):
-        ref = wall.at[z, y, rows_b]
-        send(ref, ref, ph_s.at[1, d], ph_r.at[1, d], z=wrap(z + d, nz))
+    pass_over(x, 0)
+    spread_out(1, later_lanes)
     token_start(x, high, 0, 1)
     token_start(x, low, 1, 1)
-    pass_over(x, 0)
 
     phase("tables")
     shape = (ALL, ALL)
@@ -216,60 +228,61 @@
             return wall.at[source, cut, rows_a, lanes]
         return wall.at[cut, source, rows_b, lanes]
 
-    lanes_of = (pl.ds(LANES, 3 * LANES), pl.ds(4 * LANES, 2 * LANES))
-
-    def ring_piece(ab, k, way):
-        size = (nz, ny)[ab]
-        return 0 if k < size // 2 - 1 else 1 + way
-
-    def ring_start(which, k):
+    lanes_of = (pl.ds(LANES, 3 * LANES), pl.ds(LANES, 3 * LANES), pl.ds(4 * LANES, 2 * LANES))
+    out_lanes = lanes_of[2]
+
+    def ring_hops(which, k):
         for ab in range(2):
             me, size = ((z, nz), (y, ny))[ab]
-            if k >= size // 2:
-                continue
+            last = size // 2 - 1
             for way in range(2):
-                sign = 1 - 2 * way
-                ref = ring_ref(ab, wrap(me - sign * k, size), lanes_of[which], ring_piece(ab, k, way))
-                target = wrap(me + sign, size)
-                send(
-                    ref, ref, ring_s.at[which, ab, way, k], ring_r.at[which, ab, way, k],
-                    **{"zy"[ab]: target},
-                )
+                if k > last or (k == last and which == 1 - way):
+                    continue
+                piece = which + 1 if which < 2 else (1 + way if k == last else 0)
+                yield ab, way, me, size, piece
+
+    def ring_start(which, k):
+        for ab, way, me, size, piece in ring_hops(which, k):
+            sign = 1 - 2 * way
+            ref = ring_ref(ab, wrap(me - sign * k, size), lanes_of[which], piece)
+            send(
+                ref, ref, ring_s.at[which, ab, way, k], ring_r.at[which, ab, way, k],
+                **{"zy"[ab]: wrap(me + sign, size)},
+            )
+
+    def ring_source(which, k):
+        for ab, way, me, size, piece in ring_hops(which, k):
+            sign = 1 - 2 * way
+            yield ab, way, ring_ref(ab, wrap(me - sign * (k + 1), size), lanes_of[which], piece)
 
     def ring_wait(which, k):
-        for ab in range(2):
-            me, size = ((z, nz), (y, ny))[ab]
-            if k >= size // 2:
-                continue
-            for way in range(2):
-                sign = 1 - 2 * way
-                ref = ring_ref(ab, wrap(me - sign * (k + 1), size), lanes_of[which], ring_piece(ab, k, way))
-                arrived(ref, ring_r.at[which, ab, way, k])
-
-    phase("tok_forward")
-    token_wait(xm, low, 0, 0)
-    token_start(xm, low, 0, 2)
-    token_wait(xp, high, 1, 0)
-    token_start(xp, high, 1, 2)
-
-    phase("phase1_wait")
-    first_lanes = pl.ds(0, LANES)
-    for d in range(1, ny):
-        arrived(wall.at[z, wrap(y - d, ny), rows_a], ph_r.at[0, d])
-    for d in range(1, nz):
-        ref = wall.at[z, :, rows_a, first_lanes]
-        send(ref, ref, st_s.at[0, d], st_r.at[0, d], z=wrap(z + d, nz))
-    for d in range(1, nz):
-        arrived(wall.at[wrap(z - d, nz), y, rows_b], ph_r.at[1, d])
-    for d in range(1, ny):
-        ref = wall.at[:, y, rows_b, first_lanes]
-        send(ref, ref, st_s.at[1, d], st_r.at[1, d], y=wrap(y + d, ny))
-    ring_start(0, 0)
-    ring_start(1, 0)
-
-    phase("gain_wait")
-    arrived(gains.at[other], one_r.at[0])
-    g_low, g_high = gains[0].astype(F32), gains[1].astype(F32)
+        for ab, way, ref in ring_source(which, k):
+            arrived(ref, ring_r.at[which, ab, way, k])
+
+    def service(which, k):
+        ring_wait(which, k)
+        ring_start(which, k + 1)
+
+    def peer_pieces(turn, mine_or_not):
+        if turn == 0:
+            pieces = [(z, slice(None), rows_a), (slice(None), y, rows_b)]
+            return [(2 * k, p) for k, p in enumerate(pieces)]
+        found = []
+        for ab, way, me, size, piece in ring_hops(2, turn - 1):
+            source = wrap(me - (1 - 2 * way) * turn, size)
+            span = (ny, nz)[ab]
+            cut = {0: pl.ds(0, span), 1: pl.ds(0, span // 2), 2: pl.ds(span // 2, span // 2)}[piece]
+            found.append((2 * ab + way, (source, cut, rows_a) if ab == 0 else (cut, source, rows_b)))
+        return found
+
+    def peer_start(turn):
+        for k, p in peer_pieces(turn, True):
+            send(wall.at[(*p, out_lanes)], wpeer.at[p], peer_s.at[turn, k], peer_r.at[turn, k], c=other)
+
+    def peer_wait(turn):
+        for k, p in peer_pieces(turn, False):
+            arrived(wpeer.at[p], peer_r.at[turn, k])
+
     width = 2 * tok.shape[3]
 
     def norm(block):
@@ -279,35 +292,44 @@
             mean = (jnp.sum(a * a, axis=1, keepdims=True) + jnp.sum(b * b, axis=1, keepdims=True)) / width
             scale = lax.rsqrt(mean + EPS)
             target = pl.ds(pl.multiple_of(block * ROWS + i * 32, 32), 32)
-            normed[target, : width // 2] = (a * scale * g_low).astype(BF16)
-            normed[target, width // 2 :] = (b * scale * g_high).astype(BF16)
+            normed[target, : width // 2] = (a * scale * gain_rows[0]).astype(BF16)
+            normed[target, width // 2 :] = (b * scale * gain_rows[1]).astype(BF16)
             return carry
 
         lax.fori_loop(0, ROWS // 32, some_rows, 0)
 
     phase("norm_own")
+    arrived(gains.at[other], one_r.at[0])
+    for k in range(2):
+        wide = gains[k].astype(F32)
+        gain_rows[k] = jnp.concatenate([wide[i : i + 1] for i in range(wide.shape[0])], axis=1)
     passed_over(x, 0)
     norm(x)
+    phase("phase1_state")
+    spread_in(0, first_lanes, 0)
+    for d in range(1, nz):
+        ref = wall.at[z, :, rows_a, first_lanes]
+        send(ref, ref, st_s.at[0, d], st_r.at[0, d], z=wrap(z + d, nz))
+    spread_in(0, first_lanes, 1)
+    for d in range(1, ny):
+        ref = wall.at[:, y, rows_b, first_lanes]
+        send(ref, ref, st_s.at[1, d], st_r.at[1, d], y=wrap(y + d, ny))
+    phase("tok_forward")
+    token_wait(xm, low, 0, 0)
+    token_start(xm, low, 0, 2)
+    token_wait(xp, high, 1, 0)
+    token_start(xp, high, 1, 2)
+    phase("phase1_rest")
+    spread_in(1, later_lanes, 0)
+    spread_in(1, later_lanes, 1)
+    for which in range(3):
+        ring_start(which, 0)
+    peer_start(0)
     phase("tok_wait1")
     token_wait(xm, high, 0, 1)
     pass_over(xm, 1)
     token_wait(xp, low, 1, 1)
     pass_over(xp, 2)
-    phase("ring00")
-    ring_wait(0, 0)
-    ring_start(0, 1)
-    phase("norm_mid")
-    passed_over(xm, 1)
-    norm(xm)
-    passed_over(xp, 2)
-    norm(xp)
-    phase("ring10")
-    ring_wait(1, 0)
-    ring_start(1, 1)
-    phase("tok_wait2")
-    token_wait(xo, low, 0, 2)
-    token_wait(xo, high, 1, 2)
-    pass_over(xo, 3)
 
     phase("documents")
     for turn, v in enumerate((xm, xp, xo)):
@@ -325,12 +347,18 @@
     docext[4:32] = docext[64 + 448 : 64 + 476]
     docext[36:64] = docext[64 + 480 : 64 + 508]
 
+    phase("norm_mid")
+    passed_over(xm, 1)
+    norm(xm)
+    passed_over(xp, 2)
+    norm(xp)
+    phase("tok_wait2")
+    token_wait(xo, low, 0, 2)
+    token_wait(xo, high, 1, 2)
+    pass_over(xo, 3)
     phase("norm_last")
     passed_over(xo, 3)
     norm(xo)
-    phase("ring01")
-    ring_wait(0, 1)
-    ring_start(0, 2)
 
     phase("state_w_wait")
     for d in range(1, nz):
@@ -342,6 +370,10 @@
     state_in = wall[:, :, :, :LANES].reshape(total_depth, LANES)
     in_order = nn(perm[...], nn(normed[...], state_in).astype(BF16))
     driven[...] = in_order
+    phase("ring_ab0")
+    service(0, 0)
+    service(1, 0)
+    phase("push")
     pushed[...] = nn(in_order.astype(BF16), bmat[...])
 
     def lane_cut(k):
@@ -397,18 +429,34 @@
     end, end_doc = fold(nothing, ends, 8, 8, 1)
     chain1[y, :, :STATES] = end
     chain1[y, :, STATES:] = end_doc
-    phase("ring11")
-    ring_wait(1, 1)
-    ring_start(1, 2)
     for d in range(1, ny):
         send(chain1.at[y], chain1.at[y], ch_s.at[0, d], ch_r.at[0, d], y=wrap(y + d, ny))
-
-    phase("ring02_03")
-    for k in range(2, max(nz, ny) // 2):
-        ring_wait(0, k)
-        ring_start(0, k + 1)
-    if max(nz, ny) // 2 <= 2:
-        pass
+    phase("ring_ab1")
+    service(0, 1)
+    service(1, 1)
+    phase("ring_o0")
+    service(2, 0)
+    peer_start(1)
+
+    phase("chain1_wait")
+    for d in range(1, ny):
+        arrived(chain1.at[wrap(y - d, ny)], ch_r.at[0, d])
+    end, end_doc = fold(nothing, chain1, ny, ny, 2)
+    chain2[z, :, :STATES] = end
+    chain2[z, :, STATES:] = end_doc
+    for d in range(1, nz):
+        send(chain2.at[z], chain2.at[z], ch_s.at[1, d], ch_r.at[1, d], z=wrap(z + d, nz))
+    phase("ring_ab2")
+    service(0, 2)
+    service(1, 2)
+    phase("ring_o1")
+    service(2, 1)
+    peer_start(2)
+    phase("ring_ab3")
+    for k in range(3, most // 2):
+        service(0, k)
+        service(1, k)
+
     phase("conv_in")
     conv_in = wall[:, :, :, LANES : 4 * LANES].reshape(total_depth, 3 * LANES)
     projected = nn(perm[...], nn(normed[...], conv_in).astype(BF16))
@@ -421,23 +469,10 @@
     rim_out[0:4, LANES:] = docext[64 + 476 : 64 + 480]
     rim_out[4:8, LANES:] = docext[64 + 508 : 64 + 512]
 
-    phase("chain1_wait")
-    for d in range(1, ny):
-        arrived(chain1.at[wrap(y - d, ny)], ch_r.at[0, d])
-    phase("chain1_fold")
-    end, end_doc = fold(nothing, chain1, ny, ny, 2)
-    chain2[z, :, :STATES] = end
-    chain2[z, :, STATES:] = end_doc
     send(rim_out, rim_in, one_s.at[1], one_r.at[1], z=after_z, y=after_y)
-    for d in range(1, nz):
-        send(chain2.at[z], chain2.at[z], ch_s.at[1, d], ch_r.at[1, d], z=wrap(z + d, nz))
-
-    phase("ring12_13")
-    for k in range(2, max(nz, ny) // 2):
-        ring_wait(1, k)
-        ring_start(1, k + 1)
-    out_lanes = lanes_of[1]
-    send(wall.at[:, :, :, out_lanes], wpeer, one_s.at[2], one_r.at[2], c=other)
+    phase("ring_o2")
+    service(2, 2)
+    peer_start(3)
 
     phase("rim_wait")
     arrived(rim_in, one_r.at[1])
@@ -491,38 +526,49 @@
     acts[:, LANES:] = nn(unperm[...], ssm_out).astype(BF16)
     send(acts.at[theirs, ssm_lanes], pacts.at[:, ssm_lanes], one_s.at[4], one_r.at[4], c=other)
 
+    phase("ring_o3")
+    for k in range(3, most // 2):
+        service(2, k)
+        peer_start(k + 1)
+    phase("peer_w_wait")
+    for turn in range(most // 2 + 1):
+        peer_wait(turn)
     phase("pact_wait")
-    arrived(wpeer, one_r.at[2])
     arrived(pacts.at[:, conv_lanes], one_r.at[3])
-    columns = total_depth // 2
-    own_weight = wall.at[:, :, :, out_lanes]
+    columns = total_depth // 4
     arrived(pacts.at[:, ssm_lanes], one_r.at[4])
-    phase("out_proj")
-    for h in range(2):
-        cut = slice(h * nz // 2, (h + 1) * nz // 2)
-        total = nt(acts[mine, :], wall[cut, :, :, 4 * LANES :].reshape(columns, 2 * LANES))
-        total = total + nt(pacts[...], wpeer[cut].reshape(columns, 2 * LANES))
-        part[h] = total.astype(BF16).reshape(PARTS, ROWS // 2, columns)
-        if h == 0:
-            send(part.at[0, xo], relay.at[0], rs_s.at[0, 0], rs_r.at[0, 0], x=xp)
-            send(part.at[0, xm], final.at[1, 0], rs_s.at[1, 1], rs_r.at[1, 1], x=xm)
-        else:
-            send(part.at[1, xo], relay.at[1], rs_s.at[1, 0], rs_r.at[1, 0], x=xm)
-            send(part.at[1, xp], final.at[0, 1], rs_s.at[0, 1], rs_r.at[0, 1], x=xp)
-    phase("relay0")
-    arrived(relay.at[0], rs_r.at[0, 0])
-    part[0, xp] = (part[0, xp].astype(F32) + relay[0].astype(F32)).astype(BF16)
-    send(part.at[0, xp], final.at[0, 0], rs_s.at[0, 2], rs_r.at[0, 2], x=xp)
-    phase("relay1")
-    arrived(relay.at[1], rs_r.at[1, 0])
-    part[1, xm] = (part[1, xm].astype(F32) + relay[1].astype(F32)).astype(BF16)
-    send(part.at[1, xm], final.at[1, 1], rs_s.at[1, 2], rs_r.at[1, 2], x=xm)
-    phase("final")
-    for h, turns in ((1, (1, 2)), (0, (2, 1))):
-        arrived(final.at[0, h], rs_r.at[0, turns[0]])
-        arrived(final.at[1, h], rs_r.at[1, turns[1]])
-        value = part[h, x].astype(F32) + final[0, h].astype(F32) + final[1, h].astype(F32)
-        out[:, h * columns : (h + 1) * columns] = value.astype(BF16)
+
+    def quarter(ref, cut, lanes):
+        if nz % 4 == 0:
+            return ref[cut * nz // 4 : (cut + 1) * nz // 4, :, :, lanes].reshape(columns, 2 * LANES)
+        return ref[cut // 2, cut % 2, :, lanes]
+
+    for cut in (0, 2, 1, 3):
+        phase(f"out_proj{cut}")
+        total = nt(acts[mine, :], quarter(wall, cut, slice(4 * LANES, 6 * LANES)))
+        total = total + nt(pacts[...], quarter(wpeer, cut, slice(None)))
+        part[cut] = total.astype(BF16).reshape(PARTS, ROWS // 2, columns)
+        way, turn = cut // 2, cut % 2
+        target = (xp, xm)[way]
+        send(part.at[cut, xo], relay.at[way, turn], rs_s.at[way, turn], rs_r.at[way, turn], x=target)
+    for turn in range(2):
+        send(part.at[2 + turn, xp], final.at[0, 2 + turn], rs_s.at[0, 2 + turn], rs_r.at[0, 2 + turn], x=xp)
+        send(part.at[turn, xm], final.at[1, turn], rs_s.at[1, 2 + turn], rs_r.at[1, 2 + turn], x=xm)
+    for turn in range(2):
+        for way, target in ((0, xp), (1, xm)):
+            phase(f"relay{way}{turn}")
+            cut = 2 * way + turn
+            arrived(relay.at[way, turn], rs_r.at[way, turn])
+            both = part[cut, target].astype(F32) + relay[way, turn].astype(F32)
+            part[cut, target] = both.astype(BF16)
+            send(part.at[cut, target], final.at[way, cut], rs_s.at[way, 4 + turn], rs_r.at[way, 4 + turn], x=target)
+    for cut in (0, 2, 1, 3):
+        phase(f"final{cut}")
+        summed_way, turn = cut // 2, cut % 2
+        arrived(final.at[1 - summed_way, cut], rs_r.at[1 - summed_way, 2 + turn])
+        arrived(final.at[summed_way, cut], rs_r.at[summed_way, 4 + turn])
+        value = part[cut, x].astype(F32) + final[0, cut].astype(F32) + final[1, cut].astype(F32)
+        out[:, cut * columns : (cut + 1) * columns] = value.astype(BF16)
     phase("drain")
     for copy in sent:
         copy.wait_send()
@@ -536,16 +582,16 @@
 ):
     depth = state_in_weight.shape[0]
     width = tokens.shape[1]
-    columns = nz * ny * depth // 2
+    columns = nz * ny * depth // 4
     vmem = pl.BlockSpec(memory_space=pltpu.VMEM)
-    anywhere = pl.BlockSpec(memory_space=pl.ANY)
+    hbm = pl.BlockSpec(memory_space=pltpu.HBM)
     dma = pltpu.SemaphoreType.DMA
     steps = max(nz, ny) // 2
     most = max(nz, ny)
     return pl.pallas_call(
         functools.partial(mixer_kernel, nz, ny, depth),
-        out_shape=jax.ShapeDtypeStruct((ROWS // 2, 2 * columns), BF16),
-        in_specs=[anywhere] * 18,
+        out_shape=jax.ShapeDtypeStruct((ROWS // 2, 4 * columns), BF16),
+        in_specs=[hbm] * 18,
         out_specs=vmem,
         scratch_shapes=[
             pltpu.VMEM((2, 8, 64), F32),
@@ -555,7 +601,8 @@
             pltpu.VMEM((1, LANES), F32),
             pltpu.VMEM((8, STATES), F32),
             pltpu.VMEM((PARTS, 2, ROWS, width), BF16),
-            pltpu.VMEM((2, 1, width), norm_gain.dtype),
+            pltpu.VMEM((2, width // LANES, LANES), BF16),
+            pltpu.VMEM((2, 1, width), F32),
             pltpu.VMEM((PARTS, 1, ROWS), jnp.int32),
             pltpu.VMEM((nz, ny, depth, 6 * LANES), BF16),
             pltpu.VMEM((nz, ny, depth, 2 * LANES), BF16),
@@ -577,30 +624,33 @@
             pltpu.VMEM((8, 2 * LANES), F32),
             pltpu.VMEM((ALL, 2 * LANES), BF16),
             pltpu.VMEM((ALL // 2, 2 * LANES), BF16),
-            pltpu.VMEM((2, PARTS, ROWS // 2, columns), BF16),
-            pltpu.VMEM((2, ROWS // 2, columns), BF16),
+            pltpu.VMEM((4, PARTS, ROWS // 2, columns), BF16),
             pltpu.VMEM((2, 2, ROWS // 2, columns), BF16),
+            pltpu.VMEM((2, 4, ROWS // 2, columns), BF16),
             dma((18,)),
             dma((2, 3)), dma((2, 3)),
             dma((4,)), dma((4,)),
             dma((3,)), dma((3,)),
             dma((5,)), dma((5,)),
+            dma((2, 2, most)), dma((2, 2, most)),
             dma((2, most)), dma((2, most)),
+            dma((3, 2, 2, steps)), dma((3, 2, 2, steps)),
+            dma((steps + 1, 4)), dma((steps + 1, 4)),
             dma((2, most)), dma((2, most)),
-            dma((2, 2, 2, steps)), dma((2, 2, 2, steps)),
-            dma((2, most)), dma((2, most)),
-            dma((2, 3)), dma((2, 3)),
+            dma((2, 6)), dma((2, 6)),
         ],
         compiler_params=pltpu.CompilerParams(
-            collective_id=0, has_side_effects=True, vmem_limit_bytes=60 * 1024 * 1024
+            collective_id=0, has_side_effects=True, vmem_limit_bytes=40 * 1024 * 1024
         ),
         name="mixer",
-    )(
-        tokens, state_in_weight, out_gate_weight, in_gate_weight, value_weight, conv_out_weight.T,
-        state_out_weight.T, documents[None, :], norm_gain[None, :], decay_rate, frequency,
-        step_log[None, :], input_real.transpose(0, 2, 1), input_imag.transpose(0, 2, 1),
-        readout_real, readout_imag, conv_taps, skip_gain[None, :],
-    )
+    )(*(
+        pltpu.with_memory_space_constraint(operand, pltpu.HBM) for operand in (
+            tokens, state_in_weight, out_gate_weight, in_gate_weight, value_weight, conv_out_weight.T,
+            state_out_weight.T, documents[None, :], norm_gain.reshape(-1, LANES), decay_rate, frequency,
+            step_log[None, :], input_real.transpose(0, 2, 1), input_imag.transpose(0, 2, 1),
+            readout_real, readout_imag, conv_taps, skip_gain[None, :],
+        )
+    ))
 
 
 def solution(mesh, nz=8, ny=8):

time: 74.6 us -> 70.5 us (0.945)
  local copies, waits for them, and re-layouts: 2.95 us -> 0.71 us
  Pallas kernels: 71.1 us -> 69.6 us
    unnamed x3 -> x1, local copies, waits for them, and re-layouts: 2.35 us -> 0.71 us
    pallas_call x1, Pallas kernels: 71.1 us -> 69.6 us  [shards(): pl.pallas_call(functools.partial(mixer_kernel, nz, ny, depth), out_shape=...]
where the time goes in v3:
time: 70.5 us; the launch traced here: 70.3 us
  Pallas kernels  69.6 us (99%)
  local copies, waits for them, and re-layouts  0.71 us (1%)
    pallas_call x1, Pallas kernels, shards(): pl.pallas_call(functools.partial(mixer_kernel, nz, ny, depth), out_shape=...  69.6 us

profile of v3, /device:TPU:1, one launch (start us, length us, event | category | flops | bytes accessed | tf_op | source)
XLA Modules:
  0.0 70.3 jit_solution(10793942160615674471)
XLA Ops:
  0.0 69.6 %mixer.1 = bf16[64,2048]{1,0:T(8,128)(2,1)S(1)} custom-call(bf16[128,1024]{1,0:T(8,128)(2,1)} %tok_in.1, bf16[32,512]{1,0:T(8,128)(2,1)} %w_in_0.1, bf16[32,512]{1,0:T(8,128)(2,1)} %w_in_1.1, bf16[32,512]{1,0:T(8,128)(2,1)} %w_in_2.1, bf16[32,512]{1,0:T(8,128)(2,1)} %w_in_3.1, bf16[32,512]{1,0:T(8,128)(2,1)} %bitcast.10, bf16[32,512]{1,0:T(8,128)(2,1)} %bitcast.11, ...), custom_call_target="tpu_custom_call" | custom-call | tf_op jit(solution)/shard_map/mixer/pallas_call | solution.py:591
  69.6 0.7 %copy.20 = bf16[64,2048]{1,0:T(8,128)(2,1)} copy(bf16[64,2048]{1,0:T(8,128)(2,1)S(1)} %mixer.1) | data formatting | bytes 524288

commit v4 on v3

--- a/solution.py
+++ b/solution.py
@@ -25,6 +25,11 @@
     return jnp.dot(a, b, preferred_element_type=F32)
 
 
+def halves(product, a, b):
+    middle = a.shape[0] // 2
+    return jnp.concatenate([product(a[:middle], b), product(a[middle:], b)])
+
+
 def nt(a, b):
     return lax.dot_general(a, b, (((1,), (1,)), ((), ())), preferred_element_type=F32)
 
@@ -37,7 +42,7 @@
     nz, ny, depth, tok_in, w_in_0, w_in_1, w_in_2, w_in_3, w_in_4, w_in_5, doc_in, gain_in,
     decay_in, freq_in, step_in, in_re, in_im, read_re, read_im, taps_in, skip_in, out,
     rates, step_row, mats, taps, skip, lam, tok, gains, gain_rows, docs, wall, wpeer, normed, perm, unperm, bmat, rmat, driven, pushed,
-    docext, prodext, gate, ends, chain1, chain2, links, rim_out, rim_in, acts, pacts,
+    docext, prodext, gate, ends, chain1, chain2, incoming, links, rim_out, rim_in, acts, pacts,
     part, relay, final, local_sem, tok_s, tok_r, d2d_s, d2d_r, doc_s, doc_r, one_s, one_r,
     ph_s, ph_r, st_s, st_r, ring_s, ring_r, peer_s, peer_r, ch_s, ch_r, rs_s, rs_r,
 ):
@@ -119,6 +124,12 @@
     pl.semaphore_wait(barrier, count)
 
     low, high = pl.ds(0, ROWS // 2), pl.ds(ROWS // 2, ROWS // 2)
+
+    def column_copy(d):
+        return pltpu.make_async_remote_copy(
+            src_ref=chain2.at[z], dst_ref=chain2.at[z], send_sem=ch_s.at[1, d], recv_sem=ch_r.at[1, d],
+            device_id={"sp_0": wrap(z + d, nz)}, device_id_type=pl.DeviceIdType.MESH,
+        )
 
     def token_send(block, rows, way):
         ref = tok.at[block, c, rows]
@@ -259,6 +270,31 @@
         for ab, way, ref in ring_source(which, k):
             arrived(ref, ring_r.at[which, ab, way, k])
 
+    def state_hops(ab, stage):
+        me, size = ((z, nz), (y, ny))[ab]
+        reach = 1 if size < 4 else 2
+        for way in range(2):
+            for d in range(1, size // 2 + 1):
+                if (d > reach) != (stage == 1):
+                    continue
+                piece = 1 + way if d == size // 2 else 0
+                yield way, d, piece, me, size
+
+    def state_start(ab, stage):
+        for way, d, piece, me, size in state_hops(ab, stage):
+            sign = 1 - 2 * way
+            source = wrap(me - sign * 2, size) if stage else me
+            ref = ring_ref(ab, source, first_lanes, piece)
+            send(
+                ref, ref, st_s.at[ab, way, d], st_r.at[ab, way, d],
+                **{"zy"[ab]: wrap(me + sign * (d - 2 * stage), size)},
+            )
+
+    def state_wait(ab, stage):
+        for way, d, piece, me, size in state_hops(ab, stage):
+            ref = ring_ref(ab, wrap(me - (1 - 2 * way) * d, size), first_lanes, piece)
+            arrived(ref, st_r.at[ab, way, d])
+
     def service(which, k):
         ring_wait(which, k)
         ring_start(which, k + 1)
@@ -306,14 +342,9 @@
     passed_over(x, 0)
     norm(x)
     phase("phase1_state")
-    spread_in(0, first_lanes, 0)
-    for d in range(1, nz):
-        ref = wall.at[z, :, rows_a, first_lanes]
-        send(ref, ref, st_s.at[0, d], st_r.at[0, d], z=wrap(z + d, nz))
-    spread_in(0, first_lanes, 1)
-    for d in range(1, ny):
-        ref = wall.at[:, y, rows_b, first_lanes]
-        send(ref, ref, st_s.at[1, d], st_r.at[1, d], y=wrap(y + d, ny))
+    for ab in range(2):
+        spread_in(0, first_lanes, ab)
+        state_start(ab, 0)
     phase("tok_forward")
     token_wait(xm, low, 0, 0)
     token_start(xm, low, 0, 2)
@@ -347,32 +378,41 @@
     docext[4:32] = docext[64 + 448 : 64 + 476]
     docext[36:64] = docext[64 + 480 : 64 + 508]
 
+    phase("state_stage")
+    for ab in range(2):
+        state_wait(ab, 0)
+        state_start(ab, 1)
     phase("norm_mid")
     passed_over(xm, 1)
     norm(xm)
-    passed_over(xp, 2)
-    norm(xp)
     phase("tok_wait2")
     token_wait(xo, low, 0, 2)
     token_wait(xo, high, 1, 2)
     pass_over(xo, 3)
+    phase("norm_mid2")
+    passed_over(xp, 2)
+    norm(xp)
+    phase("ring_ab0")
+    service(0, 0)
+    service(1, 0)
     phase("norm_last")
     passed_over(xo, 3)
     norm(xo)
 
+    phase("ring_o0")
+    service(2, 0)
+    peer_start(1)
     phase("state_w_wait")
-    for d in range(1, nz):
-        arrived(wall.at[wrap(z - d, nz), :, rows_a, first_lanes], st_r.at[0, d])
-    for d in range(1, ny):
-        arrived(wall.at[:, wrap(y - d, ny), rows_b, first_lanes], st_r.at[1, d])
+    for ab in range(2):
+        state_wait(ab, 1)
     phase("state_in")
     total_depth = nz * ny * depth
     state_in = wall[:, :, :, :LANES].reshape(total_depth, LANES)
-    in_order = nn(perm[...], nn(normed[...], state_in).astype(BF16))
+    in_order = halves(nn, perm, halves(nn, normed, state_in).astype(BF16))
     driven[...] = in_order
-    phase("ring_ab0")
-    service(0, 0)
-    service(1, 0)
+    phase("ring_ab1")
+    service(0, 1)
+    service(1, 1)
     phase("push")
     pushed[...] = nn(in_order.astype(BF16), bmat[...])
 
@@ -411,47 +451,63 @@
 
     def joined(carry, piece, power):
         held, doc = carry
-        now = piece[:, STATES:]
+        piece, now = piece
         link = ones_where(now == doc)
         link = jnp.concatenate([link] * (STATES // LANES), axis=1)
         a_re, a_im = lam[2 * power : 2 * power + 1, :], lam[2 * power + 1 : 2 * power + 2, :]
         moved = a_re * held + (a_im * sign) * pltpu.roll(held, 4, 0)
-        return piece[:, :STATES] + link * moved, now
+        return piece + link * moved, now
+
+    def of_ends(k):
+        return ends[k, :, :STATES], ends[k, :, STATES:]
+
+    wing = STATES // 2
+
+    def pack(buffer, index, carry):
+        held, doc = carry
+        buffer[index, 0:8, :wing] = held[:, :wing].astype(BF16)
+        buffer[index, 8:16, :wing] = held[:, wing:].astype(BF16)
+        buffer[index, 0:8, wing:] = doc.astype(BF16)
+        buffer[index, 8:16, wing:] = doc.astype(BF16)
+
+    def of(buffer):
+        def read(k):
+            message = buffer[k].astype(F32)
+            held = jnp.concatenate([message[0:8, :wing], message[8:16, :wing]], axis=1)
+            return held, message[0:8, wing:]
+
+        return read
 
     def fold(carry, pieces, count, limit, power):
         def step(k, carry):
-            new = joined(carry, pieces[k], power)
+            new = joined(carry, pieces(k), power)
             return tuple(jnp.where(k < limit, a, b) for a, b in zip(new, carry))
 
         return lax.fori_loop(0, count, step, carry)
 
     nothing = (jnp.zeros((8, STATES), F32), jnp.full((8, LANES), -1.0, F32))
-    end, end_doc = fold(nothing, ends, 8, 8, 1)
-    chain1[y, :, :STATES] = end
-    chain1[y, :, STATES:] = end_doc
+    pack(chain1, y, fold(nothing, of_ends, 8, 8, 1))
     for d in range(1, ny):
         send(chain1.at[y], chain1.at[y], ch_s.at[0, d], ch_r.at[0, d], y=wrap(y + d, ny))
-    phase("ring_ab1")
-    service(0, 1)
-    service(1, 1)
-    phase("ring_o0")
-    service(2, 0)
-    peer_start(1)
-
+    phase("ring_o1")
+    service(2, 1)
+    peer_start(2)
+
+    phase("ring_ab2")
+    service(0, 2)
+    service(1, 2)
     phase("chain1_wait")
     for d in range(1, ny):
         arrived(chain1.at[wrap(y - d, ny)], ch_r.at[0, d])
-    end, end_doc = fold(nothing, chain1, ny, ny, 2)
-    chain2[z, :, :STATES] = end
-    chain2[z, :, STATES:] = end_doc
+    pack(chain2, z, fold(nothing, of(chain1), ny, ny, 2))
     for d in range(1, nz):
-        send(chain2.at[z], chain2.at[z], ch_s.at[1, d], ch_r.at[1, d], z=wrap(z + d, nz))
-    phase("ring_ab2")
-    service(0, 2)
-    service(1, 2)
-    phase("ring_o1")
-    service(2, 1)
-    peer_start(2)
+
+        @pl.when(z + d < nz)
+        def _(d=d):
+            column_copy(d).start()
+    phase("ring_o2")
+    service(2, 2)
+    peer_start(3)
     phase("ring_ab3")
     for k in range(3, most // 2):
         service(0, k)
@@ -462,49 +518,40 @@
     projected = nn(perm[...], nn(normed[...], conv_in).astype(BF16))
     gate[...] = projected[:, :LANES]
     prodext[64:] = (projected[:, LANES : 2 * LANES] * projected[:, 2 * LANES :]).astype(BF16).astype(F32)
-    prodext[4:32] = prodext[64 + 448 : 64 + 476]
-    prodext[36:64] = prodext[64 + 480 : 64 + 508]
     rim_out[0:4, :LANES] = prodext[64 + 476 : 64 + 480]
     rim_out[4:8, :LANES] = prodext[64 + 508 : 64 + 512]
     rim_out[0:4, LANES:] = docext[64 + 476 : 64 + 480]
     rim_out[4:8, LANES:] = docext[64 + 508 : 64 + 512]
-
+    prodext[4:32] = prodext[64 + 448 : 64 + 476]
+    prodext[36:64] = prodext[64 + 480 : 64 + 508]
     send(rim_out, rim_in, one_s.at[1], one_r.at[1], z=after_z, y=after_y)
-    phase("ring_o2")
-    service(2, 2)
-    peer_start(3)
-
-    phase("rim_wait")
-    arrived(rim_in, one_r.at[1])
-    phase("conv")
-    first = here == 0
-    prodext[0:4] = rim_in[0:4, :LANES]
-    prodext[32:36] = rim_in[4:8, :LANES]
-    docext[0:4] = jnp.where(first, -1.0, rim_in[0:4, LANES:])
-    docext[32:36] = jnp.where(first, -1.0, rim_in[4:8, LANES:])
-    now = docext[64:]
-    mixed = (
-        taps[0:1].astype(F32) * prodext[0:ALL] * ones_where(docext[0:ALL] == now)
-        + taps[1:2].astype(F32) * prodext[32 : 32 + ALL] * ones_where(docext[32 : 32 + ALL] == now)
-        + taps[2:3].astype(F32) * prodext[64:]
-    )
-    conv_out = (gate[...] * mixed).astype(BF16)
-    acts[:, :LANES] = nn(unperm[...], conv_out).astype(BF16)
-    mine, theirs = (pl.ds(pl.multiple_of(v * (ALL // 2), ALL // 2), ALL // 2) for v in (c, other))
-    conv_lanes, ssm_lanes = pl.ds(0, LANES), pl.ds(LANES, LANES)
-
+    phase("ring_o3")
+    for k in range(3, most // 2):
+        service(2, k)
+        peer_start(k + 1)
     phase("chain2_wait")
+    incoming[:, :STATES], incoming[:, STATES:] = nothing
     for d in range(1, nz):
-        arrived(chain2.at[wrap(z - d, nz)], ch_r.at[1, d])
+
+        @pl.when(z >= d)
+        def _(d=d):
+            arrived(chain2.at[z - d], ch_r.at[1, d])
+
     phase("chain2_fold")
-    send(acts.at[theirs, conv_lanes], pacts.at[:, conv_lanes], one_s.at[3], one_r.at[3], c=other)
-    state = fold(nothing, chain2, nz, z, 3)
-    state = fold(state, chain1, ny, y, 2)
+
+    @pl.when(z > 0)
+    def _():
+        def step(k, carry):
+            return joined(carry, of(chain2)(k), 3)
+
+        incoming[:, :STATES], incoming[:, STATES:] = lax.fori_loop(0, z, step, nothing)
+
+    state = fold((incoming[:, :STATES], incoming[:, STATES:]), of(chain1), ny, y, 2)
+    docext[32:36] = state[1][0:4]
     for seg in range(8):
         links[seg] = state[0]
-        state = joined(state, ends[seg], 1)
+        state = joined(state, of_ends(seg), 1)
     for seg in range(8):
-        rim_state = slice(seg * 4, seg * 4 + 4)
         links[8 + seg // 2, (seg % 2) * 4 : (seg % 2) * 4 + 4] = links[seg, 0:4]
         links[12 + seg // 2, (seg % 2) * 4 : (seg % 2) * 4 + 4] = links[seg, 4:8]
     phase("fixup")
@@ -520,32 +567,55 @@
             pushed[rows_at(k), re] = pushed[rows_at(k), re] + reach * w_re
             pushed[rows_at(k), im] = pushed[rows_at(k), im] + reach * w_im
     phase("readout")
-    reading = nt(pushed[...].astype(BF16), rmat[...]) + skip[...] * driven[...]
+    reading = halves(nt, pushed[...].astype(BF16), rmat[...]) + skip[...] * driven[...]
     inner = 0.7978845608028654 * (reading + 0.044715 * (reading * reading * reading))
     ssm_out = (0.5 * reading * (1.0 + jnp.tanh(inner))).astype(BF16)
-    acts[:, LANES:] = nn(unperm[...], ssm_out).astype(BF16)
+    acts[:, LANES:] = halves(nn, unperm, ssm_out).astype(BF16)
+    mine, theirs = (pl.ds(pl.multiple_of(v * (ALL // 2), ALL // 2), ALL // 2) for v in (c, other))
+    conv_lanes, ssm_lanes = pl.ds(0, LANES), pl.ds(LANES, LANES)
     send(acts.at[theirs, ssm_lanes], pacts.at[:, ssm_lanes], one_s.at[4], one_r.at[4], c=other)
 
-    phase("ring_o3")
-    for k in range(3, most // 2):
-        service(2, k)
-        peer_start(k + 1)
-    phase("peer_w_wait")
-    for turn in range(most // 2 + 1):
-        peer_wait(turn)
-    phase("pact_wait")
-    arrived(pacts.at[:, conv_lanes], one_r.at[3])
+    phase("rim_wait")
+    docext[0:4] = jnp.full((4, LANES), -1.0, F32)
+    prodext[0:4] = jnp.zeros((4, LANES), F32)
+    prodext[32:36] = jnp.zeros((4, LANES), F32)
+
+    @pl.when(here > 0)
+    def _():
+        arrived(rim_in, one_r.at[1])
+        prodext[0:4] = rim_in[0:4, :LANES]
+        prodext[32:36] = rim_in[4:8, :LANES]
+        docext[0:4] = rim_in[0:4, LANES:]
+
+    phase("conv")
+    now = docext[64:]
+    mixed = (
+        taps[0:1].astype(F32) * prodext[0:ALL] * ones_where(docext[0:ALL] == now)
+        + taps[1:2].astype(F32) * prodext[32 : 32 + ALL] * ones_where(docext[32 : 32 + ALL] == now)
+        + taps[2:3].astype(F32) * prodext[64:]
+    )
+    conv_out = (gate[...] * mixed).astype(BF16)
+    acts[:, :LANES] = halves(nn, unperm, conv_out).astype(BF16)
+    send(acts.at[theirs, conv_lanes], pacts.at[:, conv_lanes], one_s.at[3], one_r.at[3], c=other)
+
     columns = total_depth // 4
-    arrived(pacts.at[:, ssm_lanes], one_r.at[4])
 
     def quarter(ref, cut, lanes):
         if nz % 4 == 0:
             return ref[cut * nz // 4 : (cut + 1) * nz // 4, :, :, lanes].reshape(columns, 2 * LANES)
         return ref[cut // 2, cut % 2, :, lanes]
 
+    phase("peer_w_wait")
+    for turn in range(most // 2 + 1):
+        peer_wait(turn)
+    settled = len(sent)
     for cut in (0, 2, 1, 3):
         phase(f"out_proj{cut}")
         total = nt(acts[mine, :], quarter(wall, cut, slice(4 * LANES, 6 * LANES)))
+        if cut == 0:
+            phase("pact_wait")
+            arrived(pacts.at[:, ssm_lanes], one_r.at[4])
+            arrived(pacts.at[:, conv_lanes], one_r.at[3])
         total = total + nt(pacts[...], quarter(wpeer, cut, slice(None)))
         part[cut] = total.astype(BF16).reshape(PARTS, ROWS // 2, columns)
         way, turn = cut // 2, cut % 2
@@ -554,6 +624,8 @@
     for turn in range(2):
         send(part.at[2 + turn, xp], final.at[0, 2 + turn], rs_s.at[0, 2 + turn], rs_r.at[0, 2 + turn], x=xp)
         send(part.at[turn, xm], final.at[1, turn], rs_s.at[1, 2 + turn], rs_r.at[1, 2 + turn], x=xm)
+    for copy in sent[:settled]:
+        copy.wait_send()
     for turn in range(2):
         for way, target in ((0, xp), (1, xm)):
             phase(f"relay{way}{turn}")
@@ -570,8 +642,19 @@
         value = part[cut, x].astype(F32) + final[0, cut].astype(F32) + final[1, cut].astype(F32)
         out[:, cut * columns : (cut + 1) * columns] = value.astype(BF16)
     phase("drain")
-    for copy in sent:
+    for copy in sent[settled:]:
         copy.wait_send()
+
+    @pl.when(here == 0)
+    def _():
+        arrived(rim_in, one_r.at[1])
+
+    for d in range(1, nz):
+
+        @pl.when(z + d < nz)
+        def _(d=d):
+            column_copy(d).wait_send()
+
     phase(None)
 
 
@@ -617,8 +700,9 @@
             pltpu.VMEM((64 + ALL, LANES), F32),
             pltpu.VMEM((ALL, LANES), F32),
             pltpu.VMEM((8, 8, STATES + LANES), F32),
-            pltpu.VMEM((ny, 8, STATES + LANES), F32),
-            pltpu.VMEM((nz, 8, STATES + LANES), F32),
+            pltpu.VMEM((ny, 16, STATES // 2 + LANES), BF16),
+            pltpu.VMEM((nz, 16, STATES // 2 + LANES), BF16),
+            pltpu.VMEM((8, STATES + LANES), F32),
             pltpu.VMEM((16, 8, STATES), F32),
             pltpu.VMEM((8, 2 * LANES), F32),
             pltpu.VMEM((8, 2 * LANES), F32),
@@ -633,7 +717,7 @@
             dma((3,)), dma((3,)),
             dma((5,)), dma((5,)),
             dma((2, 2, most)), dma((2, 2, most)),
-            dma((2, most)), dma((2, most)),
+            dma((2, 2, steps + 1)), dma((2, 2, steps + 1)),
             dma((3, 2, 2, steps)), dma((3, 2, 2, steps)),
             dma((steps + 1, 4)), dma((steps + 1, 4)),
             dma((2, most)), dma((2, most)),

time: 70.5 us -> 61.3 us (0.87)
  Pallas kernels: 69.6 us -> 60.5 us
    pallas_call x1, Pallas kernels: 69.6 us -> 60.5 us  [shards(): pl.pallas_call(functools.partial(mixer_kernel, nz, ny, depth), out_shape=...]
where the time goes in v4:
time: 61.3 us; the launch traced here: 61.2 us
  Pallas kernels  60.5 us (99%)
  local copies, waits for them, and re-layouts  0.71 us (1%)
    pallas_call x1, Pallas kernels, shards(): pl.pallas_call(functools.partial(mixer_kernel, nz, ny, depth), out_shape=...  60.5 us

profile of v4, /device:TPU:1, one launch (start us, length us, event | category | flops | bytes accessed | tf_op | source)
XLA Modules:
  0.0 61.2 jit_solution(6557210280265803069)
XLA Ops:
  0.0 60.5 %mixer.1 = bf16[64,2048]{1,0:T(8,128)(2,1)S(1)} custom-call(bf16[128,1024]{1,0:T(8,128)(2,1)} %tok_in.1, bf16[32,512]{1,0:T(8,128)(2,1)} %w_in_0.1, bf16[32,512]{1,0:T(8,128)(2,1)} %w_in_1.1, bf16[32,512]{1,0:T(8,128)(2,1)} %w_in_2.1, bf16[32,512]{1,0:T(8,128)(2,1)} %w_in_3.1, bf16[32,512]{1,0:T(8,128)(2,1)} %bitcast.10, bf16[32,512]{1,0:T(8,128)(2,1)} %bitcast.11, ...), custom_call_target="tpu_custom_call" | custom-call | tf_op jit(solution)/shard_map/mixer/pallas_call | solution.py:674
  60.5 0.7 %copy.20 = bf16[64,2048]{1,0:T(8,128)(2,1)} copy(bf16[64,2048]{1,0:T(8,128)(2,1)S(1)} %mixer.1) | data formatting | bytes 524288

commit v5 on v4

--- a/solution.py
+++ b/solution.py
@@ -51,7 +51,7 @@
     half = depth // 2
     most = max(nz, ny)
     other = 1 - c
-    sent, scopes = [], []
+    owed, scopes = [], []
 
     def phase(name):
         if scopes:
@@ -71,10 +71,17 @@
             device_id_type=pl.DeviceIdType.MESH,
         )
         copy.start()
-        sent.append(copy)
 
     def arrived(dst, rsem):
         pltpu.make_async_copy(dst, dst, rsem).wait()
+
+    def owe(view, ssem):
+        owed.append((view, ssem))
+
+    def settle():
+        for view, ssem in owed:
+            arrived(view, ssem)
+        owed.clear()
 
     xp, xm, xo = wrap(x + 1, PARTS), wrap(x - 1, PARTS), wrap(x + 2, PARTS)
     here = z * ny + y
@@ -106,20 +113,19 @@
 
     own_channels = pl.ds(pl.multiple_of(x * LANES, LANES), LANES)
     own_groups = pl.ds(pl.multiple_of(x * 8, 8), 8)
-    moves = [(tok_in, tok.at[x, c]), (doc_in, docs.at[x]), (gain_in, gains.at[c])]
+    moves = [(tok_in, tok.at[x, c], 0), (doc_in, docs.at[x], 1), (gain_in, gains.at[c], 2)]
     for k, w in enumerate((w_in_0, w_in_1, w_in_2, w_in_3, w_in_4, w_in_5)):
-        moves.append((w.at[:, own_channels], wall.at[z, y, :, pl.ds(k * LANES, LANES)]))
-    early = len(moves)
-    moves += [(decay_in.at[own_groups], rates.at[0]), (freq_in.at[own_groups], rates.at[1])]
-    moves += [(step_in, step_row), (taps_in.at[:, own_channels], taps), (skip_in.at[:, own_channels], skip)]
+        moves.append((w.at[:, own_channels], wall.at[z, y, :, pl.ds(k * LANES, LANES)], 3))
+    moves += [(decay_in.at[own_groups], rates.at[0], 4), (freq_in.at[own_groups], rates.at[1], 4)]
     for k, m in enumerate((in_re, in_im, read_re, read_im)):
-        moves.append((m.at[own_groups], mats.at[k]))
-    local = [pltpu.make_async_copy(a, b, local_sem.at[k]) for k, (a, b) in enumerate(moves)]
-    for copy in local:
-        copy.start()
+        moves.append((m.at[own_groups], mats.at[k], 5))
+    moves += [(step_in, step_row, 6), (taps_in.at[:, own_channels], taps, 7)]
+    moves.append((skip_in.at[:, own_channels], skip, 8))
+    for source, target, k in moves:
+        pltpu.make_async_copy(source, target, local_sem.at[k]).start()
     phase("enter")
-    for copy in local[:early]:
-        copy.wait()
+    for k, ref in enumerate((tok.at[x, c], docs.at[x], gains.at[c], wall.at[z, y])):
+        arrived(ref, local_sem.at[k])
     phase("barrier")
     pl.semaphore_wait(barrier, count)
 
@@ -127,7 +133,7 @@
 
     def column_copy(d):
         return pltpu.make_async_remote_copy(
-            src_ref=chain2.at[z], dst_ref=chain2.at[z], send_sem=ch_s.at[1, d], recv_sem=ch_r.at[1, d],
+            src_ref=chain2.at[z], dst_ref=chain2.at[z], send_sem=ch_s.at[d], recv_sem=ch_r.at[d],
             device_id={"sp_0": wrap(z + d, nz)}, device_id_type=pl.DeviceIdType.MESH,
         )
 
@@ -137,14 +143,14 @@
 
     def token_start(block, rows, way, turn):
         ref, target = token_send(block, rows, way)
-        send(ref, ref, tok_s.at[way, turn], tok_r.at[way, turn], x=target)
+        send(ref, ref, tok_s.at[0], tok_r.at[way, turn], x=target)
 
     def token_wait(block, rows, way, turn):
         arrived(tok.at[block, c, rows], tok_r.at[way, turn])
 
     def pass_over(block, turn):
         ref = tok.at[block, c]
-        send(ref, ref, d2d_s.at[turn], d2d_r.at[turn], c=other)
+        send(ref, ref, d2d_s.at[0], d2d_r.at[turn], c=other)
 
     def passed_over(block, turn):
         arrived(tok.at[block, other], d2d_r.at[turn])
@@ -153,22 +159,31 @@
     rows_a, rows_b = pl.ds(0, half), pl.ds(half, half)
     first_lanes, later_lanes = pl.ds(0, LANES), pl.ds(LANES, 5 * LANES)
 
+    def spread_view(lanes, ab):
+        if ab == 0:
+            return wall.at[0, pl.ds(0, ny - 1), rows_a, lanes]
+        return wall.at[pl.ds(0, nz - 1), 0, rows_b, lanes]
+
     def spread_out(turn, lanes):
         for d in range(1, ny):
             ref = wall.at[z, y, rows_a, lanes]
-            send(ref, ref, ph_s.at[turn, 0, d], ph_r.at[turn, 0, d], y=wrap(y + d, ny))
+            send(ref, ref, ph_s.at[turn, 0], ph_r.at[turn, 0], y=wrap(y + d, ny))
         for d in range(1, nz):
             ref = wall.at[z, y, rows_b, lanes]
-            send(ref, ref, ph_s.at[turn, 1, d], ph_r.at[turn, 1, d], z=wrap(z + d, nz))
+            send(ref, ref, ph_s.at[turn, 1], ph_r.at[turn, 1], z=wrap(z + d, nz))
+        for ab in range(2):
+            owe(spread_view(lanes, ab), ph_s.at[turn, ab])
 
     def spread_in(turn, lanes, ab):
-        for d in range(1, (ny, nz)[ab]):
-            block = (z, wrap(y - d, ny), rows_a) if ab == 0 else (wrap(z - d, nz), y, rows_b)
-            arrived(wall.at[(*block, lanes)], ph_r.at[turn, ab, d])
-
-    for turn, v in enumerate((xp, xm, xo)):
-        send(docs.at[x], docs.at[x], doc_s.at[turn], doc_r.at[turn], x=v)
+        arrived(spread_view(lanes, ab), ph_r.at[turn, ab])
+
+    for v in (xp, xm, xo):
+        send(docs.at[x], docs.at[x], doc_s.at[0], doc_r.at[0], x=v)
+    owe(docs.at[pl.ds(0, PARTS - 1)], doc_s.at[0])
     send(gains.at[c], gains.at[c], one_s.at[0], one_r.at[0], c=other)
+    owe(gains.at[c], one_s.at[0])
+    owe(tok.at[pl.ds(0, PARTS - 1), 0], tok_s.at[0])
+    owe(tok.at[:, 0], d2d_s.at[0])
     spread_out(0, first_lanes)
     token_start(x, low, 0, 0)
     token_start(x, high, 1, 0)
@@ -185,8 +200,8 @@
     t = (r >> 8) * (ROWS // 2) + (r & 63)
     turned = (t & 15) * 32 + (t >> 4) * 4 + ((r >> 6) & 3)
     unperm[...] = ones_where(n == turned).astype(BF16)
-    for copy in local[early:]:
-        copy.wait()
+    for k, ref in enumerate((rates, mats, step_row, taps, skip)):
+        arrived(ref, local_sem.at[4 + k])
     group = lax.broadcasted_iota(jnp.int32, (8, 32), 0) + x * 8
     step_log = jnp.broadcast_to(step_row[...], (8, 32))
     mine_only = lax.broadcasted_iota(jnp.int32, (8, 32), 1) == group
@@ -256,19 +271,19 @@
         for ab, way, me, size, piece in ring_hops(which, k):
             sign = 1 - 2 * way
             ref = ring_ref(ab, wrap(me - sign * k, size), lanes_of[which], piece)
-            send(
-                ref, ref, ring_s.at[which, ab, way, k], ring_r.at[which, ab, way, k],
-                **{"zy"[ab]: wrap(me + sign, size)},
-            )
-
-    def ring_source(which, k):
-        for ab, way, me, size, piece in ring_hops(which, k):
-            sign = 1 - 2 * way
-            yield ab, way, ring_ref(ab, wrap(me - sign * (k + 1), size), lanes_of[which], piece)
+            send(ref, ref, ring_s.at[which], ring_r.at[which, k], **{"zy"[ab]: wrap(me + sign, size)})
+
+    def blocks_view(array, count, lanes):
+        if count > nz * ny:
+            return array.at[pl.ds(0, count // (2 * ny)), :, :, lanes]
+        return array.at[pl.ds(0, count // ny), :, rows_a, lanes]
+
+    def ring_blocks(which, k):
+        return sum((ny, nz)[ab] // (2 if piece else 1) for ab, _, _, _, piece in ring_hops(which, k))
 
     def ring_wait(which, k):
-        for ab, way, ref in ring_source(which, k):
-            arrived(ref, ring_r.at[which, ab, way, k])
+        if ring_blocks(which, k):
+            arrived(blocks_view(wall, ring_blocks(which, k), lanes_of[which]), ring_r.at[which, k])
 
     def state_hops(ab, stage):
         me, size = ((z, nz), (y, ny))[ab]
@@ -285,39 +300,36 @@
             sign = 1 - 2 * way
             source = wrap(me - sign * 2, size) if stage else me
             ref = ring_ref(ab, source, first_lanes, piece)
-            send(
-                ref, ref, st_s.at[ab, way, d], st_r.at[ab, way, d],
-                **{"zy"[ab]: wrap(me + sign * (d - 2 * stage), size)},
-            )
+            target = wrap(me + sign * (d - 2 * stage), size)
+            send(ref, ref, st_s.at[ab, stage], st_r.at[ab, stage], **{"zy"[ab]: target})
+        if state_blocks(ab, stage):
+            owe(blocks_view(wall, state_blocks(ab, stage), first_lanes), st_s.at[ab, stage])
+
+    def state_blocks(ab, stage):
+        return sum((ny, nz)[ab] // (2 if piece else 1) for _, _, piece, _, _ in state_hops(ab, stage))
 
     def state_wait(ab, stage):
-        for way, d, piece, me, size in state_hops(ab, stage):
-            ref = ring_ref(ab, wrap(me - (1 - 2 * way) * d, size), first_lanes, piece)
-            arrived(ref, st_r.at[ab, way, d])
+        if state_blocks(ab, stage):
+            arrived(blocks_view(wall, state_blocks(ab, stage), first_lanes), st_r.at[ab, stage])
 
     def service(which, k):
         ring_wait(which, k)
         ring_start(which, k + 1)
 
-    def peer_pieces(turn, mine_or_not):
+    def peer_pieces(turn):
         if turn == 0:
-            pieces = [(z, slice(None), rows_a), (slice(None), y, rows_b)]
-            return [(2 * k, p) for k, p in enumerate(pieces)]
+            return [(z, slice(None), rows_a), (slice(None), y, rows_b)]
         found = []
         for ab, way, me, size, piece in ring_hops(2, turn - 1):
             source = wrap(me - (1 - 2 * way) * turn, size)
             span = (ny, nz)[ab]
             cut = {0: pl.ds(0, span), 1: pl.ds(0, span // 2), 2: pl.ds(span // 2, span // 2)}[piece]
-            found.append((2 * ab + way, (source, cut, rows_a) if ab == 0 else (cut, source, rows_b)))
+            found.append((source, cut, rows_a) if ab == 0 else (cut, source, rows_b))
         return found
 
     def peer_start(turn):
-        for k, p in peer_pieces(turn, True):
-            send(wall.at[(*p, out_lanes)], wpeer.at[p], peer_s.at[turn, k], peer_r.at[turn, k], c=other)
-
-    def peer_wait(turn):
-        for k, p in peer_pieces(turn, False):
-            arrived(wpeer.at[p], peer_r.at[turn, k])
+        for p in peer_pieces(turn):
+            send(wall.at[(*p, out_lanes)], wpeer.at[p], peer_s.at[0], peer_r.at[0], c=other)
 
     width = 2 * tok.shape[3]
 
@@ -363,8 +375,7 @@
     pass_over(xp, 2)
 
     phase("documents")
-    for turn, v in enumerate((xm, xp, xo)):
-        arrived(docs.at[v], doc_r.at[turn])
+    arrived(docs.at[pl.ds(0, PARTS - 1)], doc_r.at[0])
     row = lax.broadcasted_iota(jnp.int32, (ALL, ROWS), 0)
     lane = lax.broadcasted_iota(jnp.int32, (ALL, ROWS), 1)
     pick_t = ones_where(lane == ((row >> 2) & 7) * 16 + (row >> 5))
@@ -488,7 +499,7 @@
     nothing = (jnp.zeros((8, STATES), F32), jnp.full((8, LANES), -1.0, F32))
     pack(chain1, y, fold(nothing, of_ends, 8, 8, 1))
     for d in range(1, ny):
-        send(chain1.at[y], chain1.at[y], ch_s.at[0, d], ch_r.at[0, d], y=wrap(y + d, ny))
+        send(chain1.at[y], chain1.at[y], one_s.at[1], one_r.at[1], y=wrap(y + d, ny))
     phase("ring_o1")
     service(2, 1)
     peer_start(2)
@@ -497,8 +508,8 @@
     service(0, 2)
     service(1, 2)
     phase("chain1_wait")
-    for d in range(1, ny):
-        arrived(chain1.at[wrap(y - d, ny)], ch_r.at[0, d])
+    owe(chain1.at[pl.ds(0, ny - 1)], one_s.at[1])
+    arrived(chain1.at[pl.ds(0, ny - 1)], one_r.at[1])
     pack(chain2, z, fold(nothing, of(chain1), ny, ny, 2))
     for d in range(1, nz):
 
@@ -524,7 +535,8 @@
     rim_out[4:8, LANES:] = docext[64 + 508 : 64 + 512]
     prodext[4:32] = prodext[64 + 448 : 64 + 476]
     prodext[36:64] = prodext[64 + 480 : 64 + 508]
-    send(rim_out, rim_in, one_s.at[1], one_r.at[1], z=after_z, y=after_y)
+    send(rim_out, rim_in, one_s.at[2], one_r.at[2], z=after_z, y=after_y)
+    owe(rim_out, one_s.at[2])
     phase("ring_o3")
     for k in range(3, most // 2):
         service(2, k)
@@ -535,7 +547,7 @@
 
         @pl.when(z >= d)
         def _(d=d):
-            arrived(chain2.at[z - d], ch_r.at[1, d])
+            arrived(chain2.at[z - d], ch_r.at[d])
 
     phase("chain2_fold")
 
@@ -574,6 +586,7 @@
     mine, theirs = (pl.ds(pl.multiple_of(v * (ALL // 2), ALL // 2), ALL // 2) for v in (c, other))
     conv_lanes, ssm_lanes = pl.ds(0, LANES), pl.ds(LANES, LANES)
     send(acts.at[theirs, ssm_lanes], pacts.at[:, ssm_lanes], one_s.at[4], one_r.at[4], c=other)
+    owe(pacts.at[:, ssm_lanes], one_s.at[4])
 
     phase("rim_wait")
     docext[0:4] = jnp.full((4, LANES), -1.0, F32)
@@ -582,7 +595,7 @@
 
     @pl.when(here > 0)
     def _():
-        arrived(rim_in, one_r.at[1])
+        arrived(rim_in, one_r.at[2])
         prodext[0:4] = rim_in[0:4, :LANES]
         prodext[32:36] = rim_in[4:8, :LANES]
         docext[0:4] = rim_in[0:4, LANES:]
@@ -597,6 +610,7 @@
     conv_out = (gate[...] * mixed).astype(BF16)
     acts[:, :LANES] = halves(nn, unperm, conv_out).astype(BF16)
     send(acts.at[theirs, conv_lanes], pacts.at[:, conv_lanes], one_s.at[3], one_r.at[3], c=other)
+    owe(pacts.at[:, conv_lanes], one_s.at[3])
 
     columns = total_depth // 4
 
@@ -606,9 +620,7 @@
         return ref[cut // 2, cut % 2, :, lanes]
 
     phase("peer_w_wait")
-    for turn in range(most // 2 + 1):
-        peer_wait(turn)
-    settled = len(sent)
+    arrived(wpeer, peer_r.at[0])
     for cut in (0, 2, 1, 3):
         phase(f"out_proj{cut}")
         total = nt(acts[mine, :], quarter(wall, cut, slice(4 * LANES, 6 * LANES)))
@@ -620,34 +632,34 @@
         part[cut] = total.astype(BF16).reshape(PARTS, ROWS // 2, columns)
         way, turn = cut // 2, cut % 2
         target = (xp, xm)[way]
-        send(part.at[cut, xo], relay.at[way, turn], rs_s.at[way, turn], rs_r.at[way, turn], x=target)
+        send(part.at[cut, xo], relay.at[way, turn], rs_s.at[0], rs_r.at[2 * way + turn], x=target)
     for turn in range(2):
-        send(part.at[2 + turn, xp], final.at[0, 2 + turn], rs_s.at[0, 2 + turn], rs_r.at[0, 2 + turn], x=xp)
-        send(part.at[turn, xm], final.at[1, turn], rs_s.at[1, 2 + turn], rs_r.at[1, 2 + turn], x=xm)
-    for copy in sent[:settled]:
-        copy.wait_send()
+        send(part.at[2 + turn, xp], final.at[0, 2 + turn], rs_s.at[0], rs_r.at[6 + turn], x=xp)
+        send(part.at[turn, xm], final.at[1, turn], rs_s.at[0], rs_r.at[4 + turn], x=xm)
+    for which in range(3):
+        count = sum(ring_blocks(which, k) for k in range(most // 2))
+        owe(blocks_view(wall, count, lanes_of[which]), ring_s.at[which])
+    owe(wpeer, peer_s.at[0])
+    settle()
     for turn in range(2):
         for way, target in ((0, xp), (1, xm)):
             phase(f"relay{way}{turn}")
             cut = 2 * way + turn
-            arrived(relay.at[way, turn], rs_r.at[way, turn])
+            arrived(relay.at[way, turn], rs_r.at[2 * way + turn])
             both = part[cut, target].astype(F32) + relay[way, turn].astype(F32)
             part[cut, target] = both.astype(BF16)
-            send(part.at[cut, target], final.at[way, cut], rs_s.at[way, 4 + turn], rs_r.at[way, 4 + turn], x=target)
+            send(part.at[cut, target], final.at[way, cut], rs_s.at[0], rs_r.at[4 + cut], x=target)
     for cut in (0, 2, 1, 3):
         phase(f"final{cut}")
-        summed_way, turn = cut // 2, cut % 2
-        arrived(final.at[1 - summed_way, cut], rs_r.at[1 - summed_way, 2 + turn])
-        arrived(final.at[summed_way, cut], rs_r.at[summed_way, 4 + turn])
+        arrived(final.at[:, cut], rs_r.at[4 + cut])
         value = part[cut, x].astype(F32) + final[0, cut].astype(F32) + final[1, cut].astype(F32)
         out[:, cut * columns : (cut + 1) * columns] = value.astype(BF16)
     phase("drain")
-    for copy in sent[settled:]:
-        copy.wait_send()
+    arrived(part.at[pl.ds(0, 3)], rs_s.at[0])
 
     @pl.when(here == 0)
     def _():
-        arrived(rim_in, one_r.at[1])
+        arrived(rim_in, one_r.at[2])
 
     for d in range(1, nz):
 
@@ -670,7 +682,6 @@
     hbm = pl.BlockSpec(memory_space=pltpu.HBM)
     dma = pltpu.SemaphoreType.DMA
     steps = max(nz, ny) // 2
-    most = max(nz, ny)
     return pl.pallas_call(
         functools.partial(mixer_kernel, nz, ny, depth),
         out_shape=jax.ShapeDtypeStruct((ROWS // 2, 4 * columns), BF16),
@@ -711,17 +722,17 @@
             pltpu.VMEM((4, PARTS, ROWS // 2, columns), BF16),
             pltpu.VMEM((2, 2, ROWS // 2, columns), BF16),
             pltpu.VMEM((2, 4, ROWS // 2, columns), BF16),
-            dma((18,)),
-            dma((2, 3)), dma((2, 3)),
-            dma((4,)), dma((4,)),
-            dma((3,)), dma((3,)),
+            dma((9,)),
+            dma((1,)), dma((2, 3)),
+            dma((1,)), dma((PARTS,)),
+            dma((1,)), dma((1,)),
             dma((5,)), dma((5,)),
-            dma((2, 2, most)), dma((2, 2, most)),
-            dma((2, 2, steps + 1)), dma((2, 2, steps + 1)),
-            dma((3, 2, 2, steps)), dma((3, 2, 2, steps)),
-            dma((steps + 1, 4)), dma((steps + 1, 4)),
-            dma((2, most)), dma((2, most)),
-            dma((2, 6)), dma((2, 6)),
+            dma((2, 2)), dma((2, 2)),
+            dma((2, 2)), dma((2, 2)),
+            dma((3,)), dma((3, steps)),
+            dma((1,)), dma((1,)),
+            dma((nz,)), dma((nz,)),
+            dma((1,)), dma((8,)),
         ],
         compiler_params=pltpu.CompilerParams(
             collective_id=0, has_side_effects=True, vmem_limit_bytes=40 * 1024 * 1024

time: 61.3 us -> 58.9 us (0.961)
  Pallas kernels: 60.5 us -> 58.1 us
    pallas_call x1, Pallas kernels: 60.5 us -> 58.1 us  [shards(): pl.pallas_call(functools.partial(mixer_kernel, nz, ny, depth), out_shape=...]
where the time goes in v5:
time: 58.9 us; the launch traced here: 58.8 us
  Pallas kernels  58.1 us (99%)
  local copies, waits for them, and re-layouts  0.71 us (1%)
    pallas_call x1, Pallas kernels, shards(): pl.pallas_call(functools.partial(mixer_kernel, nz, ny, depth), out_shape=...  58.1 us

profile of v5, /device:TPU:1, one launch (start us, length us, event | category | flops | bytes accessed | tf_op | source)
XLA Modules:
  0.0 58.8 jit_solution(11821701720352201685)
XLA Ops:
  0.0 58.1 %mixer.1 = bf16[64,2048]{1,0:T(8,128)(2,1)S(1)} custom-call(bf16[128,1024]{1,0:T(8,128)(2,1)} %tok_in.1, bf16[32,512]{1,0:T(8,128)(2,1)} %w_in_0.1, bf16[32,512]{1,0:T(8,128)(2,1)} %w_in_1.1, bf16[32,512]{1,0:T(8,128)(2,1)} %w_in_2.1, bf16[32,512]{1,0:T(8,128)(2,1)} %w_in_3.1, bf16[32,512]{1,0:T(8,128)(2,1)} %bitcast.10, bf16[32,512]{1,0:T(8,128)(2,1)} %bitcast.11, ...), custom_call_target="tpu_custom_call" | custom-call | tf_op jit(solution)/shard_map/mixer/pallas_call | solution.py:685
  58.1 0.7 %copy.20 = bf16[64,2048]{1,0:T(8,128)(2,1)} copy(bf16[64,2048]{1,0:T(8,128)(2,1)S(1)} %mixer.1) | data formatting | bytes 524288

commit v6 on v5

--- a/solution.py
+++ b/solution.py
@@ -41,10 +41,10 @@
 def mixer_kernel(
     nz, ny, depth, tok_in, w_in_0, w_in_1, w_in_2, w_in_3, w_in_4, w_in_5, doc_in, gain_in,
     decay_in, freq_in, step_in, in_re, in_im, read_re, read_im, taps_in, skip_in, out,
-    rates, step_row, mats, taps, skip, lam, tok, gains, gain_rows, docs, wall, wpeer, normed, perm, unperm, bmat, rmat, driven, pushed,
+    rates, step_row, mats, taps, skip, lam, tok, gains, gain_rows, docs, wall_s, wall_c, wall_o, wpeer, normed, perm, unperm, bmat, rmat, driven, pushed,
     docext, prodext, gate, ends, chain1, chain2, incoming, links, rim_out, rim_in, acts, pacts,
     part, relay, final, local_sem, tok_s, tok_r, d2d_s, d2d_r, doc_s, doc_r, one_s, one_r,
-    ph_s, ph_r, st_s, st_r, ring_s, ring_r, peer_s, peer_r, ch_s, ch_r, rs_s, rs_r,
+    ph_s, ph_r, st_s, st_r, ring_s, ring_r, peer_s, peer_r, rs_s, rs_r,
 ):
     z, y = lax.axis_index("sp_0"), lax.axis_index("sp_1")
     x, c = lax.axis_index("fs"), lax.axis_index("tp")
@@ -114,8 +114,9 @@
     own_channels = pl.ds(pl.multiple_of(x * LANES, LANES), LANES)
     own_groups = pl.ds(pl.multiple_of(x * 8, 8), 8)
     moves = [(tok_in, tok.at[x, c], 0), (doc_in, docs.at[x], 1), (gain_in, gains.at[c], 2)]
-    for k, w in enumerate((w_in_0, w_in_1, w_in_2, w_in_3, w_in_4, w_in_5)):
-        moves.append((w.at[:, own_channels], wall.at[z, y, :, pl.ds(k * LANES, LANES)], 3))
+    places = [(wall_s, 0, 3)] + [(wall_c, k, 9) for k in range(3)] + [(wall_o, k, 10) for k in range(2)]
+    for w, (wall, k, index) in zip((w_in_0, w_in_1, w_in_2, w_in_3, w_in_4, w_in_5), places):
+        moves.append((w.at[:, own_channels], wall.at[z, y, :, pl.ds(k * LANES, LANES)], index))
     moves += [(decay_in.at[own_groups], rates.at[0], 4), (freq_in.at[own_groups], rates.at[1], 4)]
     for k, m in enumerate((in_re, in_im, read_re, read_im)):
         moves.append((m.at[own_groups], mats.at[k], 5))
@@ -124,8 +125,10 @@
     for source, target, k in moves:
         pltpu.make_async_copy(source, target, local_sem.at[k]).start()
     phase("enter")
-    for k, ref in enumerate((tok.at[x, c], docs.at[x], gains.at[c], wall.at[z, y])):
+    for k, ref in enumerate((tok.at[x, c], docs.at[x], gains.at[c], wall_s.at[z, y])):
         arrived(ref, local_sem.at[k])
+    for k, ref in enumerate((wall_c.at[z, y], wall_o.at[z, y])):
+        arrived(ref, local_sem.at[9 + k])
     phase("barrier")
     pl.semaphore_wait(barrier, count)
 
@@ -133,7 +136,7 @@
 
     def column_copy(d):
         return pltpu.make_async_remote_copy(
-            src_ref=chain2.at[z], dst_ref=chain2.at[z], send_sem=ch_s.at[d], recv_sem=ch_r.at[d],
+            src_ref=chain2.at[z], dst_ref=chain2.at[z], send_sem=one_s.at[5], recv_sem=one_r.at[5],
             device_id={"sp_0": wrap(z + d, nz)}, device_id_type=pl.DeviceIdType.MESH,
         )
 
@@ -157,25 +160,30 @@
 
     phase("first_sends")
     rows_a, rows_b = pl.ds(0, half), pl.ds(half, half)
-    first_lanes, later_lanes = pl.ds(0, LANES), pl.ds(LANES, 5 * LANES)
-
-    def spread_view(lanes, ab):
+
+    def blocks_view(wall, count):
+        if count > nz * ny:
+            return wall.at[pl.ds(0, count // (2 * ny))]
+        if count % ny:
+            return wall.at[0, pl.ds(0, count // 2)]
+        return wall.at[pl.ds(0, count // ny), :, rows_a]
+
+    def spread_view(wall, ab):
         if ab == 0:
-            return wall.at[0, pl.ds(0, ny - 1), rows_a, lanes]
-        return wall.at[pl.ds(0, nz - 1), 0, rows_b, lanes]
-
-    def spread_out(turn, lanes):
+            return wall.at[0, pl.ds(0, ny - 1), rows_a]
+        return wall.at[pl.ds(0, nz - 1), 0, rows_b]
+
+    def spread_out(turn, wall):
         for d in range(1, ny):
-            ref = wall.at[z, y, rows_a, lanes]
-            send(ref, ref, ph_s.at[turn, 0], ph_r.at[turn, 0], y=wrap(y + d, ny))
+            ref = wall.at[z, y, rows_a]
+            send(ref, ref, ph_s.at[turn], ph_r.at[turn, 0], y=wrap(y + d, ny))
         for d in range(1, nz):
-            ref = wall.at[z, y, rows_b, lanes]
-            send(ref, ref, ph_s.at[turn, 1], ph_r.at[turn, 1], z=wrap(z + d, nz))
-        for ab in range(2):
-            owe(spread_view(lanes, ab), ph_s.at[turn, ab])
-
-    def spread_in(turn, lanes, ab):
-        arrived(spread_view(lanes, ab), ph_r.at[turn, ab])
+            ref = wall.at[z, y, rows_b]
+            send(ref, ref, ph_s.at[turn], ph_r.at[turn, 1], z=wrap(z + d, nz))
+        owe(blocks_view(wall, ny - 1 + nz - 1), ph_s.at[turn])
+
+    def spread_in(turn, wall, ab):
+        arrived(spread_view(wall, ab), ph_r.at[turn, ab])
 
     for v in (xp, xm, xo):
         send(docs.at[x], docs.at[x], doc_s.at[0], doc_r.at[0], x=v)
@@ -184,13 +192,14 @@
     owe(gains.at[c], one_s.at[0])
     owe(tok.at[pl.ds(0, PARTS - 1), 0], tok_s.at[0])
     owe(tok.at[:, 0], d2d_s.at[0])
-    spread_out(0, first_lanes)
+    spread_out(0, wall_s)
     token_start(x, low, 0, 0)
     token_start(x, high, 1, 0)
     pass_over(x, 0)
-    spread_out(1, later_lanes)
+    spread_out(1, wall_c)
     token_start(x, high, 0, 1)
     token_start(x, low, 1, 1)
+    spread_out(2, wall_o)
 
     phase("tables")
     shape = (ALL, ALL)
@@ -247,15 +256,14 @@
     rmat[:, :STATES] = jnp.where(own_state, widened(mats[2].reshape(LANES, 64)), 0.0).astype(BF16)
     rmat[:, STATES:] = jnp.where(own_state, -widened(mats[3].reshape(LANES, 64)), 0.0).astype(BF16)
 
-    def ring_ref(ab, source, lanes, piece):
+    def ring_ref(ab, source, wall, piece):
         count = (ny, nz)[ab]
         cut = {0: pl.ds(0, count), 1: pl.ds(0, count // 2), 2: pl.ds(count // 2, count // 2)}[piece]
         if ab == 0:
-            return wall.at[source, cut, rows_a, lanes]
-        return wall.at[cut, source, rows_b, lanes]
-
-    lanes_of = (pl.ds(LANES, 3 * LANES), pl.ds(LANES, 3 * LANES), pl.ds(4 * LANES, 2 * LANES))
-    out_lanes = lanes_of[2]
+            return wall.at[source, cut, rows_a]
+        return wall.at[cut, source, rows_b]
+
+    walls = (wall_c, wall_c, wall_o)
 
     def ring_hops(which, k):
         for ab in range(2):
@@ -270,20 +278,15 @@
     def ring_start(which, k):
         for ab, way, me, size, piece in ring_hops(which, k):
             sign = 1 - 2 * way
-            ref = ring_ref(ab, wrap(me - sign * k, size), lanes_of[which], piece)
+            ref = ring_ref(ab, wrap(me - sign * k, size), walls[which], piece)
             send(ref, ref, ring_s.at[which], ring_r.at[which, k], **{"zy"[ab]: wrap(me + sign, size)})
-
-    def blocks_view(array, count, lanes):
-        if count > nz * ny:
-            return array.at[pl.ds(0, count // (2 * ny)), :, :, lanes]
-        return array.at[pl.ds(0, count // ny), :, rows_a, lanes]
 
     def ring_blocks(which, k):
         return sum((ny, nz)[ab] // (2 if piece else 1) for ab, _, _, _, piece in ring_hops(which, k))
 
     def ring_wait(which, k):
         if ring_blocks(which, k):
-            arrived(blocks_view(wall, ring_blocks(which, k), lanes_of[which]), ring_r.at[which, k])
+            arrived(blocks_view(walls[which], ring_blocks(which, k)), ring_r.at[which, k])
 
     def state_hops(ab, stage):
         me, size = ((z, nz), (y, ny))[ab]
@@ -299,18 +302,16 @@
         for way, d, piece, me, size in state_hops(ab, stage):
             sign = 1 - 2 * way
             source = wrap(me - sign * 2, size) if stage else me
-            ref = ring_ref(ab, source, first_lanes, piece)
+            ref = ring_ref(ab, source, wall_s, piece)
             target = wrap(me + sign * (d - 2 * stage), size)
-            send(ref, ref, st_s.at[ab, stage], st_r.at[ab, stage], **{"zy"[ab]: target})
-        if state_blocks(ab, stage):
-            owe(blocks_view(wall, state_blocks(ab, stage), first_lanes), st_s.at[ab, stage])
+            send(ref, ref, st_s.at[0], st_r.at[ab, stage], **{"zy"[ab]: target})
 
     def state_blocks(ab, stage):
         return sum((ny, nz)[ab] // (2 if piece else 1) for _, _, piece, _, _ in state_hops(ab, stage))
 
     def state_wait(ab, stage):
         if state_blocks(ab, stage):
-            arrived(blocks_view(wall, state_blocks(ab, stage), first_lanes), st_r.at[ab, stage])
+            arrived(blocks_view(wall_s, state_blocks(ab, stage)), st_r.at[ab, stage])
 
     def service(which, k):
         ring_wait(which, k)
@@ -329,7 +330,7 @@
 
     def peer_start(turn):
         for p in peer_pieces(turn):
-            send(wall.at[(*p, out_lanes)], wpeer.at[p], peer_s.at[0], peer_r.at[0], c=other)
+            send(wall_o.at[p], wpeer.at[p], peer_s.at[0], peer_r.at[0], c=other)
 
     width = 2 * tok.shape[3]
 
@@ -355,7 +356,7 @@
     norm(x)
     phase("phase1_state")
     for ab in range(2):
-        spread_in(0, first_lanes, ab)
+        spread_in(0, wall_s, ab)
         state_start(ab, 0)
     phase("tok_forward")
     token_wait(xm, low, 0, 0)
@@ -363,11 +364,10 @@
     token_wait(xp, high, 1, 0)
     token_start(xp, high, 1, 2)
     phase("phase1_rest")
-    spread_in(1, later_lanes, 0)
-    spread_in(1, later_lanes, 1)
-    for which in range(3):
+    spread_in(1, wall_c, 0)
+    spread_in(1, wall_c, 1)
+    for which in range(2):
         ring_start(which, 0)
-    peer_start(0)
     phase("tok_wait1")
     token_wait(xm, high, 0, 1)
     pass_over(xm, 1)
@@ -389,6 +389,11 @@
     docext[4:32] = docext[64 + 448 : 64 + 476]
     docext[36:64] = docext[64 + 480 : 64 + 508]
 
+    phase("phase1_out")
+    spread_in(2, wall_o, 0)
+    spread_in(2, wall_o, 1)
+    ring_start(2, 0)
+    peer_start(0)
     phase("state_stage")
     for ab in range(2):
         state_wait(ab, 0)
@@ -418,7 +423,7 @@
         state_wait(ab, 1)
     phase("state_in")
     total_depth = nz * ny * depth
-    state_in = wall[:, :, :, :LANES].reshape(total_depth, LANES)
+    state_in = wall_s[...].reshape(total_depth, LANES)
     in_order = halves(nn, perm, halves(nn, normed, state_in).astype(BF16))
     driven[...] = in_order
     phase("ring_ab1")
@@ -525,7 +530,7 @@
         service(1, k)
 
     phase("conv_in")
-    conv_in = wall[:, :, :, LANES : 4 * LANES].reshape(total_depth, 3 * LANES)
+    conv_in = wall_c[...].reshape(total_depth, 3 * LANES)
     projected = nn(perm[...], nn(normed[...], conv_in).astype(BF16))
     gate[...] = projected[:, :LANES]
     prodext[64:] = (projected[:, LANES : 2 * LANES] * projected[:, 2 * LANES :]).astype(BF16).astype(F32)
@@ -537,17 +542,13 @@
     prodext[36:64] = prodext[64 + 480 : 64 + 508]
     send(rim_out, rim_in, one_s.at[2], one_r.at[2], z=after_z, y=after_y)
     owe(rim_out, one_s.at[2])
-    phase("ring_o3")
-    for k in range(3, most // 2):
-        service(2, k)
-        peer_start(k + 1)
     phase("chain2_wait")
     incoming[:, :STATES], incoming[:, STATES:] = nothing
     for d in range(1, nz):
 
-        @pl.when(z >= d)
+        @pl.when(z == d)
         def _(d=d):
-            arrived(chain2.at[z - d], ch_r.at[d])
+            arrived(chain2.at[pl.ds(0, d)], one_r.at[5])
 
     phase("chain2_fold")
 
@@ -588,6 +589,11 @@
     send(acts.at[theirs, ssm_lanes], pacts.at[:, ssm_lanes], one_s.at[4], one_r.at[4], c=other)
     owe(pacts.at[:, ssm_lanes], one_s.at[4])
 
+    phase("ring_o3")
+    for k in range(3, most // 2):
+        service(2, k)
+        peer_start(k + 1)
+
     phase("rim_wait")
     docext[0:4] = jnp.full((4, LANES), -1.0, F32)
     prodext[0:4] = jnp.zeros((4, LANES), F32)
@@ -614,21 +620,21 @@
 
     columns = total_depth // 4
 
-    def quarter(ref, cut, lanes):
+    def quarter(ref, cut):
         if nz % 4 == 0:
-            return ref[cut * nz // 4 : (cut + 1) * nz // 4, :, :, lanes].reshape(columns, 2 * LANES)
-        return ref[cut // 2, cut % 2, :, lanes]
+            return ref[cut * nz // 4 : (cut + 1) * nz // 4].reshape(columns, 2 * LANES)
+        return ref[cut // 2, cut % 2]
 
     phase("peer_w_wait")
     arrived(wpeer, peer_r.at[0])
     for cut in (0, 2, 1, 3):
         phase(f"out_proj{cut}")
-        total = nt(acts[mine, :], quarter(wall, cut, slice(4 * LANES, 6 * LANES)))
+        total = nt(acts[mine, :], quarter(wall_o, cut))
         if cut == 0:
             phase("pact_wait")
             arrived(pacts.at[:, ssm_lanes], one_r.at[4])
             arrived(pacts.at[:, conv_lanes], one_r.at[3])
-        total = total + nt(pacts[...], quarter(wpeer, cut, slice(None)))
+        total = total + nt(pacts[...], quarter(wpeer, cut))
         part[cut] = total.astype(BF16).reshape(PARTS, ROWS // 2, columns)
         way, turn = cut // 2, cut % 2
         target = (xp, xm)[way]
@@ -638,7 +644,8 @@
         send(part.at[turn, xm], final.at[1, turn], rs_s.at[0], rs_r.at[4 + turn], x=xm)
     for which in range(3):
         count = sum(ring_blocks(which, k) for k in range(most // 2))
-        owe(blocks_view(wall, count, lanes_of[which]), ring_s.at[which])
+        owe(blocks_view(walls[which], count), ring_s.at[which])
+    owe(blocks_view(wall_s, sum(state_blocks(ab, stage) for ab in range(2) for stage in range(2))), st_s.at[0])
     owe(wpeer, peer_s.at[0])
     settle()
     for turn in range(2):
@@ -663,9 +670,9 @@
 
     for d in range(1, nz):
 
-        @pl.when(z + d < nz)
+        @pl.when(z + d == nz - 1)
         def _(d=d):
-            column_copy(d).wait_send()
+            arrived(chain2.at[pl.ds(0, d)], one_s.at[5])
 
     phase(None)
 
@@ -698,7 +705,9 @@
             pltpu.VMEM((2, width // LANES, LANES), BF16),
             pltpu.VMEM((2, 1, width), F32),
             pltpu.VMEM((PARTS, 1, ROWS), jnp.int32),
-            pltpu.VMEM((nz, ny, depth, 6 * LANES), BF16),
+            pltpu.VMEM((nz, ny, depth, LANES), BF16),
+            pltpu.VMEM((nz, ny, depth, 3 * LANES), BF16),
+            pltpu.VMEM((nz, ny, depth, 2 * LANES), BF16),
             pltpu.VMEM((nz, ny, depth, 2 * LANES), BF16),
             pltpu.VMEM((ALL, 2 * width), BF16),
             pltpu.VMEM((ALL, ALL), BF16),
@@ -722,16 +731,15 @@
             pltpu.VMEM((4, PARTS, ROWS // 2, columns), BF16),
             pltpu.VMEM((2, 2, ROWS // 2, columns), BF16),
             pltpu.VMEM((2, 4, ROWS // 2, columns), BF16),
-            dma((9,)),
+            dma((11,)),
             dma((1,)), dma((2, 3)),
             dma((1,)), dma((PARTS,)),
             dma((1,)), dma((1,)),
-            dma((5,)), dma((5,)),
-            dma((2, 2)), dma((2, 2)),
-            dma((2, 2)), dma((2, 2)),
+            dma((6,)), dma((6,)),
+            dma((3,)), dma((3, 2)),
+            dma((1,)), dma((2, 2)),
             dma((3,)), dma((3, steps)),
             dma((1,)), dma((1,)),
-            dma((nz,)), dma((nz,)),
             dma((1,)), dma((8,)),
         ],
         compiler_params=pltpu.CompilerParams(

time: 58.9 us -> 57.3 us (0.973)
  Pallas kernels: 58.1 us -> 56.5 us
    pallas_call x1, Pallas kernels: 58.1 us -> 56.5 us  [shards(): pl.pallas_call(functools.partial(mixer_kernel, nz, ny, depth), out_shape=...]
where the time goes in v6:
time: 57.3 us; the launch traced here: 57.2 us
  Pallas kernels  56.5 us (99%)
  local copies, waits for them, and re-layouts  0.71 us (1%)
    pallas_call x1, Pallas kernels, shards(): pl.pallas_call(functools.partial(mixer_kernel, nz, ny, depth), out_shape=...  56.5 us

profile of v6, /device:TPU:1, one launch (start us, length us, event | category | flops | bytes accessed | tf_op | source)
XLA Modules:
  0.0 57.2 jit_solution(2005811971964779925)
XLA Ops:
  0.0 56.5 %mixer.1 = bf16[64,2048]{1,0:T(8,128)(2,1)S(1)} custom-call(bf16[128,1024]{1,0:T(8,128)(2,1)} %tok_in.1, bf16[32,512]{1,0:T(8,128)(2,1)} %w_in_0.1, bf16[32,512]{1,0:T(8,128)(2,1)} %w_in_1.1, bf16[32,512]{1,0:T(8,128)(2,1)} %w_in_2.1, bf16[32,512]{1,0:T(8,128)(2,1)} %w_in_3.1, bf16[32,512]{1,0:T(8,128)(2,1)} %bitcast.10, bf16[32,512]{1,0:T(8,128)(2,1)} %bitcast.11, ...), custom_call_target="tpu_custom_call" | custom-call | tf_op jit(solution)/shard_map/mixer/pallas_call | solution.py:692
  56.5 0.7 %copy.20 = bf16[64,2048]{1,0:T(8,128)(2,1)} copy(bf16[64,2048]{1,0:T(8,128)(2,1)S(1)} %mixer.1) | data formatting | bytes 524288

commit v7 on v6

--- a/solution.py
+++ b/solution.py
@@ -42,9 +42,9 @@
     nz, ny, depth, tok_in, w_in_0, w_in_1, w_in_2, w_in_3, w_in_4, w_in_5, doc_in, gain_in,
     decay_in, freq_in, step_in, in_re, in_im, read_re, read_im, taps_in, skip_in, out,
     rates, step_row, mats, taps, skip, lam, tok, gains, gain_rows, docs, wall_s, wall_c, wall_o, wpeer, normed, perm, unperm, bmat, rmat, driven, pushed,
-    docext, prodext, gate, ends, chain1, chain2, incoming, links, rim_out, rim_in, acts, pacts,
+    docext, prodext, gate, ends, chain1, chain2, incoming, links, rimtok, rimdoc, rimprod, acts, pacts,
     part, relay, final, local_sem, tok_s, tok_r, d2d_s, d2d_r, doc_s, doc_r, one_s, one_r,
-    ph_s, ph_r, st_s, st_r, ring_s, ring_r, peer_s, peer_r, rs_s, rs_r,
+    ph_s, ph_r, st_s, st_r, ring_s, ring_r, peer_s, peer_r, rs_s, rs_r, rim_s, rim_r,
 ):
     z, y = lax.axis_index("sp_0"), lax.axis_index("sp_1")
     x, c = lax.axis_index("fs"), lax.axis_index("tp")
@@ -200,6 +200,11 @@
     token_start(x, high, 0, 1)
     token_start(x, low, 1, 1)
     spread_out(2, wall_o)
+    last_rows = tok.at[x, c, pl.ds(ROWS - 16, 16)]
+    send(last_rows, rimtok.at[x, c], rim_s.at[0], rim_r.at[0], z=after_z, y=after_y)
+    send(docs.at[x], rimdoc.at[x], rim_s.at[1], rim_r.at[1], z=after_z, y=after_y)
+    owe(last_rows, rim_s.at[0])
+    owe(docs.at[x], rim_s.at[1])
 
     phase("tables")
     shape = (ALL, ALL)
@@ -415,6 +420,14 @@
     passed_over(xo, 3)
     norm(xo)
 
+    arrived(rimtok.at[x, c], rim_r.at[0])
+    arrived(rimdoc.at[x], rim_r.at[1])
+    for v in (xp, xm, xo):
+        send(rimtok.at[x, c], rimtok.at[x, c], rim_s.at[2], rim_r.at[2], x=v)
+        send(rimdoc.at[x], rimdoc.at[x], rim_s.at[3], rim_r.at[3], x=v)
+    owe(rimtok.at[pl.ds(0, PARTS - 1), 0], rim_s.at[2])
+    owe(rimdoc.at[pl.ds(0, PARTS - 1)], rim_s.at[3])
+
     phase("ring_o0")
     service(2, 0)
     peer_start(1)
@@ -424,11 +437,15 @@
     phase("state_in")
     total_depth = nz * ny * depth
     state_in = wall_s[...].reshape(total_depth, LANES)
-    in_order = halves(nn, perm, halves(nn, normed, state_in).astype(BF16))
+    in_order = halves(nn, perm, halves(nn, normed[:ALL], state_in).astype(BF16))
     driven[...] = in_order
     phase("ring_ab1")
     service(0, 1)
     service(1, 1)
+    arrived(rimtok.at[pl.ds(0, PARTS - 1), 0], rim_r.at[2])
+    arrived(rimdoc.at[pl.ds(0, PARTS - 1)], rim_r.at[3])
+    send(rimtok.at[:, c], rimtok.at[:, c], rim_s.at[4], rim_r.at[4], c=other)
+    owe(rimtok.at[:, c], rim_s.at[4])
     phase("push")
     pushed[...] = nn(in_order.astype(BF16), bmat[...])
 
@@ -509,6 +526,18 @@
     service(2, 1)
     peer_start(2)
 
+    phase("rim_norm")
+    arrived(rimtok.at[:, other], rim_r.at[4])
+    for q in range(PARTS):
+        a, b = rimtok[q, 0].astype(F32), rimtok[q, 1].astype(F32)
+        mean = (jnp.sum(a * a, axis=1, keepdims=True) + jnp.sum(b * b, axis=1, keepdims=True)) / width
+        scale = lax.rsqrt(mean + EPS)
+        target = slice(ALL + 16 * q, ALL + 16 * q + 16)
+        normed[target, : width // 2] = (a * scale * gain_rows[0]).astype(BF16)
+        normed[target, width // 2 :] = (b * scale * gain_rows[1]).astype(BF16)
+        at_two = lax.broadcasted_iota(jnp.int32, (1, ROWS), 1) == ROWS - 2
+        two_back = jnp.sum(jnp.where(at_two, rimdoc[q].astype(F32), 0.0), axis=1, keepdims=True)
+        docext[q : q + 1] = jnp.broadcast_to(jnp.where(here == 0, -1.0, two_back), (1, LANES))
     phase("ring_ab2")
     service(0, 2)
     service(1, 2)
@@ -531,17 +560,17 @@
 
     phase("conv_in")
     conv_in = wall_c[...].reshape(total_depth, 3 * LANES)
-    projected = nn(perm[...], nn(normed[...], conv_in).astype(BF16))
+    straight = nn(normed[...], conv_in).astype(BF16)
+    ahead = straight[ALL:].astype(F32)
+    rimprod[...] = (ahead[:, LANES : 2 * LANES] * ahead[:, 2 * LANES :]).astype(BF16).astype(F32)
+    projected = nn(perm[...], straight[:ALL])
     gate[...] = projected[:, :LANES]
     prodext[64:] = (projected[:, LANES : 2 * LANES] * projected[:, 2 * LANES :]).astype(BF16).astype(F32)
-    rim_out[0:4, :LANES] = prodext[64 + 476 : 64 + 480]
-    rim_out[4:8, :LANES] = prodext[64 + 508 : 64 + 512]
-    rim_out[0:4, LANES:] = docext[64 + 476 : 64 + 480]
-    rim_out[4:8, LANES:] = docext[64 + 508 : 64 + 512]
+    for q in range(PARTS):
+        prodext[q : q + 1] = rimprod[16 * q + 14 : 16 * q + 15]
+        prodext[32 + q : 33 + q] = rimprod[16 * q + 15 : 16 * q + 16]
     prodext[4:32] = prodext[64 + 448 : 64 + 476]
     prodext[36:64] = prodext[64 + 480 : 64 + 508]
-    send(rim_out, rim_in, one_s.at[2], one_r.at[2], z=after_z, y=after_y)
-    owe(rim_out, one_s.at[2])
     phase("chain2_wait")
     incoming[:, :STATES], incoming[:, STATES:] = nothing
     for d in range(1, nz):
@@ -593,18 +622,6 @@
     for k in range(3, most // 2):
         service(2, k)
         peer_start(k + 1)
-
-    phase("rim_wait")
-    docext[0:4] = jnp.full((4, LANES), -1.0, F32)
-    prodext[0:4] = jnp.zeros((4, LANES), F32)
-    prodext[32:36] = jnp.zeros((4, LANES), F32)
-
-    @pl.when(here > 0)
-    def _():
-        arrived(rim_in, one_r.at[2])
-        prodext[0:4] = rim_in[0:4, :LANES]
-        prodext[32:36] = rim_in[4:8, :LANES]
-        docext[0:4] = rim_in[0:4, LANES:]
 
     phase("conv")
     now = docext[64:]
@@ -664,10 +681,6 @@
     phase("drain")
     arrived(part.at[pl.ds(0, 3)], rs_s.at[0])
 
-    @pl.when(here == 0)
-    def _():
-        arrived(rim_in, one_r.at[2])
-
     for d in range(1, nz):
 
         @pl.when(z + d == nz - 1)
@@ -709,7 +722,7 @@
             pltpu.VMEM((nz, ny, depth, 3 * LANES), BF16),
             pltpu.VMEM((nz, ny, depth, 2 * LANES), BF16),
             pltpu.VMEM((nz, ny, depth, 2 * LANES), BF16),
-            pltpu.VMEM((ALL, 2 * width), BF16),
+            pltpu.VMEM((ALL + 16 * PARTS, 2 * width), BF16),
             pltpu.VMEM((ALL, ALL), BF16),
             pltpu.VMEM((ALL, ALL), BF16),
             pltpu.VMEM((LANES, 2 * STATES), BF16),
@@ -724,8 +737,9 @@
             pltpu.VMEM((nz, 16, STATES // 2 + LANES), BF16),
             pltpu.VMEM((8, STATES + LANES), F32),
             pltpu.VMEM((16, 8, STATES), F32),
-            pltpu.VMEM((8, 2 * LANES), F32),
-            pltpu.VMEM((8, 2 * LANES), F32),
+            pltpu.VMEM((PARTS, 2, 16, width), BF16),
+            pltpu.VMEM((PARTS, 1, ROWS), jnp.int32),
+            pltpu.VMEM((16 * PARTS, LANES), F32),
             pltpu.VMEM((ALL, 2 * LANES), BF16),
             pltpu.VMEM((ALL // 2, 2 * LANES), BF16),
             pltpu.VMEM((4, PARTS, ROWS // 2, columns), BF16),
@@ -741,6 +755,7 @@
             dma((3,)), dma((3, steps)),
             dma((1,)), dma((1,)),
             dma((1,)), dma((8,)),
+            dma((5,)), dma((5,)),
         ],
         compiler_params=pltpu.CompilerParams(
             collective_id=0, has_side_effects=True, vmem_limit_bytes=40 * 1024 * 1024

time: 57.3 us -> 57.7 us (level)
  no operation moved by 1% of the time
where the time goes in v7:
time: 57.7 us; the launch traced here: 57.6 us
  Pallas kernels  56.9 us (99%)
  local copies, waits for them, and re-layouts  0.71 us (1%)
    pallas_call x1, Pallas kernels, shards(): pl.pallas_call(functools.partial(mixer_kernel, nz, ny, depth), out_shape=...  56.9 us

profile of v7, /device:TPU:1, one launch (start us, length us, event | category | flops | bytes accessed | tf_op | source)
XLA Modules:
  0.0 57.6 jit_solution(11273926496194875026)
XLA Ops:
  0.0 56.9 %mixer.1 = bf16[64,2048]{1,0:T(8,128)(2,1)S(1)} custom-call(bf16[128,1024]{1,0:T(8,128)(2,1)} %tok_in.1, bf16[32,512]{1,0:T(8,128)(2,1)} %w_in_0.1, bf16[32,512]{1,0:T(8,128)(2,1)} %w_in_1.1, bf16[32,512]{1,0:T(8,128)(2,1)} %w_in_2.1, bf16[32,512]{1,0:T(8,128)(2,1)} %w_in_3.1, bf16[32,512]{1,0:T(8,128)(2,1)} %bitcast.10, bf16[32,512]{1,0:T(8,128)(2,1)} %bitcast.11, ...), custom_call_target="tpu_custom_call" | custom-call | tf_op jit(solution)/shard_map/mixer/pallas_call | solution.py:705
  56.9 0.7 %copy.20 = bf16[64,2048]{1,0:T(8,128)(2,1)} copy(bf16[64,2048]{1,0:T(8,128)(2,1)S(1)} %mixer.1) | data formatting | bytes 524288

commit v8 on v7

--- a/solution.py
+++ b/solution.py
@@ -535,9 +535,11 @@
         target = slice(ALL + 16 * q, ALL + 16 * q + 16)
         normed[target, : width // 2] = (a * scale * gain_rows[0]).astype(BF16)
         normed[target, width // 2 :] = (b * scale * gain_rows[1]).astype(BF16)
-        at_two = lax.broadcasted_iota(jnp.int32, (1, ROWS), 1) == ROWS - 2
-        two_back = jnp.sum(jnp.where(at_two, rimdoc[q].astype(F32), 0.0), axis=1, keepdims=True)
-        docext[q : q + 1] = jnp.broadcast_to(jnp.where(here == 0, -1.0, two_back), (1, LANES))
+        for back in (2, 1):
+            there = lax.broadcasted_iota(jnp.int32, (1, ROWS), 1) == ROWS - back
+            number = jnp.sum(jnp.where(there, rimdoc[q].astype(F32), 0.0), axis=1, keepdims=True)
+            target = 32 * (2 - back) + q
+            docext[target : target + 1] = jnp.broadcast_to(jnp.where(here == 0, -1.0, number), (1, LANES))
     phase("ring_ab2")
     service(0, 2)
     service(1, 2)
@@ -571,6 +573,21 @@
         prodext[32 + q : 33 + q] = rimprod[16 * q + 15 : 16 * q + 16]
     prodext[4:32] = prodext[64 + 448 : 64 + 476]
     prodext[36:64] = prodext[64 + 480 : 64 + 508]
+    mine, theirs = (pl.ds(pl.multiple_of(v * (ALL // 2), ALL // 2), ALL // 2) for v in (c, other))
+    conv_lanes, ssm_lanes = pl.ds(0, LANES), pl.ds(LANES, LANES)
+
+    phase("conv")
+    now = docext[64:]
+    mixed = (
+        taps[0:1].astype(F32) * prodext[0:ALL] * ones_where(docext[0:ALL] == now)
+        + taps[1:2].astype(F32) * prodext[32 : 32 + ALL] * ones_where(docext[32 : 32 + ALL] == now)
+        + taps[2:3].astype(F32) * prodext[64:]
+    )
+    conv_out = (gate[...] * mixed).astype(BF16)
+    acts[:, :LANES] = halves(nn, unperm, conv_out).astype(BF16)
+    send(acts.at[theirs, conv_lanes], pacts.at[:, conv_lanes], one_s.at[3], one_r.at[3], c=other)
+    owe(pacts.at[:, conv_lanes], one_s.at[3])
+
     phase("chain2_wait")
     incoming[:, :STATES], incoming[:, STATES:] = nothing
     for d in range(1, nz):
@@ -589,7 +606,6 @@
         incoming[:, :STATES], incoming[:, STATES:] = lax.fori_loop(0, z, step, nothing)
 
     state = fold((incoming[:, :STATES], incoming[:, STATES:]), of(chain1), ny, y, 2)
-    docext[32:36] = state[1][0:4]
     for seg in range(8):
         links[seg] = state[0]
         state = joined(state, of_ends(seg), 1)
@@ -613,27 +629,12 @@
     inner = 0.7978845608028654 * (reading + 0.044715 * (reading * reading * reading))
     ssm_out = (0.5 * reading * (1.0 + jnp.tanh(inner))).astype(BF16)
     acts[:, LANES:] = halves(nn, unperm, ssm_out).astype(BF16)
-    mine, theirs = (pl.ds(pl.multiple_of(v * (ALL // 2), ALL // 2), ALL // 2) for v in (c, other))
-    conv_lanes, ssm_lanes = pl.ds(0, LANES), pl.ds(LANES, LANES)
     send(acts.at[theirs, ssm_lanes], pacts.at[:, ssm_lanes], one_s.at[4], one_r.at[4], c=other)
     owe(pacts.at[:, ssm_lanes], one_s.at[4])
-
     phase("ring_o3")
     for k in range(3, most // 2):
         service(2, k)
         peer_start(k + 1)
-
-    phase("conv")
-    now = docext[64:]
-    mixed = (
-        taps[0:1].astype(F32) * prodext[0:ALL] * ones_where(docext[0:ALL] == now)
-        + taps[1:2].astype(F32) * prodext[32 : 32 + ALL] * ones_where(docext[32 : 32 + ALL] == now)
-        + taps[2:3].astype(F32) * prodext[64:]
-    )
-    conv_out = (gate[...] * mixed).astype(BF16)
-    acts[:, :LANES] = halves(nn, unperm, conv_out).astype(BF16)
-    send(acts.at[theirs, conv_lanes], pacts.at[:, conv_lanes], one_s.at[3], one_r.at[3], c=other)
-    owe(pacts.at[:, conv_lanes], one_s.at[3])
 
     columns = total_depth // 4
 

time: 57.7 us -> 57.4 us (level)
  no operation moved by 1% of the time
where the time goes in v8:
time: 57.4 us; the launch traced here: 57.2 us
  Pallas kernels  56.5 us (98%)
  local copies, waits for them, and re-layouts  0.71 us (1%)
    pallas_call x1, Pallas kernels, shards(): pl.pallas_call(functools.partial(mixer_kernel, nz, ny, depth), out_shape=...  56.5 us

profile of v8, /device:TPU:1, one launch (start us, length us, event | category | flops | bytes accessed | tf_op | source)
XLA Modules:
  0.0 57.2 jit_solution(882851537028451313)
XLA Ops:
  0.0 56.5 %mixer.1 = bf16[64,2048]{1,0:T(8,128)(2,1)S(1)} custom-call(bf16[128,1024]{1,0:T(8,128)(2,1)} %tok_in.1, bf16[32,512]{1,0:T(8,128)(2,1)} %w_in_0.1, bf16[32,512]{1,0:T(8,128)(2,1)} %w_in_1.1, bf16[32,512]{1,0:T(8,128)(2,1)} %w_in_2.1, bf16[32,512]{1,0:T(8,128)(2,1)} %w_in_3.1, bf16[32,512]{1,0:T(8,128)(2,1)} %bitcast.10, bf16[32,512]{1,0:T(8,128)(2,1)} %bitcast.11, ...), custom_call_target="tpu_custom_call" | custom-call | tf_op jit(solution)/shard_map/mixer/pallas_call | solution.py:706
  56.5 0.7 %copy.20 = bf16[64,2048]{1,0:T(8,128)(2,1)} copy(bf16[64,2048]{1,0:T(8,128)(2,1)S(1)} %mixer.1) | data formatting | bytes 524288
